TPU v7x, 128 devices: a whole 4x4x4 slice. The times are simulated.
128 devices in a mesh: ep: 16 (over z, x), tp: 8 (over y, core).
Axes of the slice: x: 4, y: 4, z: 4, core: 2. Of those that a mesh axis runs over, the one named last changes fastest.
Arguments:
- mix_tokens: bfloat16 [16384, 2048], P('ep'), may hold values from -6 to 6
- mix_gain: float32 [2048], replicated, may hold values from 0.1 to 1.9
- w_query: bfloat16 [2048, 2048], P(None, 'tp'), may hold values from -0.125 to 0.125
- w_forget_fwd: bfloat16 [2048, 2048], P(None, 'tp'), may hold values from -0.125 to 0.125
- w_forget_bwd: bfloat16 [2048, 2048], P(None, 'tp'), may hold values from -0.125 to 0.125
- w_value: bfloat16 [2048, 2048], P(None, 'tp'), may hold values from -0.125 to 0.125
- decay_floor: float32 [2048], P('tp'), may hold values from 0.975 to 1
- decay_shift: float32 [16384, 16], P('ep', 'tp'), may hold values from -1.3 to 0
- head_gain: float32 [128], replicated, may hold values from 0.1 to 1.9
- w_out: bfloat16 [2048, 2048], replicated, may hold values from -0.125 to 0.125
- moe_tokens: bfloat16 [6144, 2048], P('ep'), may hold values from -6 to 6
- moe_gain: float32 [2048], replicated, may hold values from 0.1 to 1.9
- routes: int32 [6144, 2], P('ep'), may hold values from 0 to 15, all different within a row; in each aligned block of 384 rows (0 to 383, 384 to 767, ...) at most 72 rows name the same one
- route_logits: float32 [6144, 2], P('ep'), may hold values from -6 to 6
- w_expert_gate: bfloat16 [16, 2048, 5120], P('ep', None, 'tp'), may hold values from -0.125 to 0.125
- w_expert_up: bfloat16 [16, 2048, 5120], P('ep', None, 'tp'), may hold values from -0.125 to 0.125
- w_expert_down: bfloat16 [16, 5120, 2048], P('ep', 'tp'), may hold values from -0.078125 to 0.078125
Outputs:
- mixed_out: bfloat16 [16384, 2048], P(('ep', 'tp'))
- moe_out: bfloat16 [6144, 2048], P('ep', 'tp')
Inputs may be any that keep to these rules, and one draw needn't show every extreme that they name: `routes`: in each aligned block of 384 rows (the rows of one index of ep) no expert is named by more than 72 rows, and in some block an expert is named by exactly 72; the two entries of a row differ.
All inputs are finite; a program needn't handle non-finite values.
Results may differ from a plain program's by a relative error of at most 0.014.
Values may be sent and summed in bfloat16 or wider, within the bound.
No kernel may reach another device: no remote copies, remote signals or barrier semaphores. Data moves between devices by JAX's collectives and lax.ppermute only.
A program may use at most 128 MiB of HBM per device.

v0:
```python
import math

import jax
import jax.numpy as jnp
from jax import lax
from jax.sharding import Mesh
from jax.sharding import PartitionSpec as P

DK = 128
DV = 128
EP = ("ep_0", "ep_1")
EP_TP = ("ep_0", "ep_1", "tp")


EPSILON = 1e-06


def nothing_yet(value, identity):
    return jax.tree.map(
        lambda a, e: jnp.broadcast_to(jnp.asarray(e, a.dtype), a.shape), value, identity
    )


def prefix_by_axis(value, axes, combine, identity, reverse):
    before = start = nothing_yet(value, identity)
    total = value
    for axis in reversed(axes):
        count, index = (lax.axis_size(axis), lax.axis_index(axis))
        pieces = jax.tree.map(
            lambda part, kind: lax.all_gather(part.astype(kind), axis),
            total,
            (jnp.bfloat16, jnp.bfloat16),
        )
        inside, total = (start, start)
        for k in reversed(range(count)) if reverse else range(count):
            passed = k > index if reverse else k < index
            total = combine(
                total, jax.tree.map(lambda part, own: part[k].astype(own.dtype), pieces, value)
            )
            inside = jax.tree.map(lambda new, old: jnp.where(passed, new, old), total, inside)
        before = combine(inside, before)
    return before


def rms_rows(array, norm_gain):
    floats = array.astype(jnp.float32)
    factor = lax.rsqrt(jnp.mean(floats * floats, axis=-1, keepdims=True) + EPSILON)
    return floats * factor * norm_gain


def decay_terms(pre_act, lower_bound, shifts, head_count):
    squashed = jax.nn.sigmoid(pre_act.astype(jnp.float32))
    key_rows = (1.0 - lower_bound)[None, :] * (1.0 - squashed)
    key_rows = key_rows.reshape(key_rows.shape[0], head_count, key_rows.shape[1] // head_count)
    log_decay = jnp.log1p(-key_rows) + shifts[:, :, None]
    return (key_rows, log_decay)


def sweep_forward(queries, key_rows, values, log_decay, blk_rows):
    token_count, head_count, key_width = queries.shape
    value_width = values.shape[2]
    block_count = token_count // blk_rows
    lower_mask = jnp.tril(jnp.ones((blk_rows, blk_rows), jnp.float32))

    def to_blocks(array):
        return array.reshape(block_count, blk_rows, head_count, array.shape[2])

    def advance(carried, block):
        states, offset = carried
        block_q, block_k, block_v, block_g = block
        running = jnp.cumsum(block_g, axis=0)
        query_grown = block_q * jnp.exp(running)
        key_shrunk = block_k * jnp.exp(-running)
        scores = jnp.einsum("thd,shd->hts", query_grown, key_shrunk) * lower_mask[None]
        result = jnp.einsum("hts,shv->thv", scores, block_v) + jnp.einsum(
            "thd,hdv->thv", query_grown, states
        )
        block_end = running[-1]
        states = jnp.exp(block_end)[:, :, None] * states + jnp.einsum(
            "shd,shv->hdv", block_k * jnp.exp(block_end[None] - running), block_v
        )
        return ((states, offset + block_end), (result, offset[None] + running))

    starting = (
        jnp.zeros((head_count, key_width, value_width), jnp.float32),
        jnp.zeros((head_count, key_width), jnp.float32),
    )
    blocks_in = (to_blocks(queries), to_blocks(key_rows), to_blocks(values), to_blocks(log_decay))
    (states, totals), (results, cumulative) = lax.scan(advance, starting, blocks_in)
    return (
        results.reshape(token_count, head_count, value_width),
        cumulative.reshape(token_count, head_count, key_width),
        totals,
        states,
    )


def sweep_back(queries, key_rows, values, log_decay, blk_rows):
    token_count, head_count, key_width = queries.shape
    value_width = values.shape[2]
    block_count = token_count // blk_rows
    upper_mask = jnp.triu(jnp.ones((blk_rows, blk_rows), jnp.float32))

    def to_blocks(array):
        return array.reshape(block_count, blk_rows, head_count, array.shape[2])

    def advance(carried, block):
        states, offset = carried
        block_q, block_k, block_v, block_g = block
        block_sum = jnp.sum(block_g, axis=0)
        suffix = block_sum[None] - jnp.cumsum(block_g, axis=0) + block_g
        query_grown = block_q * jnp.exp(suffix)
        key_shrunk = block_k * jnp.exp(-suffix)
        scores = jnp.einsum("thd,shd->hts", query_grown, key_shrunk) * upper_mask[None]
        result = jnp.einsum("hts,shv->thv", scores, block_v) + jnp.einsum(
            "thd,hdv->thv", query_grown, states
        )
        states = jnp.exp(block_sum)[:, :, None] * states + jnp.einsum(
            "shd,shv->hdv", block_k * jnp.exp(block_sum[None] - suffix), block_v
        )
        return ((states, offset + block_sum), (result, offset[None] + suffix))

    starting = (
        jnp.zeros((head_count, key_width, value_width), jnp.float32),
        jnp.zeros((head_count, key_width), jnp.float32),
    )
    blocks_in = (to_blocks(queries), to_blocks(key_rows), to_blocks(values), to_blocks(log_decay))
    (states, totals), (results, cumulative) = lax.scan(advance, starting, blocks_in, reverse=True)
    return (
        results.reshape(token_count, head_count, value_width),
        cumulative.reshape(token_count, head_count, key_width),
        totals,
        states,
    )


def chain_join(earlier, later):
    return (earlier[0] + later[0], jnp.exp(later[0])[:, :, None] * earlier[1] + later[1])


def slot_positions(route_rows, expert_count, capacity):
    flattened = route_rows.reshape(-1)
    onehot = (flattened[:, None] == jnp.arange(expert_count, dtype=jnp.int32)[None, :]).astype(
        jnp.int32
    )
    before = jnp.cumsum(onehot, axis=0) - onehot
    slot_rank = jnp.sum(before * onehot, axis=1)
    return (flattened * capacity + slot_rank).reshape(route_rows.shape)


def body(
    mix_tokens,
    mix_gain,
    w_query,
    w_forget_fwd,
    w_forget_bwd,
    w_value,
    decay_floor,
    decay_shift,
    head_gain,
    w_out,
    moe_tokens,
    moe_gain,
    routes,
    route_logits,
    w_expert_gate,
    w_expert_up,
    w_expert_down,
):
    tp_size = lax.axis_size("tp")
    ep_size = lax.axis_size(EP)
    seg_rows = mix_tokens.shape[0]
    head_count = w_query.shape[1] // DK
    blk_rows = math.gcd(seg_rows, 128)
    normed = rms_rows(mix_tokens, mix_gain).astype(jnp.bfloat16)

    def project(weight):
        return jnp.dot(normed, weight, preferred_element_type=jnp.float32).astype(jnp.bfloat16)

    queries = jax.nn.silu(project(w_query).astype(jnp.float32)).reshape(seg_rows, head_count, DK)
    values = project(w_value).astype(jnp.float32).reshape(seg_rows, head_count, DV)
    keys_fwd, forward_log_decay = decay_terms(
        project(w_forget_fwd), decay_floor, decay_shift, head_count
    )
    keys_bwd, logs_bwd = decay_terms(project(w_forget_bwd), decay_floor, decay_shift, head_count)
    out_fwd, cum_fwd, total_fwd, summary_fwd = sweep_forward(
        queries, keys_fwd, values, forward_log_decay, blk_rows
    )
    out_bwd, cum_bwd, total_bwd, summary_bwd = sweep_back(
        queries, keys_bwd, values, logs_bwd, blk_rows
    )
    identity = (jnp.zeros_like(total_fwd), jnp.zeros_like(summary_fwd))
    incoming_fwd = prefix_by_axis((total_fwd, summary_fwd), EP, chain_join, identity, False)[1]
    incoming_bwd = prefix_by_axis((total_bwd, summary_bwd), EP, chain_join, identity, True)[1]
    grown_both = jnp.stack([queries * jnp.exp(cum_fwd), queries * jnp.exp(cum_bwd)], axis=2)
    carried_both = jnp.stack([incoming_fwd, incoming_bwd], axis=1)
    combined = out_fwd + out_bwd + jnp.einsum("thed,hedv->thv", grown_both, carried_both)
    readout = rms_rows(combined, head_gain).reshape(seg_rows, head_count * DV).astype(jnp.bfloat16)
    regrouped = lax.all_to_all(readout, "tp", split_axis=0, concat_axis=1, tiled=True)
    mixed_out = jnp.dot(regrouped, w_out, preferred_element_type=jnp.float32).astype(jnp.bfloat16)
    token_rows = moe_tokens.shape[0]
    model_cols = moe_tokens.shape[1]
    pick_count = routes.shape[1]
    capacity = 3 * token_rows // ep_size
    part_cols = model_cols // tp_size
    normed_moe = rms_rows(moe_tokens, moe_gain).astype(jnp.bfloat16)
    position = slot_positions(routes, ep_size, capacity)
    local_rows = jnp.arange(pick_count * token_rows, dtype=jnp.int32) // pick_count
    slot_token = (
        jnp.full((ep_size * capacity,), token_rows, jnp.int32)
        .at[position.reshape(-1)]
        .set(local_rows)
    )
    gate_weight = w_expert_gate[0]
    up_weight = w_expert_up[0]
    down_weight = w_expert_down[0]
    own_cols = lax.dynamic_slice_in_dim(normed_moe, lax.axis_index("tp") * part_cols, part_cols, 1)
    padded = jnp.concatenate([own_cols, jnp.zeros((1, part_cols), jnp.bfloat16)], axis=0)
    outgoing = padded[slot_token].reshape(ep_size, capacity, part_cols)
    arrived = lax.all_to_all(outgoing, EP, split_axis=0, concat_axis=0, tiled=True)
    pieces = lax.all_gather(arrived, "tp", axis=2, tiled=True)
    flattened = pieces.reshape(-1, pieces.shape[2])
    gate_acts = jnp.dot(flattened, gate_weight, preferred_element_type=jnp.float32)
    up_acts = jnp.dot(flattened, up_weight, preferred_element_type=jnp.float32)
    hidden = (jax.nn.silu(gate_acts) * up_acts).astype(jnp.bfloat16)
    partial_value = jnp.dot(hidden, down_weight, preferred_element_type=jnp.float32)
    summed = lax.psum_scatter(
        partial_value.astype(jnp.bfloat16), "tp", scatter_dimension=1, tiled=True
    )
    returned = lax.all_to_all(
        summed.reshape(ep_size, capacity, part_cols), EP, split_axis=0, concat_axis=0, tiled=True
    )
    flat_back = returned.reshape(ep_size * capacity, part_cols)
    picked = flat_back[position].astype(jnp.float32)
    weights = jax.nn.sigmoid(route_logits - jnp.flip(route_logits, 1))
    moe_out = jnp.sum(picked * weights[:, :, None], axis=1).astype(jnp.bfloat16)
    return (mixed_out, moe_out)


def solution(mesh):
    finer = Mesh(mesh.devices.reshape(4, 4, mesh.shape["tp"]), ("ep_0", "ep_1", "tp"))
    return jax.shard_map(
        body,
        mesh=finer,
        in_specs=(
            P(EP, None),
            P(),
            P(None, "tp"),
            P(None, "tp"),
            P(None, "tp"),
            P(None, "tp"),
            P("tp"),
            P(EP, "tp"),
            P(),
            P(),
            P(EP, None),
            P(),
            P(EP, None),
            P(EP, None),
            P(EP, None, "tp"),
            P(EP, None, "tp"),
            P(EP, "tp", None),
        ),
        out_specs=(P(EP_TP, None), P(EP, "tp")),
        check_vma=False,
    )
```

profile of v0, /device:TPU:0, one launch (start us, length us, event | category | flops | bytes accessed | tf_op | source)
XLA Modules:
  0.0 330.4 jit_solution(3483865044686736720)
XLA Ops:
  7.2 3.6 %convert_element_type.559 = f32[384,2048]{1,0:T(8,128)} convert(bf16[384,2048]{1,0:T(8,128)(2,1)} %param.31) | non-fusion elementwise | flops 786432 | bytes 4718592 | tf_op jit(solution)/shard_map/convert_element_type | solution.py:46
  14.8 3.4 %scatter_custom_fusion = s32[1152]{0:T(1024)S(1)} fusion(s32[768]{0:T(1024)S(1)} %fusion.161, s32[768]{0:T(1024)S(1)} %add_select_fusion, s32[]{:T(128)} %constant.148.clone.1), kind=kCustom, calls=%fused_computation.233 | custom fusion | bytes 4612 | tf_op jit(solution)/shard_map/scatter | solution.py:212
  20.2 4.6 %gather_fusion = bf16[1152,256]{1,0:T(8,128)(2,1)} fusion(bf16[385,256]{1,0:T(8,128)(2,1)S(1)} %concatenate.3, s32[2048]{0:T(1024)S(1)} %pad_clamp_fusion), kind=kCustom, calls=%fused_computation | custom fusion | bytes 1184256 | tf_op jit(solution)/shard_map/gather | solution.py:219
  24.8 8.0 %all-to-all-start.1 = ((bf16[16,72,256]{2,1,0:T(8,128)(2,1)}), bf16[16,72,256]{2,1,0:T(8,128)(2,1)S(1)}, u32[]{:S(2)}, u32[]{:S(2)}) async-start(bf16[16,72,256]{2,1,0:T(8,128)(2,1)} %bitcast.468), calls=%async_computation.1 | async-start | bytes 1179648 | tf_op jit(solution)/shard_map/all_to_all | solution.py:220
  33.1 3.2 fusion.60
  37.7 2.2 fusion.92
  40.0 2.2 fusion.84
  42.2 2.3 convert_multiply_fusion.2
  44.6 2.1 fusion.85
  46.6 2.7 reshape_reshape.17
  49.4 2.7 reshape_reshape.21
  53.1 2.7 reshape_reshape.20
  55.8 2.0 reshape.731
  57.8 1.9 copy.113
  59.7 5.4 %log-plus-one_add_fusion.1 = (f32[8,128,2,128]{3,2,1,0:T(2,128)}, f32[8,128,2,128]{3,2,1,0:T(2,128)}) fusion(f32[8,128,2,128]{3,2,1,0:T(2,128)} %reshape_reshape.17, f32[8,128,2]{2,1,0:T(8,128)} %bitcast.469, f32[8,128,2,128]{3,2,1,0:T(2,128)} %reshape_reshape.21), kind=kLoop, calls=%fused_computation.128 | loop fusion | flops 1048576 | bytes 4202496 | tf_op jit(solution)/shard_map/add | solution.py:55
  68.7 48.9 %while.38 = (s32[]{:T(128)}, f32[2,128,128]{2,1,0:T(8,128)S(1)}, f32[2,128]{1,0:T(2,128)S(1)}, f32[8,128,2,128]{1,3,2,0:T(8,128)}, f32[8,128,2,128]{3,2,1,0:T(2,...) while((s32[]{:T(128)}, f32[2,128,128]{2,1,0:T(8,128)S(1)}, ...), condition=%wide.region_3.4_spmd.clone, body=%wide.region_1.3_spmd.clone.sunk | while | flops 38273536 | bytes 2437757 | solution.py:89
  71.2 1.8 fusion.240
  77.3 1.8 fusion.240
  89.5 1.8 fusion.240
  95.6 1.8 fusion.240
  101.8 1.8 fusion.240
  107.9 1.8 fusion.240
  114.0 1.8 fusion.240
  117.6 8.6 %fusion.66 = f32[1152,640]{1,0:T(8,128)} fusion(bf16[1152,2048]{1,0:T(8,128)(2,1)} %bitcast.474, bf16[1,2048,640]{2,1,0:T(8,128)(2,1)} %param.35), kind=kOutput, calls=%fused_computation.91 | convolution fusion | flops 3019898880 | bytes 10289152 | tf_op jit(solution)/shard_map/dot_general | solution.py:223
  126.2 13.2 %convolution_convert_fusion = bf16[1152,2048]{1,0:T(8,128)(2,1)} fusion(bf16[1,640,2048]{2,1,0:T(8,128)(2,1)S(1)} %copy-done, bf16[1152,2048]{1,0:T(8,128)(2,1)} %bitcast.475, f32[1152,640]{1,0:T(8,128)} %fusion.66, bf16[1,2048,640]{2,1,0:T(8,128)(2,1)} %param.36), kind=kOutput, calls=%fused_computation.85 | convolution fusion | flops 6046580736 | bytes 17629184 | tf_op jit(solution)/shard_map/dot_general | solution.py:226
  141.8 50.8 %while.39 = (s32[]{:T(128)}, f32[2,128,128]{2,1,0:T(8,128)S(1)}, f32[2,128]{1,0:T(2,128)S(1)}, f32[8,128,2,128]{1,3,2,0:T(8,128)}, f32[8,128,2,128]{3,2,1,0:T(2,...) while((s32[]{:T(128)}, f32[2,128,128]{2,1,0:T(8,128)S(1)}, ...), condition=%wide.region_7.8_spmd.clone, body=%wide.region_4.7_spmd.clone.sunk | while | flops 38437124 | bytes 3094181 | solution.py:128
  144.6 1.8 fusion.251
  151.0 1.8 fusion.251
  157.3 1.8 fusion.251
  163.6 1.9 fusion.251
  170.0 1.8 fusion.251
  176.4 1.8 fusion.251
  182.7 1.8 fusion.251
  194.2 13.0 %all-gather.1 = bf16[8,128,128]{2,1,0:T(8,128)(2,1)S(1)} all-gather(bf16[2,128,128]{2,1,0:T(8,128)(2,1)S(1)} %convert_element_type.502), channel_id=3, replica_groups=mesh['ep_0'=4,'ep_1'=4,'tp'=8] {'ep_1'}, dimensions={0}, use_global_device_ids=true | all-gather | bytes 327680 | tf_op jit(solution)/shard_map/all_gather | solution.py:30
  207.8 9.6 %all-gather.4 = bf16[4,2,128]{2,1,0:T(2,128)(2,1)S(1)} all-gather(bf16[1,2,128]{2,1,0:T(2,128)(2,1)S(1)} %convert_bitcast_fusion.17), channel_id=2, replica_groups=mesh['ep_0'=4,'ep_1'=4,'tp'=8] {'ep_1'}, dimensions={0}, use_global_device_ids=true | all-gather | bytes 2560 | tf_op jit(solution)/shard_map/all_gather | solution.py:30
  217.6 12.5 %all_gather.48 = bf16[4,2,128,128]{3,2,1,0:T(8,128)(2,1)S(1)} all-gather(bf16[1,2,128,128]{3,2,1,0:T(8,128)(2,1)S(1)} %copy.121), channel_id=1, replica_groups=mesh['ep_0'=4,'ep_1'=4,'tp'=8] {'ep_0'}, dimensions={0}, use_global_device_ids=true | all-gather | bytes 327680 | tf_op jit(solution)/shard_map/all_gather | solution.py:30
  230.6 12.3 %all-gather.3 = bf16[8,128,128]{2,1,0:T(8,128)(2,1)S(1)} all-gather(bf16[2,128,128]{2,1,0:T(8,128)(2,1)S(1)} %convert_element_type.534), channel_id=5, replica_groups=mesh['ep_0'=4,'ep_1'=4,'tp'=8] {'ep_1'}, dimensions={0}, use_global_device_ids=true | all-gather | bytes 327680 | tf_op jit(solution)/shard_map/all_gather | solution.py:30
  243.4 7.0 %all-gather.5 = bf16[4,2,128]{2,1,0:T(2,128)(2,1)S(1)} all-gather(bf16[1,2,128]{2,1,0:T(2,128)(2,1)S(1)} %convert_bitcast_fusion.16), channel_id=4, replica_groups=mesh['ep_0'=4,'ep_1'=4,'tp'=8] {'ep_1'}, dimensions={0}, use_global_device_ids=true | all-gather | bytes 2560 | tf_op jit(solution)/shard_map/all_gather | solution.py:30
  250.7 12.5 %all_gather.54 = bf16[4,2,128,128]{3,2,1,0:T(8,128)(2,1)S(1)} all-gather(bf16[1,2,128,128]{3,2,1,0:T(8,128)(2,1)S(1)} %copy.134), channel_id=1, replica_groups=mesh['ep_0'=4,'ep_1'=4,'tp'=8] {'ep_0'}, dimensions={0}, use_global_device_ids=true | all-gather | bytes 327680 | tf_op jit(solution)/shard_map/all_gather | solution.py:30
  265.1 9.5 %all_gather.45 = bf16[4,2,128]{2,1,0:T(2,128)(2,1)S(1)} all-gather(bf16[1,2,128]{2,1,0:T(2,128)(2,1)S(1)} %get-tuple-element.469), channel_id=1, replica_groups=mesh['ep_0'=4,'ep_1'=4,'tp'=8] {'ep_0'}, dimensions={0}, use_global_device_ids=true | all-gather | bytes 2560 | tf_op jit(solution)/shard_map/all_gather | solution.py:30
  274.6 7.0 %all_gather.51 = bf16[4,2,128]{2,1,0:T(2,128)(2,1)S(1)} all-gather(bf16[1,2,128]{2,1,0:T(2,128)(2,1)S(1)} %get-tuple-element.479), channel_id=1, replica_groups=mesh['ep_0'=4,'ep_1'=4,'tp'=8] {'ep_0'}, dimensions={0}, use_global_device_ids=true | all-gather | bytes 2560 | tf_op jit(solution)/shard_map/all_gather | solution.py:30
  283.8 4.5 %all-to-all-start = ((bf16[8,128,256]{1,2,0:T(8,128)(2,1)}), bf16[8,128,256]{1,2,0:T(8,128)(2,1)S(1)}, u32[]{:S(2)}, u32[]{:S(2)}) async-start(bf16[8,128,256]{1,2,0:T(8,128)(2,1)} %copy.146), calls=%async_computation | async-start | bytes 1048576 | tf_op jit(solution)/shard_map/all_to_all | solution.py:199
  288.6 10.0 %all-to-all-done = bf16[8,128,256]{1,2,0:T(8,128)(2,1)S(1)} async-done(((bf16[8,128,256]{1,2,0:T(8,128)(2,1)}), bf16[8,128,256]{1,2,0:T(8,128)(2,1)S(1)}, u32[]{:S(2)}, u32[]{:S(2)}) %all-to-all-start) | async-done | bytes 524320 | tf_op jit(solution)/shard_map/all_to_all | solution.py:199
  299.5 4.9 %all-to-all-start.2 = ((bf16[16,72,256]{2,1,0:T(8,128)(2,1)}), bf16[16,72,256]{2,1,0:T(8,128)(2,1)S(1)}, u32[]{:S(2)}, u32[]{:S(2)}) async-start(bf16[16,72,256]{2,1,0:T(8,128)(2,1)} %bitcast.472), calls=%async_computation.3 | async-start | bytes 1179648 | tf_op jit(solution)/shard_map/all_to_all | solution.py:230
  305.2 5.8 %convolution_convert_fusion.1 = bf16[128,2048]{1,0:T(8,128)(2,1)} fusion(bf16[128,2048]{0,1:T(8,128)(2,1)} %bitcast.465, bf16[2048,2048]{1,0:T(8,128)(2,1)} %param.30), kind=kOutput, calls=%fused_computation.93 | convolution fusion | flops 1074003968 | bytes 9437184 | tf_op jit(solution)/shard_map/dot_general | solution.py:200
  311.0 5.3 %all-to-all-done.2 = bf16[16,72,256]{2,1,0:T(8,128)(2,1)S(1)} async-done(((bf16[16,72,256]{2,1,0:T(8,128)(2,1)}), bf16[16,72,256]{2,1,0:T(8,128)(2,1)S(1)}, u32[]{:S(2)}, u32[]{:S(2)}) %all-to-all-start.2) | async-done | bytes 589856 | tf_op jit(solution)/shard_map/all_to_all | solution.py:230
  316.3 3.3 gather_fusion.1
  320.9 2.7 multiply_reduce_fusion.2
  (271 shorter events, 98.7 us)
Async XLA Ops:
  7.2 119.1 %copy-start = (bf16[1,640,2048]{2,1,0:T(8,128)(2,1)S(1)}, bf16[1,640,2048]{2,1,0:T(8,128)(2,1)}, u32[]{:S(2)}) copy-start(bf16[1,640,2048]{2,1,0:T(8,128)(2,1)} %param.37) | copy-start | bytes 7864324
  7.2 3.6 %copy-start.4 = (bf16[384,2048]{1,0:T(8,128)(2,1)S(1)}, bf16[384,2048]{1,0:T(8,128)(2,1)}, u32[]{:S(2)}) copy-start(bf16[384,2048]{1,0:T(8,128)(2,1)} %param.31) | copy-start | bytes 4718596
  7.2 4.0 %copy-start.17 = (s32[384,2]{0,1:T(2,128)S(1)}, s32[384,2]{0,1:T(2,128)}, u32[]{:S(2)}) copy-start(s32[384,2]{0,1:T(2,128)} %param.33) | copy-start | bytes 9220
  20.2 16.1 %copy-start.18 = (f32[256]{0:T(256)S(1)}, f32[256]{0:T(256)}, u32[]{:S(2)}) copy-start(f32[256]{0:T(256)} %param.27) | copy-start | bytes 3076
  20.2 16.2 %copy-start.15 = (f32[2048]{0:T(1024)S(1)}, f32[2048]{0:T(1024)}, u32[]{:S(2)}) copy-start(f32[2048]{0:T(1024)} %param.22) | copy-start | bytes 24580
  24.8 40.3 %all-to-all-start.1 = ((bf16[16,72,256]{2,1,0:T(8,128)(2,1)}), bf16[16,72,256]{2,1,0:T(8,128)(2,1)S(1)}, u32[]{:S(2)}, u32[]{:S(2)}) async-start(bf16[16,72,256]{2,1,0:T(8,128)(2,1)} %bitcast.468), calls=%async_computation.1 | async-start | bytes 1179648 | tf_op jit(solution)/shard_map/all_to_all | solution.py:220
  32.8 84.8 %all-gather.8.cloned.1.call-start = ((), (), s32[]{:S(2)}) async-start(), calls=%async_computation.4 | async-start | bytes 5308416 | tf_op jit(solution)/shard_map/all_gather | solution.py:221
  33.1 3.5 %copy-start.2 = (bf16[1024,2048]{1,0:T(8,128)(2,1)S(1)}, bf16[1024,2048]{1,0:T(8,128)(2,1)}, u32[]{:S(2)}) copy-start(bf16[1024,2048]{1,0:T(8,128)(2,1)} %param.21) | copy-start | bytes 12582916
  36.5 1.2 copy-start.20
  37.7 2.2 copy-start.21
  40.0 2.3 copy-start.22
  42.2 2.3 copy-start.23
  44.6 7.5 %copy-start.16 = (f32[1024,2]{0,1:T(2,128)S(1)}, f32[1024,2]{0,1:T(2,128)}, u32[]{:S(2)}) copy-start(f32[1024,2]{0,1:T(2,128)} %param.28) | copy-start | bytes 24580
  65.1 0.8 copy-start.12
  66.0 232.7 %reduce-scatter.2.cloned.1.call-start = ((), (), s32[]{:S(2)}) async-start(), calls=%async_computation.5 | async-start | bytes 5308416 | tf_op jit(solution)/shard_map/reduce_scatter | solution.py:227
  139.4 2.4 copy-start.3
  141.8 50.8 %copy-start.6 = (f32[1024,256]{1,0:T(8,128)S(1)}, f32[1024,256]{1,0:T(8,128)}, u32[]{:S(2)}) copy-start(f32[1024,256]{1,0:T(8,128)} %convert_multiply_fusion.2) | copy-start | bytes 3145732
  192.7 71.1 %copy-start.7 = (f32[8,128,2,128]{3,2,1,0:T(2,128)S(1)}, f32[8,128,2,128]{3,2,1,0:T(2,128)}, u32[]{:S(2)}) copy-start(f32[8,128,2,128]{3,2,1,0:T(2,128)} %get-tuple-element.265) | copy-start | bytes 3145732
  230.1 34.3 %copy-start.8 = (f32[8,128,2,128]{3,2,1,0:T(2,128)S(1)}, f32[8,128,2,128]{3,2,1,0:T(2,128)}, u32[]{:S(2)}) copy-start(f32[8,128,2,128]{3,2,1,0:T(2,128)} %get-tuple-element.264) | copy-start | bytes 3145732
  264.3 17.6 %copy-start.9 = (f32[1024,2,1,128]{3,1,0,2:T(2,128)S(1)}, f32[1024,2,1,128]{3,1,0,2:T(2,128)}, u32[]{:S(2)}) copy-start(f32[1024,2,1,128]{3,1,0,2:T(2,128)} %reshape.725) | copy-start | bytes 3145732
  265.0 17.1 %copy-start.10 = (f32[8,128,2,128]{1,3,2,0:T(8,128)S(1)}, f32[8,128,2,128]{1,3,2,0:T(8,128)}, u32[]{:S(2)}) copy-start(f32[8,128,2,128]{1,3,2,0:T(8,128)} %get-tuple-element.259) | copy-start | bytes 3145732
  265.0 17.1 %copy-start.11 = (f32[8,128,2,128]{1,3,2,0:T(8,128)S(1)}, f32[8,128,2,128]{1,3,2,0:T(8,128)}, u32[]{:S(2)}) copy-start(f32[8,128,2,128]{1,3,2,0:T(8,128)} %get-tuple-element.258) | copy-start | bytes 3145732
  281.9 0.8 copy-start.19
  282.1 6.2 %copy-start.13 = (s32[384,2]{1,0:T(8,128)S(1)}, s32[384,2]{1,0:T(8,128)}, u32[]{:S(2)}) copy-start(s32[384,2]{1,0:T(8,128)} %get-tuple-element.463) | copy-start | bytes 9220
  282.1 6.4 %copy-start.14 = (f32[384,2]{0,1:T(2,128)S(1)}, f32[384,2]{0,1:T(2,128)}, u32[]{:S(2)}) copy-start(f32[384,2]{0,1:T(2,128)} %param.34) | copy-start | bytes 9220
  283.8 14.8 %all-to-all-start = ((bf16[8,128,256]{1,2,0:T(8,128)(2,1)}), bf16[8,128,256]{1,2,0:T(8,128)(2,1)S(1)}, u32[]{:S(2)}, u32[]{:S(2)}) async-start(bf16[8,128,256]{1,2,0:T(8,128)(2,1)} %copy.146), calls=%async_computation | async-start | bytes 1048576 | tf_op jit(solution)/shard_map/all_to_all | solution.py:199
  298.7 0.8 copy-start.5
  299.5 16.8 %all-to-all-start.2 = ((bf16[16,72,256]{2,1,0:T(8,128)(2,1)}), bf16[16,72,256]{2,1,0:T(8,128)(2,1)S(1)}, u32[]{:S(2)}, u32[]{:S(2)}) async-start(bf16[16,72,256]{2,1,0:T(8,128)(2,1)} %bitcast.472), calls=%async_computation.3 | async-start | bytes 1179648 | tf_op jit(solution)/shard_map/all_to_all | solution.py:230
  305.2 18.4 %copy-start.1 = (bf16[1,640,2048]{2,1,0:T(8,128)(2,1)S(1)}, bf16[1,640,2048]{2,1,0:T(8,128)(2,1)}, u32[]{:S(2)}) copy-start(bf16[1,640,2048]{2,1,0:T(8,128)(2,1)} %param.37) | copy-start | bytes 7864324
Sparse Core Ops, SparseCore 0:
  66.1 39.4 all-gather.7
  139.5 40.8 reduce-scatter.1
where the time goes:
time: 333 us; the launch traced here: 330 us
  matrix products  86.5 us (26%)
  blocking collectives  83.3 us (25%)
  other arithmetic  70.3 us (21%)
  local copies, waits for them, and re-layouts  41.6 us (12%)
  starting transfers between devices  17.8 us (5%)
  waiting for transfers between devices  15.4 us (5%)
  between operations  14.8 us (4%)
    all_gather x8, blocking collectives, prefix_by_axis(): lax.all_gather(part.astype(kind), axis)  83.3 us
    dot_general x16, matrix products, advance(): jnp.einsum('hts,shv->thv', scores, block_v)  29.3 us
    dot_general x1, matrix products, body(): jnp.dot(hidden, down_weight, preferred_element_type=jnp.float32)  13.2 us
    dynamic_update_slice x16, other arithmetic, sweep_forward(): lax.scan(advance, starting, blocks_in)  11.4 us
    another operation x4, local copies, waits for them, and re-layouts, to_blocks(): return array.reshape(block_count, blk_rows, head_count, array.shape[2])  10.1 us
    all_to_all x1, waiting for transfers between devices, body(): lax.all_to_all(readout, 'tp', split_axis=0, concat_axis=1, tiled=True)  10 us
    mul x8, other arithmetic, advance(): key_shrunk = block_k * jnp.exp(-running)  9.65 us
    mul x8, other arithmetic, advance(): query_grown = block_q * jnp.exp(suffix)  9.2 us
  transfers between devices with their start and end apart: 5, of which 2 were waited for; matrix products, arithmetic and copies ran while one was open for 45% of the time, Pallas kernels for 0%

commit v1 on v0

v1 whole, which is shorter than its diff:
```python
import functools

import jax
import jax.numpy as jnp
from jax import lax
from jax.experimental import pallas as pl
from jax.experimental.pallas import tpu as pltpu
from jax.sharding import Mesh
from jax.sharding import PartitionSpec as P

DK = 128
DV = 128
BLK = 128
EP = ("z", "x")
TP = ("y", "c")
ALL = ("z", "x", "y", "c")
EPSILON = 1e-06
BF = jnp.bfloat16
F32 = jnp.float32
CHUNKS = ((0, 72),)
VMEM_LIMIT = 56 * 1024 * 1024


def params(*semantics):
    return pltpu.CompilerParams(
        dimension_semantics=semantics if semantics else None, vmem_limit_bytes=VMEM_LIMIT
    )


def dot(a, b):
    return jnp.dot(a, b, preferred_element_type=F32)


def dot_nt(a, b):
    return lax.dot_general(a, b, (((1,), (1,)), ((), ())), preferred_element_type=F32)


def dot_tn(a, b):
    return lax.dot_general(a, b, (((0,), (0,)), ((), ())), preferred_element_type=F32)


def rms_scale(floats):
    return lax.rsqrt(jnp.mean(floats * floats, axis=-1, keepdims=True) + EPSILON)


def dispatch_kernel(idx_ref, tok_ref, gain_ref, routes_ref, *outs, chunks, experts):
    half = tok_ref.shape[1] // 2
    rows = tok_ref.shape[0]
    scale = rms_scale(tok_ref[...].astype(F32))
    start = pl.multiple_of(idx_ref[0] * half, half)
    own = tok_ref[:, pl.ds(start, half)].astype(F32)
    normed = (own * scale * gain_ref[:, pl.ds(start, half)]).astype(BF)
    e0 = routes_ref[0:1, :]
    e1 = routes_ref[1:2, :]
    expert_iota = lax.broadcasted_iota(jnp.int32, (experts, rows), 0)
    oh0 = (expert_iota == e0).astype(F32)
    oh1 = (expert_iota == e1).astype(F32)
    earlier = (
        lax.broadcasted_iota(jnp.int32, (rows, rows), 0)
        < lax.broadcasted_iota(jnp.int32, (rows, rows), 1)
    ).astype(F32)
    before = dot((oh0 + oh1).astype(BF), earlier.astype(BF))
    slot0 = jnp.sum(oh0 * before, axis=0, keepdims=True).astype(jnp.int32)
    slot1 = jnp.sum(oh1 * (before + oh0), axis=0, keepdims=True).astype(jnp.int32)
    for out, (first, count) in zip(outs, chunks):
        total = experts * count

        def place(expert, slot):
            inside = (slot >= first) & (slot < first + count)
            return jnp.where(inside, expert * count + slot - first, -1)

        p0 = place(e0, slot0)
        p1 = place(e1, slot1)
        row_iota = lax.broadcasted_iota(jnp.int32, (total, rows), 0)
        chosen = ((row_iota == p0) | (row_iota == p1)).astype(F32).astype(BF)
        out[...] = dot(chosen, normed).astype(BF)


def dispatch(idx, tokens, gain, routes_t, experts):
    half = tokens.shape[1] // 2
    return pl.pallas_call(
        functools.partial(dispatch_kernel, chunks=CHUNKS, experts=experts),
        out_shape=tuple(jax.ShapeDtypeStruct((experts * n, half), BF) for _, n in CHUNKS),
        in_specs=[
            pl.BlockSpec(memory_space=pltpu.SMEM),
            pl.BlockSpec(memory_space=pltpu.VMEM),
            pl.BlockSpec(memory_space=pltpu.VMEM),
            pl.BlockSpec(memory_space=pltpu.VMEM),
        ],
        out_specs=tuple(pl.BlockSpec(memory_space=pltpu.VMEM) for _ in CHUNKS),
        compiler_params=params(),
        name="dispatch",
    )(idx, tokens, gain, routes_t)


def tri_sum(tri, g):
    high = g.astype(BF)
    low = (g - high.astype(F32)).astype(BF)
    return dot(tri, high) + dot(tri, low)


def local_kernel(
    x_ref,
    gain_ref,
    wq_ref,
    wf_ref,
    wb_ref,
    wv_ref,
    floor_ref,
    shift_ref,
    o_ref,
    qf_ref,
    qb_ref,
    msg_ref,
    q_s,
    v_s,
    kb_s,
    gb_s,
    st_s,
    off_s,
    *,
    steps,
    rows,
    heads,
):
    step = pl.program_id(0)
    width = heads * DK

    @pl.when(step == 0)
    def _():
        st_s[...] = jnp.zeros_like(st_s)
        off_s[...] = jnp.zeros_like(off_s)

    x = x_ref[...].astype(F32)
    normed = (x * rms_scale(x) * gain_ref[...]).astype(BF)

    def project(w_ref):
        return dot(normed, w_ref[...]).astype(BF)

    q_pre = project(wq_ref).astype(F32)
    queries = q_pre * jax.nn.sigmoid(q_pre)
    values = project(wv_ref)
    shift = shift_ref[...]
    shift_wide = jnp.concatenate(
        [jnp.broadcast_to(shift[:, h : h + 1], (rows, DK)) for h in range(heads)], axis=1
    )
    room = 1.0 - floor_ref[...]

    def decay(w_ref):
        keys = room * (1.0 - jax.nn.sigmoid(project(w_ref).astype(F32)))
        return keys, jnp.log1p(-keys) + shift_wide

    keys_f, logs_f = decay(wf_ref)
    keys_b, logs_b = decay(wb_ref)
    base = pl.multiple_of(step * rows, rows)
    q_s[pl.ds(base, rows), :] = queries
    v_s[pl.ds(base, rows), :] = values
    kb_s[pl.ds(base, rows), :] = keys_b
    gb_s[pl.ds(base, rows), :] = logs_b

    row_iota = lax.broadcasted_iota(jnp.int32, (BLK, BLK), 0)
    col_iota = lax.broadcasted_iota(jnp.int32, (BLK, BLK), 1)
    lower = row_iota >= col_iota
    upper = row_iota <= col_iota
    lower_one = lower.astype(F32).astype(BF)
    upper_one = upper.astype(F32).astype(BF)

    def block(q, k, v, g, tri_one, mask, end_row, states, offset):
        run = tri_sum(tri_one, g)
        end = run[end_row : end_row + 1, :]
        grown = q * jnp.exp(run)
        grown_b = grown.astype(BF)
        shrunk = (k * jnp.exp(-run)).astype(BF)
        closing = (k * jnp.exp(end - run)).astype(BF)
        kept = jnp.exp(end)
        result = []
        new_states = []
        for h in range(heads):
            lanes = slice(h * DK, (h + 1) * DK)
            scores = jnp.where(mask, dot_nt(grown_b[:, lanes], shrunk[:, lanes]), 0.0).astype(BF)
            st = states[h]
            result.append(
                dot(scores, v[:, lanes]) + dot_nt(grown_b[:, lanes], st.astype(BF))
            )
            new_states.append(st * kept[:, lanes] + dot_tn(v[:, lanes], closing[:, lanes]))
        carried = (grown * jnp.exp(offset)).astype(BF)
        return jnp.concatenate(result, axis=1), new_states, carried, offset + end

    def write_message(first, states, total):
        kept = jnp.exp(total)
        high = kept.astype(BF)
        low = (kept - high.astype(F32)).astype(BF)
        for h in range(heads):
            lanes = slice(h * DK, (h + 1) * DK)
            tail = jnp.concatenate(
                [high[:, lanes], low[:, lanes], jnp.zeros((6, DK), BF)], axis=0
            )
            for part in range(4):
                msg_ref[first + h * 4 + part, 0:32, :] = states[h][
                    part * 32 : (part + 1) * 32, :
                ].astype(BF)
                msg_ref[first + h * 4 + part, 32:40, :] = tail

    states = [st_s[h] for h in range(heads)]
    offset = off_s[...]
    for b in range(rows // BLK):
        rs = slice(b * BLK, (b + 1) * BLK)
        result, states, carried, offset = block(
            queries[rs], keys_f[rs], values[rs], logs_f[rs], lower_one, lower, BLK - 1, states, offset
        )
        at = pl.multiple_of(base + b * BLK, BLK)
        o_ref[pl.ds(at, BLK), :] = result
        qf_ref[pl.ds(at, BLK), :] = carried
    for h in range(heads):
        st_s[h] = states[h]
    off_s[...] = offset

    @pl.when(step == steps - 1)
    def _():
        write_message(0, states, offset)
        back = [jnp.zeros((DV, DK), F32) for _ in range(heads)]
        total = jnp.zeros((1, width), F32)
        for b in reversed(range(steps * rows // BLK)):
            rs = slice(b * BLK, (b + 1) * BLK)
            result, back, carried, total = block(
                q_s[rs, :], kb_s[rs, :], v_s[rs, :], gb_s[rs, :], upper_one, upper, 0, back, total
            )
            o_ref[rs, :] = o_ref[rs, :] + result
            qb_ref[rs, :] = carried
        write_message(4 * heads, back, total)


def local_sweeps(tokens, gain, wq, wf, wb, wv, floor, shift):
    seg, model = tokens.shape
    width = wq.shape[1]
    heads = width // DK
    rows = 256
    steps = seg // rows
    whole = lambda shape: pl.BlockSpec(shape, lambda i: tuple(0 for _ in shape))
    return pl.pallas_call(
        functools.partial(local_kernel, steps=steps, rows=rows, heads=heads),
        grid=(steps,),
        out_shape=(
            jax.ShapeDtypeStruct((seg, width), F32),
            jax.ShapeDtypeStruct((seg, width), BF),
            jax.ShapeDtypeStruct((seg, width), BF),
            jax.ShapeDtypeStruct((8 * heads, 40, DK), BF),
        ),
        in_specs=[
            pl.BlockSpec((rows, model), lambda i: (i, 0)),
            whole((1, model)),
            whole((model, width)),
            whole((model, width)),
            whole((model, width)),
            whole((model, width)),
            whole((1, width)),
            pl.BlockSpec((rows, heads), lambda i: (i, 0)),
        ],
        out_specs=(
            whole((seg, width)),
            whole((seg, width)),
            whole((seg, width)),
            whole((8 * heads, 40, DK)),
        ),
        scratch_shapes=[
            pltpu.VMEM((seg, width), F32),
            pltpu.VMEM((seg, width), BF),
            pltpu.VMEM((seg, width), F32),
            pltpu.VMEM((seg, width), F32),
            pltpu.VMEM((heads, DV, DK), F32),
            pltpu.VMEM((1, width), F32),
        ],
        compiler_params=params("arbitrary"),
        name="local_sweeps",
    )(tokens, gain, wq, wf, wb, wv, floor, shift)


def scan_kernel(idx_ref, msg_ref, out_ref):
    count = msg_ref.shape[0]
    backward = idx_ref[2] >= count // 2
    state = jnp.zeros((32, DK), F32)
    for i in range(count):
        at = jnp.where(backward, count - 1 - i, i)
        out_ref[at] = state.astype(BF)
        block = msg_ref[at].astype(F32)
        kept = block[32:33, :] + block[33:34, :]
        state = state * kept + block[0:32, :]


def scan_states(idx, message):
    return pl.pallas_call(
        scan_kernel,
        out_shape=jax.ShapeDtypeStruct((message.shape[0], 32, DK), BF),
        in_specs=[
            pl.BlockSpec(memory_space=pltpu.SMEM),
            pl.BlockSpec(memory_space=pltpu.VMEM),
        ],
        out_specs=pl.BlockSpec(memory_space=pltpu.VMEM),
        compiler_params=params(),
        name="scan_states",
    )(idx, message)


def finish_kernel(o_ref, qf_ref, qb_ref, states_ref, gain_ref, out_ref, *, heads):
    for h in range(heads):
        lanes = slice(h * DK, (h + 1) * DK)
        ahead = states_ref[h * DV : (h + 1) * DV, :]
        behind = states_ref[(heads + h) * DV : (heads + h + 1) * DV, :]
        o = (
            o_ref[:, lanes]
            + dot_nt(qf_ref[:, lanes], ahead)
            + dot_nt(qb_ref[:, lanes], behind)
        )
        out_ref[:, lanes] = (o * rms_scale(o) * gain_ref[...]).astype(BF)


def finish(o, qf, qb, states, gain):
    seg, width = o.shape
    rows = 256
    tile = pl.BlockSpec((rows, width), lambda i: (i, 0))
    return pl.pallas_call(
        functools.partial(finish_kernel, heads=width // DK),
        grid=(seg // rows,),
        out_shape=jax.ShapeDtypeStruct((seg, width), BF),
        in_specs=[
            tile,
            tile,
            tile,
            pl.BlockSpec(states.shape, lambda i: (0, 0)),
            pl.BlockSpec((1, DV), lambda i: (0, 0)),
        ],
        out_specs=tile,
        compiler_params=params("arbitrary"),
        name="finish",
    )(o, qf, qb, states, gain)


def project_kernel(r_ref, w_ref, out_ref):
    groups, _, width = r_ref.shape
    rows = jnp.concatenate([r_ref[g] for g in range(groups)], axis=1)
    out_ref[...] = dot(rows, w_ref[...]).astype(BF)


def project_out(regrouped, w_out):
    groups, rows, width = regrouped.shape
    model = w_out.shape[1]
    cols = 512
    return pl.pallas_call(
        project_kernel,
        grid=(model // cols,),
        out_shape=jax.ShapeDtypeStruct((rows, model), BF),
        in_specs=[
            pl.BlockSpec((groups, rows, width), lambda j: (0, 0, 0)),
            pl.BlockSpec((groups * width, cols), lambda j: (0, j)),
        ],
        out_specs=pl.BlockSpec((rows, cols), lambda j: (0, j)),
        compiler_params=params("arbitrary"),
        name="project_out",
    )(regrouped, w_out)


def hidden_kernel(idx_ref, own_ref, other_ref, wg_ref, wu_ref, wd_ref, h_ref, part_ref, *, groups):
    core = idx_ref[0]
    half = own_ref.shape[1]
    cols = part_ref.shape[2]
    mine = pl.ds(pl.multiple_of(core * half, half), half)
    theirs = pl.ds(pl.multiple_of((1 - core) * half, half), half)
    own = own_ref[...]
    other = other_ref[...]
    gate = dot(own, wg_ref[mine, :]) + dot(other, wg_ref[theirs, :])
    up = dot(own, wu_ref[mine, :]) + dot(other, wu_ref[theirs, :])
    hidden = (gate * jax.nn.sigmoid(gate) * up).astype(BF)
    h_ref[...] = hidden
    for g in range(groups):
        start = pl.multiple_of((2 * g + 1 - core) * cols, cols)
        part_ref[g] = dot(hidden, wd_ref[:, pl.ds(start, cols)]).astype(BF)


def expert_hidden(idx, own, other, wg, wu, wd, groups, row_block):
    rows, half = own.shape
    ff = wg.shape[1]
    model = wd.shape[1]
    cols = model // (2 * groups)
    whole = lambda shape: pl.BlockSpec(shape, lambda i, s: tuple(0 for _ in shape))
    return pl.pallas_call(
        functools.partial(hidden_kernel, groups=groups),
        grid_spec=pltpu.PrefetchScalarGridSpec(
            num_scalar_prefetch=1,
            grid=(rows // row_block,),
            in_specs=[
                pl.BlockSpec((row_block, half), lambda i, s: (i, 0)),
                pl.BlockSpec((row_block, half), lambda i, s: (i, 0)),
                whole(wg.shape),
                whole(wu.shape),
                whole(wd.shape),
            ],
            out_specs=(
                pl.BlockSpec((row_block, ff), lambda i, s: (i, 0)),
                pl.BlockSpec((groups, row_block, cols), lambda i, s: (0, i, 0)),
            ),
        ),
        out_shape=(
            jax.ShapeDtypeStruct((rows, ff), BF),
            jax.ShapeDtypeStruct((groups, rows, cols), BF),
        ),
        compiler_params=params("arbitrary"),
        name="expert_hidden",
    )(idx, own, other, wg, wu, wd)


def down_kernel(idx_ref, h_ref, wd_ref, got_ref, out_ref):
    mine = dot(h_ref[...], wd_ref[...]).astype(BF)
    out_ref[0] = (mine.astype(F32) + got_ref[0].astype(F32)).astype(BF)


def expert_down(idx, hidden, wd, received, groups, row_block):
    rows, ff = hidden.shape
    cols = received.shape[2]
    block = lambda d, s: (s[1] + d) % groups
    return pl.pallas_call(
        down_kernel,
        grid_spec=pltpu.PrefetchScalarGridSpec(
            num_scalar_prefetch=1,
            grid=(groups,),
            in_specs=[
                pl.BlockSpec((rows, ff), lambda d, s: (0, 0)),
                pl.BlockSpec((ff, cols), lambda d, s: (0, 2 * block(d, s) + s[0])),
                pl.BlockSpec((1, rows, cols), lambda d, s: (block(d, s), 0, 0)),
            ],
            out_specs=pl.BlockSpec((1, rows, cols), lambda d, s: (d, 0, 0)),
        ),
        out_shape=jax.ShapeDtypeStruct((groups, rows, cols), BF),
        compiler_params=params("arbitrary"),
        name="expert_down",
    )(idx, hidden, wd, received)


def combine_kernel(routes_ref, logits_ref, *refs, chunks, experts):
    returned, out_ref = refs[:-1], refs[-1]
    rows = routes_ref.shape[0]
    expert_iota = lax.broadcasted_iota(jnp.int32, (rows, experts), 1)
    e0 = routes_ref[:, 0:1]
    e1 = routes_ref[:, 1:2]
    oh0 = (expert_iota == e0).astype(F32)
    oh1 = (expert_iota == e1).astype(F32)
    earlier = (
        lax.broadcasted_iota(jnp.int32, (rows, rows), 1)
        < lax.broadcasted_iota(jnp.int32, (rows, rows), 0)
    ).astype(F32)
    before = dot(earlier.astype(BF), (oh0 + oh1).astype(BF))
    slot0 = jnp.sum(oh0 * before, axis=1, keepdims=True).astype(jnp.int32)
    slot1 = jnp.sum(oh1 * (before + oh0), axis=1, keepdims=True).astype(jnp.int32)
    logits = logits_ref[...]
    gap = logits[:, 0:1] - logits[:, 1:2]

    def picked(expert, slot):
        total = 0.0
        for ref, (first, count) in zip(returned, chunks):
            inside = (slot >= first) & (slot < first + count)
            place = jnp.where(inside, expert * count + slot - first, -1)
            lane_iota = lax.broadcasted_iota(jnp.int32, (rows, experts * count), 1)
            chosen = (lane_iota == place).astype(F32).astype(BF)
            total = total + dot(chosen, ref[...])
        return total

    out_ref[...] = (
        picked(e0, slot0) * jax.nn.sigmoid(gap) + picked(e1, slot1) * jax.nn.sigmoid(-gap)
    ).astype(BF)


def combine(routes, logits, returned, experts):
    rows = routes.shape[0]
    cols = returned[0].shape[1]
    return pl.pallas_call(
        functools.partial(combine_kernel, chunks=CHUNKS, experts=experts),
        out_shape=jax.ShapeDtypeStruct((rows, cols), BF),
        in_specs=[pl.BlockSpec(memory_space=pltpu.VMEM) for _ in range(2 + len(returned))],
        out_specs=pl.BlockSpec(memory_space=pltpu.VMEM),
        compiler_params=params(),
        name="combine",
    )(routes, logits, *returned)


def ring(count, shift):
    return [(i, (i + shift) % count) for i in range(count)]


def body(
    mix_tokens,
    mix_gain,
    w_query,
    w_forget_fwd,
    w_forget_bwd,
    w_value,
    decay_floor,
    decay_shift,
    head_gain,
    w_out,
    moe_tokens,
    moe_gain,
    routes,
    route_logits,
    w_expert_gate,
    w_expert_up,
    w_expert_down,
):
    experts = lax.axis_size(EP)
    groups = lax.axis_size("y")
    core, chip = lax.axis_index("c"), lax.axis_index("y")
    idx = jnp.stack([core, chip, lax.axis_index(EP)]).astype(jnp.int32)
    swap = [(0, 1), (1, 0)]
    wg, wu, wd = w_expert_gate[0], w_expert_up[0], w_expert_down[0]

    outgoing = dispatch(idx, moe_tokens, moe_gain[None], routes.T, experts)
    arrived = []
    for rows, (_, count) in zip(outgoing, CHUNKS):
        shaped = rows.reshape(experts, count, rows.shape[1])
        got = lax.all_to_all(shaped, EP, split_axis=0, concat_axis=0, tiled=True)
        arrived.append(got.reshape(rows.shape))

    o, qf, qb, message = local_sweeps(
        mix_tokens,
        mix_gain[None],
        w_query,
        w_forget_fwd,
        w_forget_bwd,
        w_value,
        decay_floor[None],
        decay_shift,
    )
    summaries = lax.all_to_all(message, EP, split_axis=0, concat_axis=0, tiled=True)
    incoming = scan_states(idx, summaries)
    incoming = lax.all_to_all(incoming, EP, split_axis=0, concat_axis=0, tiled=True)

    returned = []
    for own, (_, count) in zip(arrived, CHUNKS):
        other = lax.ppermute(own, "c", swap)
        block = own.shape[0] // max(1, own.shape[0] // 320)
        hidden, for_partner = expert_hidden(idx, own, other, wg, wu, wd, groups, block)
        received = lax.ppermute(for_partner, "c", swap)
        pair = expert_down(idx, hidden, wd, received, groups, block)
        parts = [pair[0]] + [lax.ppermute(pair[d], "y", ring(groups, d)) for d in range(1, groups)]
        summed = sum(part.astype(F32) for part in parts).astype(BF)
        shaped = summed.reshape(experts, count, summed.shape[1])
        back = lax.all_to_all(shaped, EP, split_axis=0, concat_axis=0, tiled=True)
        returned.append(back.reshape(summed.shape))

    readout = finish(o, qf, qb, incoming.reshape(-1, DK), head_gain[None])
    tp_size = lax.axis_size(TP)
    shaped = readout.reshape(tp_size, -1, readout.shape[1])
    regrouped = lax.all_to_all(shaped, TP, split_axis=0, concat_axis=0, tiled=True)
    mixed_out = project_out(regrouped, w_out)
    moe_out = combine(routes, route_logits, returned, experts)
    return (mixed_out, moe_out)


def solution(mesh):
    finer = Mesh(mesh.devices.reshape(4, 4, 4, 2), ALL)
    return jax.shard_map(
        body,
        mesh=finer,
        in_specs=(
            P(EP, None),
            P(),
            P(None, TP),
            P(None, TP),
            P(None, TP),
            P(None, TP),
            P(TP),
            P(EP, TP),
            P(),
            P(),
            P(EP, None),
            P(),
            P(EP, None),
            P(EP, None),
            P(EP, None, TP),
            P(EP, None, TP),
            P(EP, TP, None),
        ),
        out_specs=(P(ALL, None), P(EP, TP)),
        check_vma=False,
    )
```

time: 333 us -> 170 us (0.51)
  matrix products: 86.5 us -> 0 us
  other arithmetic: 70.3 us -> 3.03 us
  Pallas kernels: 0 us -> 58.4 us
  local copies, waits for them, and re-layouts: 41.6 us -> 7.9 us
  blocking collectives: 83.3 us -> 63.7 us
  between operations: 14.8 us -> 0.72 us
  waiting for transfers between devices: 15.4 us -> 21.8 us
  starting transfers between devices: 17.8 us -> 13.2 us
    dot_general x56 -> x0, matrix products: 86.5 us -> none  [the longest x16 29.3 us: advance(): jnp.einsum('hts,shv->thv', scores, block_v)]
    all_gather x8 -> x0, blocking collectives: 83.3 us -> none  [prefix_by_axis(): lax.all_gather(part.astype(kind), axis)]
    all_to_all x0 -> x3, blocking collectives: none -> 63.7 us  [the longest x1 39.2 us: body(): got = lax.all_to_all(shaped, EP, split_axis=0, concat_axis=0, tiled=True)]
    pallas_call x0 -> x8, Pallas kernels: none -> 58.4 us  [the longest x1 17.1 us: local_sweeps(): pl.pallas_call(functools.partial(local_kernel, steps=steps, rows=rows, he...]
    mul x17 -> x0, other arithmetic: 19 us -> none  [the longest x8 9.65 us: advance(): key_shrunk = block_k * jnp.exp(-running)]
    another operation x18 -> x1, other arithmetic: 18.7 us -> 0.67 us  [body(): idx = jnp.stack([core, chip, lax.axis_index(EP)]).astype(jnp.int32)]
    another operation x8 -> x0, local copies, waits for them, and re-layouts: 15 us -> none  [the longest x4 10.1 us: to_blocks(): return array.reshape(block_count, blk_rows, head_count, array.shape[2])]
    dynamic_update_slice x16 -> x0, other arithmetic: 11.4 us -> none  [sweep_forward(): lax.scan(advance, starting, blocks_in)]
  transfers between devices with their start and end apart: 5 -> 7, of which waited for: 2 -> 4; matrix products, arithmetic and copies ran while one was open for 45% -> 3% of each run, Pallas kernels for 0% -> 17%
where the time goes in v1:
time: 170 us; the launch traced here: 169 us
  blocking collectives  63.7 us (37%)
  Pallas kernels  58.4 us (34%)
  waiting for transfers between devices  21.8 us (13%)
  starting transfers between devices  13.2 us (8%)
  local copies, waits for them, and re-layouts  7.9 us (5%)
  other arithmetic  3.03 us (2%)
    all_to_all x1, blocking collectives, body(): got = lax.all_to_all(shaped, EP, split_axis=0, concat_axis=0, tiled=True)  39.2 us
    pallas_call x1, Pallas kernels, local_sweeps(): pl.pallas_call(functools.partial(local_kernel, steps=steps, rows=rows, he...  17.1 us
    pallas_call x1, Pallas kernels, expert_hidden(): pl.pallas_call(functools.partial(hidden_kernel, groups=groups), grid_spec...  15.2 us
    all_to_all x1, blocking collectives, body(): lax.all_to_all(message, EP, split_axis=0, concat_axis=0, tiled=True)  12.3 us
    all_to_all x1, blocking collectives, body(): lax.all_to_all(incoming, EP, split_axis=0, concat_axis=0, tiled=True)  12.2 us
    all_to_all x1, waiting for transfers between devices, body(): lax.all_to_all(shaped, TP, split_axis=0, concat_axis=0, tiled=True)  7.84 us
    pallas_call x1, Pallas kernels, expert_down(): pl.pallas_call(down_kernel, grid_spec=pltpu.PrefetchScalarGridSpec(num_sc...  6.58 us
    unnamed x19, local copies, waits for them, and re-layouts  6.35 us
  transfers between devices with their start and end apart: 7, of which 4 were waited for; matrix products, arithmetic and copies ran while one was open for 3% of the time, Pallas kernels for 17%

profile of v1, /device:TPU:0, one launch (start us, length us, event | category | flops | bytes accessed | tf_op | source)
XLA Modules:
  0.0 168.7 jit_solution(6268073029244274680)
XLA Ops:
  0.6 0.7 pad_add_fusion.idx_ref
  1.3 4.7 %dispatch.1 = bf16[1152,1024]{1,0:T(8,128)(2,1)} custom-call(s32[3]{0:T(128)} %pad_add_fusion.idx_ref, bf16[384,2048]{1,0:T(8,128)(2,1)} %tok_ref.1, f32[1,2048]{1,0:T(1,128)} %bitcast.39, s32[2,384]{1,0:T(2,128)} %bitcast.38), custom_call_target="tpu_custom_call" | custom-call | tf_op jit(solution)/shard_map/dispatch/pallas_call | solution.py:81
  6.0 39.2 %all_to_all.25 = bf16[16,72,1024]{2,1,0:T(8,128)(2,1)S(1)} all-to-all(bf16[16,72,1024]{2,1,0:T(8,128)(2,1)} %bitcast.30), channel_id=1, replica_groups=mesh['z'=4,'x'=4,'y'=4,'c'=2] {'z','x'}, dimensions={0} | all-to-all | bytes 4718592 | tf_op jit(solution)/shard_map/all_to_all | solution.py:518
  45.2 0.0 copy-start
  45.2 0.0 collective-permute-start
  45.2 4.5 %collective-permute-done.other_ref = bf16[1152,1024]{1,0:T(8,128)(2,1)S(1)} collective-permute-done((bf16[1152,1024]{1,0:T(8,128)(2,1)S(1)}, bf16[1152,1024]{1,0:T(8,128)(2,1)S(1)}, u32[]{:S(2)}, u32[]{:S(2)}) %collective-permute-start) | collective-permute-done | bytes 2359328 | tf_op jit(solution)/shard_map/ppermute | solution.py:537
  49.7 0.0 copy-start.2
  49.7 0.0 copy-done
  49.7 1.4 copy-done.2
  51.1 15.2 %expert_hidden.1 = (bf16[1152,640]{1,0:T(8,128)(2,1)}, bf16[4,1152,256]{2,1,0:T(8,128)(2,1)}) custom-call(s32[3]{0:T(128)} %pad_add_fusion.idx_ref, bf16[1152,1024]{1,0:T(8,128)(2,1)} %bitcast.32, bf16[1152,1024]{1,0:T(8,128)(2,1)} %copy-done.2, bf16[2048,640]{1,0:T(8,128)(2,1)} %bitcast.33, bf16[2048,640]{1,0:T(8,128)(2,1)} %bitcast.34, ...), custom_call_target="tpu_custom_call" | custom-call | tf_op jit(solution)/shard_map/expert_hidden/pallas_call | solution.py:385
  66.3 0.1 collective-permute-start.1
  66.4 4.6 %collective-permute-done.1.got_ref = bf16[4,1152,256]{2,1,0:T(8,128)(2,1)S(1)} collective-permute-done((bf16[4,1152,256]{2,1,0:T(8,128)(2,1)}, bf16[4,1152,256]{2,1,0:T(8,128)(2,1)S(1)}, u32[]{:S(2)}, u32[]{:S(2)}) %collective-permute-start.1) | collective-permute-done | bytes 2359328 | tf_op jit(solution)/shard_map/ppermute | solution.py:540
  71.0 0.0 copy-start.3
  71.0 1.4 copy-done.3
  72.4 6.6 %expert_down.1 = bf16[4,1152,256]{2,1,0:T(8,128)(2,1)} custom-call(s32[3]{0:T(128)} %pad_add_fusion.idx_ref, bf16[1152,640]{1,0:T(8,128)(2,1)} %get-tuple-element.12.h_ref, bf16[640,2048]{1,0:T(8,128)(2,1)} %bitcast.29, bf16[4,1152,256]{2,1,0:T(8,128)(2,1)} %copy-done.3), custom_call_target="tpu_custom_call" | custom-call | tf_op jit(solution)/shard_map/expert_down/pallas_call | solution.py:420
  79.0 0.0 copy-start.6
  79.0 1.5 slice_bitcast_fusion.2
  80.6 1.6 collective-permute-start.2
  82.2 2.9 %collective-permute-start.3 = (bf16[1152,256]{1,0:T(8,128)(2,1)S(1)}, bf16[1152,256]{1,0:T(8,128)(2,1)S(1)}, u32[]{:S(2)}, u32[]{:S(2)}) collective-permute-start(bf16[1152,256]{1,0:T(8,128)(2,1)S(1)} %get-tuple-element.16), channel_id=1, source_target_pairs={{0,4},{2,6},{4,0},{6,2},{1,5},{3,7},{5,1},{7,3},{8,12},{10,14},{12... | collective-permute-start | bytes 1769480 | tf_op jit(solution)/shard_map/ppermute | solution.py:542
  85.1 1.3 collective-permute-start.4
  86.5 0.0 copy-done.6
  86.5 1.0 copy.19.shift_ref
  87.5 17.1 %local_sweeps.1 = (f32[1024,256]{1,0:T(8,128)}, bf16[1024,256]{1,0:T(8,128)(2,1)}, bf16[1024,256]{1,0:T(8,128)(2,1)}, bf16[16,40,128]{2,1,0:T(8,128)(2,1)}) custom-call(bf16[1024,2048]{1,0:T(8,128)(2,1)} %x_ref.1, f32[1,2048]{1,0:T(1,128)} %bitcast.40, bf16[2048,256]{1,0:T(8,128)(2,1)} %wq_ref.1, bf16[2048,256]{1,0:T(8,128)(2,1)} %wf_ref.1, ...), custom_call_target="tpu_custom_call" | custom-call | tf_op jit(solution)/shard_map/local_sweeps/pallas_call | solution.py:240
  104.6 12.3 %all_to_all.26.msg_ref = bf16[16,40,128]{2,1,0:T(8,128)(2,1)} all-to-all(bf16[16,40,128]{2,1,0:T(8,128)(2,1)} %get-tuple-element.11), channel_id=1, replica_groups=mesh['z'=4,'x'=4,'y'=4,'c'=2] {'z','x'}, dimensions={0} | all-to-all | bytes 327680 | tf_op jit(solution)/shard_map/all_to_all | solution.py:531
  117.0 1.6 scan_states.1
  118.6 12.2 %all_to_all.27 = bf16[16,32,128]{2,1,0:T(8,128)(2,1)} all-to-all(bf16[16,32,128]{2,1,0:T(8,128)(2,1)} %scan_states.1), channel_id=1, replica_groups=mesh['z'=4,'x'=4,'y'=4,'c'=2] {'z','x'}, dimensions={0} | all-to-all | bytes 262144 | tf_op jit(solution)/shard_map/all_to_all | solution.py:533
  130.7 4.2 %finish.1 = bf16[1024,256]{1,0:T(8,128)(2,1)} custom-call(f32[1024,256]{1,0:T(8,128)} %get-tuple-element.8.o_ref, bf16[1024,256]{1,0:T(8,128)(2,1)} %get-tuple-element.9.qf_ref, bf16[1024,256]{1,0:T(8,128)(2,1)} %get-tuple-element.10.qb_ref, bf16[512,128]{1,0:T(8,128)(2,1)} %bitcast.37, f32[1,128]{1,0:T(1,128)} %bitcast.42), custom_call_target="tpu_custom_call" | custom-call | tf_op jit(solution)/shard_map/finish/pallas_call | solution.py:321
  135.0 0.0 copy-start.5
  135.0 3.6 %all-to-all-start.2 = ((bf16[8,128,256]{2,1,0:T(8,128)(2,1)}), bf16[8,128,256]{2,1,0:T(8,128)(2,1)S(1)}, u32[]{:S(2)}, u32[]{:S(2)}) async-start(bf16[8,128,256]{2,1,0:T(8,128)(2,1)} %bitcast.36), calls=%async_computation.2 | async-start | bytes 1048576 | tf_op jit(solution)/shard_map/all_to_all | solution.py:551
  138.6 0.0 copy-start.7
  138.6 0.0 collective-permute-done.2
  138.6 0.0 collective-permute-done.3
  138.6 0.0 collective-permute-done.4
  138.7 2.4 %fusion.2 = bf16[1152,256]{1,0:T(8,128)(2,1)} fusion(bf16[1152,256]{1,0:T(8,128)(2,1)} %collective-permute-done.4, bf16[1152,256]{1,0:T(8,128)(2,1)S(1)} %collective-permute-done.3, bf16[1152,256]{1,0:T(8,128)(2,1)S(1)} %collective-permute-done.2, bf16[4,1152,256]{2,1,0:T(8,128)(2,1)} %expert_down.1), kind=kLoop, calls=%fused_computation.3 | loop fusion | flops 2359296 | bytes 2949120 | tf_op jit(solution)/shard_map/convert_element_type | solution.py:543
  141.0 7.8 %all-to-all-done.2.r_ref = bf16[8,128,256]{2,1,0:T(8,128)(2,1)S(1)} async-done(((bf16[8,128,256]{2,1,0:T(8,128)(2,1)}), bf16[8,128,256]{2,1,0:T(8,128)(2,1)S(1)}, u32[]{:S(2)}, u32[]{:S(2)}) %all-to-all-start.2) | async-done | bytes 524320 | tf_op jit(solution)/shard_map/all_to_all | solution.py:551
  148.8 0.0 copy-start.4
  148.8 3.6 %all-to-all-start.4 = ((bf16[16,72,256]{2,1,0:T(8,128)(2,1)}), bf16[16,72,256]{2,1,0:T(8,128)(2,1)S(1)}, u32[]{:S(2)}, u32[]{:S(2)}) async-start(bf16[16,72,256]{2,1,0:T(8,128)(2,1)} %bitcast.19), calls=%async_computation.4 | async-start | bytes 1179648 | tf_op jit(solution)/shard_map/all_to_all | solution.py:545
  152.4 0.0 copy-done.5
  152.4 0.8 copy.20.routes_ref
  153.3 0.0 copy-done.7
  153.3 0.8 copy.21.logits_ref
  154.1 0.0 copy-done.4
  154.1 5.7 %project_out.1 = bf16[128,2048]{1,0:T(8,128)(2,1)} custom-call(bf16[8,128,256]{2,1,0:T(8,128)(2,1)} %copy-done.4, bf16[2048,2048]{1,0:T(8,128)(2,1)} %w_ref.1), custom_call_target="tpu_custom_call" | custom-call | tf_op jit(solution)/shard_map/project_out/pallas_call | solution.py:348
  159.8 4.8 %all-to-all-done.4 = bf16[16,72,256]{2,1,0:T(8,128)(2,1)S(1)} async-done(((bf16[16,72,256]{2,1,0:T(8,128)(2,1)}), bf16[16,72,256]{2,1,0:T(8,128)(2,1)S(1)}, u32[]{:S(2)}, u32[]{:S(2)}) %all-to-all-start.4) | async-done | bytes 589856 | tf_op jit(solution)/shard_map/all_to_all | solution.py:545
  164.6 0.0 copy-start.1
  164.6 0.8 copy-done.1
  165.5 3.2 %combine.1 = bf16[384,256]{1,0:T(8,128)(2,1)} custom-call(s32[384,2]{1,0:T(8,128)} %copy.20.routes_ref, f32[384,2]{1,0:T(8,128)} %copy.21.logits_ref, bf16[1152,256]{1,0:T(8,128)(2,1)} %bitcast.35), custom_call_target="tpu_custom_call" | custom-call | tf_op jit(solution)/shard_map/combine/pallas_call | solution.py:474
Async XLA Ops:
  45.2 4.5 %copy-start = (bf16[16,72,1024]{2,1,0:T(8,128)(2,1)}, bf16[16,72,1024]{2,1,0:T(8,128)(2,1)S(1)}, u32[]{:S(2)}) copy-start(bf16[16,72,1024]{2,1,0:T(8,128)(2,1)S(1)} %all_to_all.25) | copy-start | bytes 7077892
  45.2 4.5 %collective-permute-start = (bf16[1152,1024]{1,0:T(8,128)(2,1)S(1)}, bf16[1152,1024]{1,0:T(8,128)(2,1)S(1)}, u32[]{:S(2)}, u32[]{:S(2)}) collective-permute-start(bf16[1152,1024]{1,0:T(8,128)(2,1)S(1)} %bitcast.31), channel_id=1, source_target_pairs={{0,1},{1,0},{2,3},{3,2},{4,5},{5,4},{6,7},{7,6},{8,9},{9,8},{10,11... | collective-permute-start | bytes 7077896 | tf_op jit(solution)/shard_map/ppermute | solution.py:537
  49.7 1.4 copy-start.2
  66.3 4.7 %collective-permute-start.1 = (bf16[4,1152,256]{2,1,0:T(8,128)(2,1)}, bf16[4,1152,256]{2,1,0:T(8,128)(2,1)S(1)}, u32[]{:S(2)}, u32[]{:S(2)}) collective-permute-start(bf16[4,1152,256]{2,1,0:T(8,128)(2,1)} %get-tuple-element.13), channel_id=1, source_target_pairs={{0,1},{1,0},{2,3},{3,2},{4,5},{5,4},{6,7},{7,6},{8,9},{9,8},{10,11... | collective-permute-start | bytes 7077896 | tf_op jit(solution)/shard_map/ppermute | solution.py:540
  71.0 1.4 copy-start.3
  79.0 7.5 %copy-start.6 = (f32[1024,2]{0,1:T(2,128)S(1)}, f32[1024,2]{0,1:T(2,128)}, u32[]{:S(2)}) copy-start(f32[1024,2]{0,1:T(2,128)} %param.24) | copy-start | bytes 24580
  80.6 58.0 %collective-permute-start.2 = (bf16[1152,256]{1,0:T(8,128)(2,1)S(1)}, bf16[1152,256]{1,0:T(8,128)(2,1)S(1)}, u32[]{:S(2)}, u32[]{:S(2)}) collective-permute-start(bf16[1152,256]{1,0:T(8,128)(2,1)S(1)} %get-tuple-element.14), channel_id=1, source_target_pairs={{0,2},{2,4},{4,6},{6,0},{1,3},{3,5},{5,7},{7,1},{8,10},{10,12},{12... | collective-permute-start | bytes 1769480 | tf_op jit(solution)/shard_map/ppermute | solution.py:542
  82.2 56.4 %collective-permute-start.3 = (bf16[1152,256]{1,0:T(8,128)(2,1)S(1)}, bf16[1152,256]{1,0:T(8,128)(2,1)S(1)}, u32[]{:S(2)}, u32[]{:S(2)}) collective-permute-start(bf16[1152,256]{1,0:T(8,128)(2,1)S(1)} %get-tuple-element.16), channel_id=1, source_target_pairs={{0,4},{2,6},{4,0},{6,2},{1,5},{3,7},{5,1},{7,3},{8,12},{10,14},{12... | collective-permute-start | bytes 1769480 | tf_op jit(solution)/shard_map/ppermute | solution.py:542
  85.1 53.5 %collective-permute-start.4 = (bf16[1152,256]{1,0:T(8,128)(2,1)S(1)}, bf16[1152,256]{1,0:T(8,128)(2,1)}, u32[]{:S(2)}, u32[]{:S(2)}) collective-permute-start(bf16[1152,256]{1,0:T(8,128)(2,1)S(1)} %get-tuple-element.15), channel_id=1, source_target_pairs={{0,6},{2,0},{4,2},{6,4},{1,7},{3,1},{5,3},{7,5},{8,14},{10,8},{12,... | collective-permute-start | bytes 1769480 | tf_op jit(solution)/shard_map/ppermute | solution.py:542
  135.0 17.5 %copy-start.5 = (s32[384,2]{0,1:T(2,128)S(1)}, s32[384,2]{0,1:T(2,128)}, u32[]{:S(2)}) copy-start(s32[384,2]{0,1:T(2,128)} %param.29) | copy-start | bytes 9220
  135.0 13.9 %all-to-all-start.2 = ((bf16[8,128,256]{2,1,0:T(8,128)(2,1)}), bf16[8,128,256]{2,1,0:T(8,128)(2,1)S(1)}, u32[]{:S(2)}, u32[]{:S(2)}) async-start(bf16[8,128,256]{2,1,0:T(8,128)(2,1)} %bitcast.36), calls=%async_computation.2 | async-start | bytes 1048576 | tf_op jit(solution)/shard_map/all_to_all | solution.py:551
  138.6 14.7 %copy-start.7 = (f32[384,2]{0,1:T(2,128)S(1)}, f32[384,2]{0,1:T(2,128)}, u32[]{:S(2)}) copy-start(f32[384,2]{0,1:T(2,128)} %param.30) | copy-start | bytes 9220
  148.8 5.3 %copy-start.4 = (bf16[8,128,256]{2,1,0:T(8,128)(2,1)}, bf16[8,128,256]{2,1,0:T(8,128)(2,1)S(1)}, u32[]{:S(2)}) copy-start(bf16[8,128,256]{2,1,0:T(8,128)(2,1)S(1)} %all-to-all-done.2.r_ref) | copy-start | bytes 1572868
  148.8 15.8 %all-to-all-start.4 = ((bf16[16,72,256]{2,1,0:T(8,128)(2,1)}), bf16[16,72,256]{2,1,0:T(8,128)(2,1)S(1)}, u32[]{:S(2)}, u32[]{:S(2)}) async-start(bf16[16,72,256]{2,1,0:T(8,128)(2,1)} %bitcast.19), calls=%async_computation.4 | async-start | bytes 1179648 | tf_op jit(solution)/shard_map/all_to_all | solution.py:545
  164.6 0.8 copy-start.1

commit v2 on v1

v2 whole, which is shorter than its diff:
```python
import functools

import jax
import jax.numpy as jnp
from jax import lax
from jax.experimental import pallas as pl
from jax.experimental.pallas import tpu as pltpu
from jax.sharding import Mesh
from jax.sharding import PartitionSpec as P

DK = 128
DV = 128
BLK = 128
EP = ("z", "x")
TP = ("y", "c")
ALL = ("z", "x", "y", "c")
EPSILON = 1e-06
BF = jnp.bfloat16
F32 = jnp.float32
CHUNKS = ((0, 72),)
COST_UNIT = 250e6


def params(mib, *semantics):
    return pltpu.CompilerParams(
        dimension_semantics=semantics if semantics else None, vmem_limit_bytes=mib * 1024 * 1024
    )


def cost(micros):
    return pl.CostEstimate(flops=int(micros * COST_UNIT), transcendentals=0, bytes_accessed=0)


def after(kernel, at, deps):
    def run(*refs):
        kernel(*refs[:at], *refs[at + len(deps) :])

    return run


def any_specs(deps):
    return [pl.BlockSpec(memory_space=pl.ANY) for _ in deps]


def dot(a, b):
    return jnp.dot(a, b, preferred_element_type=F32)


def dot_nt(a, b):
    return lax.dot_general(a, b, (((1,), (1,)), ((), ())), preferred_element_type=F32)


def dot_tn(a, b):
    return lax.dot_general(a, b, (((0,), (0,)), ((), ())), preferred_element_type=F32)


def rms_scale(floats):
    return lax.rsqrt(jnp.mean(floats * floats, axis=-1, keepdims=True) + EPSILON)


def dispatch_kernel(idx_ref, tok_ref, gain_ref, routes_ref, *outs, chunks, experts):
    half = tok_ref.shape[1] // 2
    rows = tok_ref.shape[0]
    scale = rms_scale(tok_ref[...].astype(F32))
    start = pl.multiple_of(idx_ref[0] * half, half)
    own = tok_ref[:, pl.ds(start, half)].astype(F32)
    normed = (own * scale * gain_ref[:, pl.ds(start, half)]).astype(BF)
    e0 = routes_ref[0:1, :]
    e1 = routes_ref[1:2, :]
    expert_iota = lax.broadcasted_iota(jnp.int32, (experts, rows), 0)
    oh0 = (expert_iota == e0).astype(F32)
    oh1 = (expert_iota == e1).astype(F32)
    earlier = (
        lax.broadcasted_iota(jnp.int32, (rows, rows), 0)
        < lax.broadcasted_iota(jnp.int32, (rows, rows), 1)
    ).astype(F32)
    before = dot((oh0 + oh1).astype(BF), earlier.astype(BF))
    slot0 = jnp.sum(oh0 * before, axis=0, keepdims=True).astype(jnp.int32)
    slot1 = jnp.sum(oh1 * (before + oh0), axis=0, keepdims=True).astype(jnp.int32)
    for out, (first, count) in zip(outs, chunks):
        total = experts * count

        def place(expert, slot):
            inside = (slot >= first) & (slot < first + count)
            return jnp.where(inside, expert * count + slot - first, -1)

        p0 = place(e0, slot0)
        p1 = place(e1, slot1)
        row_iota = lax.broadcasted_iota(jnp.int32, (total, rows), 0)
        chosen = ((row_iota == p0) | (row_iota == p1)).astype(F32).astype(BF)
        out[...] = dot(chosen, normed).astype(BF)


def dispatch(idx, tokens, gain, routes_t, experts):
    half = tokens.shape[1] // 2
    return pl.pallas_call(
        functools.partial(dispatch_kernel, chunks=CHUNKS, experts=experts),
        out_shape=tuple(jax.ShapeDtypeStruct((experts * n, half), BF) for _, n in CHUNKS),
        in_specs=[
            pl.BlockSpec(memory_space=pltpu.SMEM),
            pl.BlockSpec(memory_space=pltpu.VMEM),
            pl.BlockSpec(memory_space=pltpu.VMEM),
            pl.BlockSpec(memory_space=pltpu.VMEM),
        ],
        out_specs=tuple(pl.BlockSpec(memory_space=pltpu.VMEM) for _ in CHUNKS),
        compiler_params=params(16),
        cost_estimate=cost(5),
        name="dispatch",
    )(idx, tokens, gain, routes_t)


def tri_sum(tri, g):
    high = g.astype(BF)
    low = (g - high.astype(F32)).astype(BF)
    return dot(tri, high) + dot(tri, low)


def local_kernel(
    idx_ref,
    x_ref,
    gain_ref,
    wq_ref,
    wf_ref,
    wb_ref,
    wv_ref,
    floor_ref,
    shift_ref,
    o_ref,
    qf_ref,
    qb_ref,
    msg_ref,
    q_s,
    v_s,
    kb_s,
    gb_s,
    st_s,
    off_s,
    kept_s,
    *,
    steps,
    rows,
    heads,
):
    step = pl.program_id(0)
    width = heads * DK

    @pl.when(step == 0)
    def _():
        st_s[...] = jnp.zeros_like(st_s)
        off_s[...] = jnp.zeros_like(off_s)
        kept_s[...] = jnp.zeros_like(kept_s)

    x = x_ref[...].astype(F32)
    normed = (x * rms_scale(x) * gain_ref[...]).astype(BF)

    def project(w_ref):
        return dot(normed, w_ref[...]).astype(BF)

    q_pre = project(wq_ref).astype(F32)
    queries = q_pre * jax.nn.sigmoid(q_pre)
    values = project(wv_ref)
    shift = shift_ref[...]
    shift_wide = jnp.concatenate(
        [jnp.broadcast_to(shift[:, h : h + 1], (rows, DK)) for h in range(heads)], axis=1
    )
    room = 1.0 - floor_ref[...]

    def decay(w_ref):
        keys = room * (1.0 - jax.nn.sigmoid(project(w_ref).astype(F32)))
        return keys, jnp.log1p(-keys) + shift_wide

    keys_f, logs_f = decay(wf_ref)
    keys_b, logs_b = decay(wb_ref)
    base = pl.multiple_of(step * rows, rows)
    q_s[pl.ds(base, rows), :] = queries
    v_s[pl.ds(base, rows), :] = values
    kb_s[pl.ds(base, rows), :] = keys_b
    gb_s[pl.ds(base, rows), :] = logs_b

    row_iota = lax.broadcasted_iota(jnp.int32, (BLK, BLK), 0)
    col_iota = lax.broadcasted_iota(jnp.int32, (BLK, BLK), 1)
    lower = row_iota >= col_iota
    upper = row_iota <= col_iota
    lower_one = lower.astype(F32).astype(BF)
    upper_one = upper.astype(F32).astype(BF)

    def block(q, k, v, g, tri_one, mask, end_row, states, offset):
        run = tri_sum(tri_one, g)
        end = run[end_row : end_row + 1, :]
        grown = q * jnp.exp(run)
        grown_b = grown.astype(BF)
        shrunk = (k * jnp.exp(-run)).astype(BF)
        closing = (k * jnp.exp(end - run)).astype(BF)
        kept = jnp.exp(end)
        result = []
        new_states = []
        for h in range(heads):
            lanes = slice(h * DK, (h + 1) * DK)
            scores = jnp.where(mask, dot_nt(grown_b[:, lanes], shrunk[:, lanes]), 0.0).astype(BF)
            st = states[h]
            result.append(
                dot(scores, v[:, lanes]) + dot_nt(grown_b[:, lanes], st.astype(BF))
            )
            new_states.append(st * kept[:, lanes] + dot_tn(v[:, lanes], closing[:, lanes]))
        carried = (grown * jnp.exp(offset)).astype(BF)
        return jnp.concatenate(result, axis=1), new_states, carried, offset + end

    def write_message(way, states, total):
        kept = jnp.exp(total)
        high = kept.astype(BF).astype(F32)
        for h in range(heads):
            lanes = slice(h * DK, (h + 1) * DK)
            kept_s[h : h + 1, :] = high[:, lanes]
            kept_s[heads + h : heads + h + 1, :] = (kept - high)[:, lanes]
        whole = jnp.concatenate(list(states) + [kept_s[...]], axis=0).astype(BF)

        def write(target, _):
            msg_ref[target] = whole
            return 0

        here = idx_ref[2]
        if way == 0:
            lax.fori_loop(here, msg_ref.shape[0], write, 0)
        else:
            lax.fori_loop(0, here, write, 0)

    states = [st_s[h] for h in range(heads)]
    offset = off_s[...]
    for b in range(rows // BLK):
        rs = slice(b * BLK, (b + 1) * BLK)
        result, states, carried, offset = block(
            queries[rs], keys_f[rs], values[rs], logs_f[rs], lower_one, lower, BLK - 1, states, offset
        )
        at = pl.multiple_of(base + b * BLK, BLK)
        o_ref[pl.ds(at, BLK), :] = result
        qf_ref[pl.ds(at, BLK), :] = carried
    for h in range(heads):
        st_s[h] = states[h]
    off_s[...] = offset

    @pl.when(step == steps - 1)
    def _():
        write_message(0, states, offset)
        back = [jnp.zeros((DV, DK), F32) for _ in range(heads)]
        total = jnp.zeros((1, width), F32)
        for b in reversed(range(steps * rows // BLK)):
            rs = slice(b * BLK, (b + 1) * BLK)
            result, back, carried, total = block(
                q_s[rs, :], kb_s[rs, :], v_s[rs, :], gb_s[rs, :], upper_one, upper, 0, back, total
            )
            o_ref[rs, :] = o_ref[rs, :] + result
            qb_ref[rs, :] = carried
        write_message(1, back, total)


def local_sweeps(idx, tokens, gain, wq, wf, wb, wv, floor, shift, segments, deps=()):
    seg, model = tokens.shape
    width = wq.shape[1]
    heads = width // DK
    rows = 256
    steps = seg // rows
    whole = lambda shape: pl.BlockSpec(shape, lambda i: tuple(0 for _ in shape))
    return pl.pallas_call(
        after(functools.partial(local_kernel, steps=steps, rows=rows, heads=heads), 9, deps),
        grid=(steps,),
        out_shape=(
            jax.ShapeDtypeStruct((seg, width), F32),
            jax.ShapeDtypeStruct((seg, width), BF),
            jax.ShapeDtypeStruct((seg, width), BF),
            jax.ShapeDtypeStruct((segments, heads * DV + 8, DK), BF),
        ),
        in_specs=[
            pl.BlockSpec(memory_space=pltpu.SMEM),
            pl.BlockSpec((rows, model), lambda i: (i, 0)),
            whole((1, model)),
            whole((model, width)),
            whole((model, width)),
            whole((model, width)),
            whole((model, width)),
            whole((1, width)),
            pl.BlockSpec((rows, heads), lambda i: (i, 0)),
            *any_specs(deps),
        ],
        out_specs=(
            whole((seg, width)),
            whole((seg, width)),
            whole((seg, width)),
            whole((segments, heads * DV + 8, DK)),
        ),
        scratch_shapes=[
            pltpu.VMEM((seg, width), F32),
            pltpu.VMEM((seg, width), BF),
            pltpu.VMEM((seg, width), F32),
            pltpu.VMEM((seg, width), F32),
            pltpu.VMEM((heads, DV, DK), F32),
            pltpu.VMEM((1, width), F32),
            pltpu.VMEM((8, DK), F32),
        ],
        compiler_params=params(28, "arbitrary"),
        cost_estimate=cost(17),
        name="local_sweeps",
    )(idx, tokens, gain, wq, wf, wb, wv, floor, shift, *deps)


def finish_kernel(idx_ref, *refs, heads):
    line_ref, gain_ref, *outs, states_ref = refs[6:]
    here = idx_ref[2]
    count = line_ref.shape[0]

    @pl.when(pl.program_id(0) == 0)
    def _():
        zeros = tuple(jnp.zeros((DV, DK), F32) for _ in range(heads))

        def join(source, states):
            new = []
            for h, state in enumerate(states):
                tail = line_ref[source, heads * DV :, :].astype(F32)
                kept = tail[h : h + 1, :] + tail[heads + h : heads + h + 1, :]
                new.append(
                    state * kept + line_ref[source, h * DV : (h + 1) * DV, :].astype(F32)
                )
            return tuple(new)

        ahead = lax.fori_loop(0, here, join, zeros)
        behind = lax.fori_loop(0, count - 1 - here, lambda i, st: join(count - 1 - i, st), zeros)
        for p, state in enumerate(ahead + behind):
            states_ref[p * DV : (p + 1) * DV, :] = state.astype(BF)

    for (o_ref, qf_ref, qb_ref), out_ref in zip((refs[0:3], refs[3:6]), outs):
        for h in range(heads):
            lanes = slice(h * DK, (h + 1) * DK)
            ahead = states_ref[h * DV : (h + 1) * DV, :]
            behind = states_ref[(heads + h) * DV : (heads + h + 1) * DV, :]
            o = (
                o_ref[:, lanes]
                + dot_nt(qf_ref[:, lanes], ahead)
                + dot_nt(qb_ref[:, lanes], behind)
            )
            out_ref[0, :, lanes] = (o * rms_scale(o) * gain_ref[...]).astype(BF)


def finish(idx, o, qf, qb, line, gain, groups, deps=()):
    seg, width = o.shape
    rows = seg // (2 * groups)

    def tile(other):
        return pl.BlockSpec(
            (rows, width), lambda d, s: (2 * ((s[1] + d) % groups) + jnp.bitwise_xor(s[0], other), 0)
        )

    out = pl.BlockSpec((1, rows, width), lambda d, s: (d, 0, 0))
    shape = jax.ShapeDtypeStruct((groups, rows, width), BF)
    return pl.pallas_call(
        after(functools.partial(finish_kernel, heads=width // DK), 9, deps),
        grid_spec=pltpu.PrefetchScalarGridSpec(
            num_scalar_prefetch=1,
            grid=(groups,),
            in_specs=[
                *(tile(other) for other in (0, 0, 0, 1, 1, 1)),
                pl.BlockSpec(line.shape, lambda d, s: (0, 0, 0)),
                pl.BlockSpec(gain.shape, lambda d, s: (0, 0)),
                *any_specs(deps),
            ],
            out_specs=(out, out),
            scratch_shapes=[pltpu.VMEM((2 * width, DK), BF)],
        ),
        out_shape=(shape, shape),
        compiler_params=params(12, "arbitrary"),
        cost_estimate=cost(4),
        name="finish",
    )(idx, o, qf, qb, o, qf, qb, line, gain, *deps)


def combine_kernel(routes_ref, logits_ref, *refs, chunks, experts):
    returned, out_ref = refs[:-1], refs[-1]
    rows = routes_ref.shape[0]
    expert_iota = lax.broadcasted_iota(jnp.int32, (rows, experts), 1)
    e0 = routes_ref[:, 0:1]
    e1 = routes_ref[:, 1:2]
    oh0 = (expert_iota == e0).astype(F32)
    oh1 = (expert_iota == e1).astype(F32)
    earlier = (
        lax.broadcasted_iota(jnp.int32, (rows, rows), 1)
        < lax.broadcasted_iota(jnp.int32, (rows, rows), 0)
    ).astype(F32)
    before = dot(earlier.astype(BF), (oh0 + oh1).astype(BF))
    slot0 = jnp.sum(oh0 * before, axis=1, keepdims=True).astype(jnp.int32)
    slot1 = jnp.sum(oh1 * (before + oh0), axis=1, keepdims=True).astype(jnp.int32)
    logits = logits_ref[...]
    gap = logits[:, 0:1] - logits[:, 1:2]

    def picked(expert, slot):
        total = 0.0
        for result, (first, count) in zip(returned, chunks):
            inside = (slot >= first) & (slot < first + count)
            place = jnp.where(inside, expert * count + slot - first, -1)
            lane_iota = lax.broadcasted_iota(jnp.int32, (rows, experts * count), 1)
            chosen = (lane_iota == place).astype(F32).astype(BF)
            total = total + dot(chosen, result[...])
        return total

    out_ref[...] = (
        picked(e0, slot0) * jax.nn.sigmoid(gap) + picked(e1, slot1) * jax.nn.sigmoid(-gap)
    ).astype(BF)


def combine(routes, logits, returned, experts):
    rows = routes.shape[0]
    cols = returned[0].shape[1]
    return pl.pallas_call(
        functools.partial(combine_kernel, chunks=CHUNKS, experts=experts),
        out_shape=jax.ShapeDtypeStruct((rows, cols), BF),
        in_specs=[pl.BlockSpec(memory_space=pltpu.VMEM) for _ in range(2 + len(returned))],
        out_specs=pl.BlockSpec(memory_space=pltpu.VMEM),
        compiler_params=params(12),
        cost_estimate=cost(4),
        name="combine",
    )(routes, logits, *returned)


def ring(count, shift):
    return [(i, (i + shift) % count) for i in range(count)]


def body(
    mix_tokens,
    mix_gain,
    w_query,
    w_forget_fwd,
    w_forget_bwd,
    w_value,
    decay_floor,
    decay_shift,
    head_gain,
    w_out,
    moe_tokens,
    moe_gain,
    routes,
    route_logits,
    w_expert_gate,
    w_expert_up,
    w_expert_down,
):
    experts = lax.axis_size(EP)
    groups = lax.axis_size("y")
    core, chip = lax.axis_index("c"), lax.axis_index("y")
    idx = jnp.stack([core, chip, lax.axis_index(EP)]).astype(jnp.int32)
    swap = [(0, 1), (1, 0)]
    wg, wu, wd = w_expert_gate[0], w_expert_up[0], w_expert_down[0]

    outgoing = dispatch(idx, moe_tokens, moe_gain[None], routes.T, experts)
    o, qf, qb, message = local_sweeps(
        idx,
        mix_tokens,
        mix_gain[None],
        w_query,
        w_forget_fwd,
        w_forget_bwd,
        w_value,
        decay_floor[None],
        decay_shift,
        experts,
        deps=outgoing,
    )
    part = wd.shape[1] // (2 * groups)

    def by_core(which):
        return jnp.concatenate(
            [
                lax.dynamic_slice_in_dim(wd, (2 * g + which) * part, part, axis=1)
                for g in range(groups)
            ],
            axis=1,
        )

    def rolled(weight, shares, order):
        rows = weight.shape[0] // shares
        return jnp.concatenate(
            [lax.dynamic_slice_in_dim(weight, at * rows, rows) for at in order], axis=0
        )

    wg, wu = (rolled(w, 2, (core, 1 - core)) for w in (wg, wu))
    w_out_rolled = rolled(w_out, groups, [(chip + groups - d) % groups for d in range(groups)])
    wd_theirs, wd_mine, wg, wu, w_out_rolled = lax.optimization_barrier(
        (by_core(1 - core), by_core(core), wg, wu, w_out_rolled)
    )
    (rows,), ((_, count),) = outgoing, CHUNKS
    shaped = rows.reshape(experts, count, rows.shape[1])
    got = lax.all_to_all(shaped, EP, split_axis=0, concat_axis=0, tiled=True)
    own = got.reshape(rows.shape)
    other = lax.ppermute(own, "c", swap)
    line = lax.all_to_all(message, EP, split_axis=0, concat_axis=0, tiled=True)
    x = lax.optimization_barrier(jnp.concatenate([own, other], axis=1))
    hidden = (jax.nn.silu(dot(x, wg)) * dot(x, wu)).astype(BF)
    for_partner = dot(hidden, wd_theirs).astype(BF)
    received = lax.ppermute(for_partner, "c", swap)
    mine = lax.optimization_barrier(dot(hidden, wd_mine).astype(BF))
    received, _ = lax.optimization_barrier((received, line))
    cols = received.shape[1] // groups
    pair = jnp.stack(
        [
            (mine[:, at : at + cols].astype(F32) + received[:, at : at + cols].astype(F32)).astype(BF)
            for at in range(0, received.shape[1], cols)
        ]
    )
    shaped = pair.reshape((groups * experts, count, cols))
    back = lax.all_to_all(shaped, ("y", "z", "x"), split_axis=0, concat_axis=0, tiled=True)
    back = back.reshape(pair.shape)
    summed = sum(back[g].astype(F32) for g in range(groups)).astype(BF)
    returned = [summed]
    keep, give = finish(idx, o, qf, qb, line, head_gain[None], groups, deps=(shaped,))
    given = lax.ppermute(give, "c", swap)
    lower = jnp.where(core == 0, keep, given)
    upper = jnp.where(core == 0, given, keep)
    parts = [jnp.stack([lower[d], upper[d]]) for d in range(groups)]
    moved = [parts[0]] + [lax.ppermute(parts[d], "y", ring(groups, d)) for d in range(1, groups)]
    moe_out = combine(routes, route_logits, returned, experts)
    features = jnp.concatenate([part[i] for part in moved for i in range(2)], axis=1)
    mixed_out = dot(features, w_out_rolled).astype(BF)
    return (mixed_out, moe_out)


def solution(mesh):
    finer = Mesh(mesh.devices.reshape(4, 4, 4, 2), ALL)

    return jax.shard_map(
        body,
        mesh=finer,
        in_specs=(
            P(EP, None),
            P(),
            P(None, TP),
            P(None, TP),
            P(None, TP),
            P(None, TP),
            P(TP),
            P(EP, TP),
            P(),
            P(),
            P(EP, None),
            P(),
            P(EP, None),
            P(EP, None),
            P(EP, None, TP),
            P(EP, None, TP),
            P(EP, TP, None),
        ),
        out_specs=(P(ALL, None), P(EP, TP)),
        check_vma=False,
    )
```

time: 170 us -> 200 us (1.18)
  blocking collectives: 63.7 us -> 0 us
  waiting for transfers between devices: 21.8 us -> 76.9 us
  Pallas kernels: 58.4 us -> 23.2 us
  other arithmetic: 3.03 us -> 30.9 us
  matrix products: 0 us -> 22.1 us
  local copies, waits for them, and re-layouts: 7.9 us -> 20.6 us
  starting transfers between devices: 13.2 us -> 23.9 us
    all_to_all x3 -> x0, blocking collectives: 63.7 us -> none  [the longest x1 39.2 us: body(): got = lax.all_to_all(shaped, EP, split_axis=0, concat_axis=0, tiled=True)]
    all_to_all x2 -> x3, waiting for transfers between devices: 12.6 us -> 49.1 us  [the longest x1 35.7 us: body(): got = lax.all_to_all(shaped, EP, split_axis=0, concat_axis=0, tiled=True)]
    pallas_call x6 -> x2, Pallas kernels: 50.5 us -> 17.5 us  [the longest x1 13.9 us: local_sweeps(): pl.pallas_call(after(functools.partial(local_kernel, steps=steps, rows=ro...]
    ppermute x3 -> x4, waiting for transfers between devices: 0.01 us -> 27.9 us  [the longest x3 27.9 us: body(): lax.ppermute(parts[d], 'y', ring(groups, d))]
    concatenate x0 -> x5, other arithmetic: none -> 24.9 us  [the longest x3 20.9 us: rolled(): jnp.concatenate([lax.dynamic_slice_in_dim(weight, at * rows, rows) for at...]
    dot_general x0 -> x5, matrix products: none -> 22.1 us  [dot(): return jnp.dot(a, b, preferred_element_type=F32)]
    all_to_all x2 -> x3, starting transfers between devices: 7.21 us -> 18.6 us  [the longest x1 7.99 us: body(): got = lax.all_to_all(shaped, EP, split_axis=0, concat_axis=0, tiled=True)]
    unnamed x19 -> x58, local copies, waits for them, and re-layouts: 6.35 us -> 15.5 us
  transfers between devices with their start and end apart: 7 -> 9, of which waited for: 4 -> 3; matrix products, arithmetic and copies ran while one was open for 3% -> 20% of each run, Pallas kernels for 17% -> 7%
where the time goes in v2:
time: 200 us; the launch traced here: 199 us
  waiting for transfers between devices  76.9 us (38%)
  other arithmetic  30.9 us (15%)
  starting transfers between devices  23.9 us (12%)
  Pallas kernels  23.2 us (12%)
  matrix products  22.1 us (11%)
  local copies, waits for them, and re-layouts  20.6 us (10%)
    all_to_all x1, waiting for transfers between devices, body(): got = lax.all_to_all(shaped, EP, split_axis=0, concat_axis=0, tiled=True)  35.7 us
    ppermute x3, waiting for transfers between devices, body(): lax.ppermute(parts[d], 'y', ring(groups, d))  27.9 us
    dot_general x5, matrix products, dot(): return jnp.dot(a, b, preferred_element_type=F32)  22.1 us
    concatenate x3, other arithmetic, rolled(): jnp.concatenate([lax.dynamic_slice_in_dim(weight, at * rows, rows) for at...  20.9 us
    unnamed x58, local copies, waits for them, and re-layouts  15.5 us
    pallas_call x1, Pallas kernels, local_sweeps(): pl.pallas_call(after(functools.partial(local_kernel, steps=steps, rows=ro...  13.9 us
    all_to_all x1, waiting for transfers between devices, body(): line = lax.all_to_all(message, EP, split_axis=0, concat_axis=0, tiled=True)  13.3 us
    all_to_all x1, starting transfers between devices, body(): got = lax.all_to_all(shaped, EP, split_axis=0, concat_axis=0, tiled=True)  7.99 us
  transfers between devices with their start and end apart: 9, of which 3 were waited for; matrix products, arithmetic and copies ran while one was open for 20% of the time, Pallas kernels for 7%

profile of v2, /device:TPU:0, one launch (start us, length us, event | category | flops | bytes accessed | tf_op | source)
XLA Modules:
  0.0 198.8 jit_solution(570266533636153882)
XLA Ops:
  0.7 0.7 copy-done.1
  1.4 1.4 copy-done.5
  2.8 0.7 copy-done.10
  3.5 3.8 %dispatch.1.refs_9_ = bf16[1152,1024]{1,0:T(8,128)(2,1)} custom-call(s32[3]{0:T(128)S(1)} %pad_add_fusion.idx_ref.refs_0_, bf16[384,2048]{1,0:T(8,128)(2,1)S(1)} %copy-done.5, f32[1,2048]{1,0:T(1,128)S(1)} %bitcast.89, s32[2,384]{1,0:T(2,128)S(1)} %bitcast.87), custom_call_target="tpu_custom_call" | custom-call | flops 1250000000 | tf_op jit(solution)/shard_map/dispatch/pallas_call | solution.py:96
  7.3 8.0 %all-to-all-start.1 = ((bf16[16,72,1024]{2,1,0:T(8,128)(2,1)}), bf16[16,72,1024]{2,1,0:T(8,128)(2,1)S(1)}, u32[]{:S(2)}, u32[]{:S(2)}) async-start(bf16[16,72,1024]{2,1,0:T(8,128)(2,1)} %bitcast.8), calls=%async_computation.1 | async-start | bytes 4718592 | tf_op jit(solution)/shard_map/all_to_all | solution.py:489
  15.3 35.7 %all-to-all-done.1 = bf16[16,72,1024]{2,1,0:T(8,128)(2,1)S(1)} async-done(((bf16[16,72,1024]{2,1,0:T(8,128)(2,1)}), bf16[16,72,1024]{2,1,0:T(8,128)(2,1)S(1)}, u32[]{:S(2)}, u32[]{:S(2)}) %all-to-all-start.1) | async-done | bytes 2359328 | tf_op jit(solution)/shard_map/all_to_all | solution.py:489
  51.1 1.9 dynamic-slice_bitcast_fusion.7
  53.0 1.7 pad_maximum_fusion.5
  54.6 1.0 copy-done.15
  55.6 0.8 copy-done.16
  56.4 0.5 dynamic-slice_bitcast_fusion.1
  56.9 1.7 pad_maximum_fusion.2
  58.6 1.8 pad_maximum_fusion.3
  60.4 1.5 slice-done.1
  61.9 2.8 %constant_dynamic-slice_fusion.3 = (bf16[512,2048]{1,0:T(8,128)(2,1)S(1)}, bf16[512,2048]{1,0:T(8,128)(2,1)S(1)}, bf16[512,2048]{1,0:T(8,128)(2,1)S(1)}, bf16[512,2048]{1,0:T(8,128)(2,1)}) fusion(bf16[2048,2048]{1,0:T(8,128)(2,1)S(1)} %bitcast.95, s32[]{:T(128)S(6)} %select_n.87, s32[]{:T(128)S(6)} %select_n.89, s32[]{:T(128)S(6)} %select_n.93, s32[]{:T(128)S(6)} %select_n.91), kind=kLoop, calls=%fused_computation.56 | loop fusion | bytes 16777232 | tf_op jit(solution)/shard_map/dynamic_slice | solution.py:479
  64.7 17.3 %pad_maximum_fusion = bf16[2048,2048]{1,0:T(8,128)(2,1)} fusion(bf16[512,2048]{1,0:T(8,128)(2,1)S(1)} %get-tuple-element.28, bf16[512,2048]{1,0:T(8,128)(2,1)} %get-tuple-element.29, bf16[512,2048]{1,0:T(8,128)(2,1)S(1)} %get-tuple-element.27, bf16[512,2048]{1,0:T(8,128)(2,1)S(1)} %get-tuple-element.26), kind=kLoop, calls=%fused_computation | loop fusion | flops 33554432 | bytes 16777216 | tf_op jit(solution)/shard_map/concatenate | solution.py:478
  82.0 2.3 %pad_maximum_fusion.1 = bf16[1152,2048]{1,0:T(8,128)(2,1)S(1)} fusion(bf16[1152,1024]{1,0:T(8,128)(2,1)} %collective-permute-done, bf16[1152,1024]{1,0:T(8,128)(2,1)S(1)} %bitcast.93), kind=kLoop, calls=%fused_computation.1 | loop fusion | flops 9437184 | bytes 9437184 | tf_op jit(solution)/shard_map/concatenate | solution.py:493
  84.4 0.1 copy-done.13
  84.5 3.8 %fusion.14 = f32[1152,640]{1,0:T(8,128)S(1)} fusion(bf16[1152,2048]{1,0:T(8,128)(2,1)S(1)} %pad_maximum_fusion.1, bf16[2048,640]{1,0:T(8,128)(2,1)S(1)} %copy-done.13), kind=kOutput, calls=%fused_computation.60 | convolution fusion | flops 3019898880 | bytes 10289152 | tf_op jit(solution)/shard_map/dot_general | solution.py:46
  88.3 4.2 %multiply_convert_fusion = bf16[1152,640]{1,0:T(8,128)(2,1)S(1)} fusion(f32[1152,640]{1,0:T(8,128)S(1)} %fusion.14, bf16[1152,2048]{1,0:T(8,128)(2,1)S(1)} %pad_maximum_fusion.1, bf16[2048,640]{1,0:T(8,128)(2,1)S(1)} %copy-done.14), kind=kOutput, calls=%fused_computation.4 | convolution fusion | flops 3024322560 | bytes 11763712 | tf_op jit(solution)/shard_map/dot_general | solution.py:46
  92.6 3.5 %convolution_convert_fusion = bf16[1152,1024]{1,0:T(8,128)(2,1)} fusion(bf16[1152,640]{1,0:T(8,128)(2,1)S(1)} %multiply_convert_fusion, bf16[640,1024]{1,0:T(8,128)(2,1)S(1)} %copy-done.17), kind=kOutput, calls=%fused_computation.2 | convolution fusion | flops 1511129088 | bytes 5144576 | tf_op jit(solution)/shard_map/dot_general | solution.py:46
  96.0 0.5 collective-permute-start.1
  96.5 0.2 copy.19.refs_8_
  96.8 2.2 %copy-done.4 = bf16[1024,2048]{1,0:T(8,128)(2,1)S(1)} copy-done((bf16[1024,2048]{1,0:T(8,128)(2,1)S(1)}, bf16[1024,2048]{1,0:T(8,128)(2,1)}, u32[]{:S(2)}) %copy-start.4) | copy-done | bytes 4194328
  99.0 1.2 copy-done.6
  100.2 1.2 copy-done.7
  101.4 1.2 copy-done.8
  102.7 1.2 copy-done.9
  103.9 13.9 %local_sweeps.1 = (f32[1024,256]{1,0:T(8,128)S(1)}, bf16[1024,256]{1,0:T(8,128)(2,1)S(1)}, bf16[1024,256]{1,0:T(8,128)(2,1)S(1)}, bf16[16,264,128]{2,1,0:T(8,128)(2,1)S(1)}) custom-call(s32[3]{0:T(128)S(1)} %pad_add_fusion.idx_ref.refs_0_, bf16[1024,2048]{1,0:T(8,128)(2,1)S(1)} %copy-done.4, f32[1,2048]{1,0:T(1,128)S(1)} %bitcast.90, ...), custom_call_target="tpu_custom_call" | custom-call | flops 4249999872 | tf_op jit(solution)/shard_map/local_sweeps/pallas_call | solution.py:263
  117.8 1.0 copy-done
  118.8 3.7 %all-to-all-start = ((bf16[16,264,128]{2,1,0:T(8,128)(2,1)}), bf16[16,264,128]{2,1,0:T(8,128)(2,1)S(1)}, u32[]{:S(2)}, u32[]{:S(2)}) async-start(bf16[16,264,128]{2,1,0:T(8,128)(2,1)} %copy-done), calls=%async_computation | async-start | bytes 2162688 | tf_op jit(solution)/shard_map/all_to_all | solution.py:492
  122.5 5.2 %convolution_convert_fusion.1 = bf16[1152,1024]{1,0:T(8,128)(2,1)} fusion(bf16[1152,640]{1,0:T(8,128)(2,1)} %copy-done.21, bf16[640,1024]{1,0:T(8,128)(2,1)} %get-tuple-element.20), kind=kOutput, calls=%fused_computation.3 | convolution fusion | flops 1511129088 | bytes 5144576 | tf_op jit(solution)/shard_map/dot_general | solution.py:46
  127.7 13.3 %all-to-all-done.refs_7_ = bf16[16,264,128]{2,1,0:T(8,128)(2,1)S(1)} async-done(((bf16[16,264,128]{2,1,0:T(8,128)(2,1)}), bf16[16,264,128]{2,1,0:T(8,128)(2,1)S(1)}, u32[]{:S(2)}, u32[]{:S(2)}) %all-to-all-start) | async-done | bytes 1081376 | tf_op jit(solution)/shard_map/all_to_all | solution.py:492
  141.0 2.9 %fusion = (bf16[1,1152,256]{2,1,0:T(8,128)(2,1)S(1)}, bf16[1,1152,256]{2,1,0:T(8,128)(2,1)S(1)}, bf16[1,1152,256]{2,1,0:T(8,128)(2,1)S(1)}, bf16[1,1152,256]{2,1,0:T(8,128)(2,1)S(1)}) fusion(bf16[1152,1024]{1,0:T(8,128)(2,1)} %convolution_convert_fusion.1, bf16[1152,1024]{1,0:T(8,128)(2,1)} %collective-permute-done.1), kind=kLoop, calls=%fused_computation.20 | loop fusion | flops 4718592 | bytes 7077888 | tf_op jit(solution)/shard_map/stack | solution.py:500
  144.0 1.7 pad_maximum_fusion.4
  145.7 3.5 %finish.1 = (bf16[4,128,256]{2,1,0:T(8,128)(2,1)S(1)}, bf16[4,128,256]{2,1,0:T(8,128)(2,1)}) custom-call(s32[3]{0:T(128)S(1)} %pad_add_fusion.idx_ref.refs_0_, f32[1024,256]{1,0:T(8,128)S(1)} %get-tuple-element.14.refs_1_.refs_4_, bf16[1024,256]{1,0:T(8,128)(2,1)S(1)} %get-tuple-element.15.refs_2_.refs_5_, ...), custom_call_target="tpu_custom_call" | custom-call | flops 1000000000 | tf_op jit(solution)/shard_map/finish/pallas_call | solution.py:353
  149.2 0.1 copy.20.routes_ref
  149.4 0.1 copy.21.logits_ref
  149.5 6.9 %all-to-all-start.2 = ((bf16[64,72,256]{2,1,0:T(8,128)(2,1)}), bf16[64,72,256]{2,1,0:T(8,128)(2,1)S(1)}, u32[]{:S(2)}, u32[]{:S(2)}) async-start(bf16[64,72,256]{2,1,0:T(8,128)(2,1)} %bitcast.26.refs_9_), calls=%async_computation.2 | async-start | bytes 4718592 | tf_op jit(solution)/shard_map/all_to_all | solution.py:507
  156.5 0.7 copy-done.18
  157.2 1.0 broadcast_select_fusion
  158.3 3.1 %collective-permute-start.5 = (bf16[2,128,256]{2,1,0:T(8,128)(2,1)S(1)}, bf16[2,128,256]{2,1,0:T(8,128)(2,1)S(1)}, u32[]{:S(2)}, u32[]{:S(2)}) collective-permute-start(bf16[2,128,256]{2,1,0:T(8,128)(2,1)S(1)} %pad_maximum_fusion.9), channel_id=1, source_target_pairs={{0,6},{2,0},{4,2},{6,4},{1,7},{3,1},{5,3},{7,5},{8,14},{10,8},{12,... | collective-permute-start | bytes 393224 | tf_op jit(solution)/shard_map/ppermute | solution.py:516
  161.3 0.7 collective-permute-start.4
  162.1 1.0 collective-permute-start.3
  163.1 27.9 %collective-permute-done.3 = bf16[2,128,256]{2,1,0:T(8,128)(2,1)S(1)} collective-permute-done((bf16[2,128,256]{2,1,0:T(8,128)(2,1)S(1)}, bf16[2,128,256]{2,1,0:T(8,128)(2,1)S(1)}, u32[]{:S(2)}, u32[]{:S(2)}) %collective-permute-start.3) | collective-permute-done | bytes 131104 | tf_op jit(solution)/shard_map/ppermute | solution.py:516
  191.1 5.5 %convolution_convert_fusion.2 = bf16[128,2048]{1,0:T(8,128)(2,1)} fusion(bf16[128,2048]{1,0:T(8,128)(2,1)S(1)} %fusion.4, bf16[2048,2048]{1,0:T(8,128)(2,1)} %pad_maximum_fusion), kind=kOutput, calls=%fused_computation.7 | convolution fusion | flops 1074003968 | bytes 9437184 | tf_op jit(solution)/shard_map/dot_general | solution.py:46
  196.5 0.3 add_convert_fusion
  196.9 2.0 combine.1
  (57 shorter events, 0.3 us)
Async XLA Ops:
  0.7 0.7 copy-start.1
  1.4 1.4 copy-start.5
  2.8 0.7 copy-start.10
  7.3 43.8 %all-to-all-start.1 = ((bf16[16,72,1024]{2,1,0:T(8,128)(2,1)}), bf16[16,72,1024]{2,1,0:T(8,128)(2,1)S(1)}, u32[]{:S(2)}, u32[]{:S(2)}) async-start(bf16[16,72,1024]{2,1,0:T(8,128)(2,1)} %bitcast.8), calls=%async_computation.1 | async-start | bytes 4718592 | tf_op jit(solution)/shard_map/all_to_all | solution.py:489
  51.0 31.0 %collective-permute-start = (bf16[1152,1024]{1,0:T(8,128)(2,1)S(1)}, bf16[1152,1024]{1,0:T(8,128)(2,1)}, u32[]{:S(2)}, u32[]{:S(2)}) collective-permute-start(bf16[1152,1024]{1,0:T(8,128)(2,1)S(1)} %bitcast.92), channel_id=1, source_target_pairs={{0,1},{1,0},{2,3},{3,2},{4,5},{5,4},{6,7},{7,6},{8,9},{9,8},{10,11... | collective-permute-start | bytes 7077896 | tf_op jit(solution)/shard_map/ppermute | solution.py:491
  52.9 2.7 %copy-start.15 = (bf16[1,2048,640]{2,1,0:T(8,128)(2,1)S(1)}, bf16[1,2048,640]{2,1,0:T(8,128)(2,1)}, u32[]{:S(2)}) copy-start(bf16[1,2048,640]{2,1,0:T(8,128)(2,1)} %param.32) | copy-start | bytes 7864324
  53.0 3.5 %copy-start.16 = (bf16[1,2048,640]{2,1,0:T(8,128)(2,1)S(1)}, bf16[1,2048,640]{2,1,0:T(8,128)(2,1)}, u32[]{:S(2)}) copy-start(bf16[1,2048,640]{2,1,0:T(8,128)(2,1)} %param.31) | copy-start | bytes 7864324
  56.4 4.0 %slice-start = ((s8[8388608]{0:T(1024)(128)(4,1)}), s8[4194304]{0:T(1024)(128)(4,1)S(1)}, s32[]{:S(2)}) async-start(s8[8388608]{0:T(1024)(128)(4,1)} %bitcast.94), calls=%async_computation.3 | async-start | bytes 8388608
  56.9 5.0 %slice-start.1 = ((s8[8388608]{0:T(1024)(128)(4,1)}), s8[4194304]{0:T(1024)(128)(4,1)S(1)}, s32[]{:S(2)}) async-start(s8[8388608]{0:T(1024)(128)(4,1)} %bitcast.94), calls=%async_computation.4 | async-start | bytes 8388608
  82.0 2.4 %copy-start.13 = (bf16[2048,640]{1,0:T(8,128)(2,1)S(1)}, bf16[2048,640]{1,0:T(8,128)(2,1)}, u32[]{:S(2)}) copy-start(bf16[2048,640]{1,0:T(8,128)(2,1)} %pad_maximum_fusion.2) | copy-start | bytes 7864324
  84.5 3.9 %copy-start.14 = (bf16[2048,640]{1,0:T(8,128)(2,1)S(1)}, bf16[2048,640]{1,0:T(8,128)(2,1)}, u32[]{:S(2)}) copy-start(bf16[2048,640]{1,0:T(8,128)(2,1)} %pad_maximum_fusion.3) | copy-start | bytes 7864324
  88.3 4.2 %copy-start.17 = (bf16[640,1024]{1,0:T(8,128)(2,1)S(1)}, bf16[640,1024]{1,0:T(8,128)(2,1)}, u32[]{:S(2)}) copy-start(bf16[640,1024]{1,0:T(8,128)(2,1)} %get-tuple-element.21) | copy-start | bytes 3932164
  92.5 3.5 %copy-start.21 = (bf16[1152,640]{1,0:T(8,128)(2,1)}, bf16[1152,640]{1,0:T(8,128)(2,1)S(1)}, u32[]{:S(2)}) copy-start(bf16[1152,640]{1,0:T(8,128)(2,1)S(1)} %multiply_convert_fusion) | copy-start | bytes 4423684
  92.5 4.0 %copy-start.19 = (f32[1024,2]{0,1:T(2,128)S(1)}, f32[1024,2]{0,1:T(2,128)}, u32[]{:S(2)}) copy-start(f32[1024,2]{0,1:T(2,128)} %param.24) | copy-start | bytes 24580
  92.6 4.2 %copy-start.11 = (f32[2048]{0:T(1024)S(1)}, f32[2048]{0:T(1024)}, u32[]{:S(2)}) copy-start(f32[2048]{0:T(1024)} %param.18) | copy-start | bytes 24580
  92.6 4.2 %copy-start.12 = (f32[256]{0:T(256)S(1)}, f32[256]{0:T(256)}, u32[]{:S(2)}) copy-start(f32[256]{0:T(256)} %param.23) | copy-start | bytes 3076
  96.0 45.0 %collective-permute-start.1 = (bf16[1152,1024]{1,0:T(8,128)(2,1)}, bf16[1152,1024]{1,0:T(8,128)(2,1)}, u32[]{:S(2)}, u32[]{:S(2)}) collective-permute-start(bf16[1152,1024]{1,0:T(8,128)(2,1)} %convolution_convert_fusion), channel_id=1, source_target_pairs={{0,1},{1,0},{2,3},{3,2},{4,5},{5,4},{6,7},{7,6},{8,9},{9,8},{10,11... | collective-permute-start | bytes 7077896 | tf_op jit(solution)/shard_map/ppermute | solution.py:496
  96.8 2.2 %copy-start.4 = (bf16[1024,2048]{1,0:T(8,128)(2,1)S(1)}, bf16[1024,2048]{1,0:T(8,128)(2,1)}, u32[]{:S(2)}) copy-start(bf16[1024,2048]{1,0:T(8,128)(2,1)} %refs_1_.1) | copy-start | bytes 12582916
  99.0 1.2 copy-start.6
  100.2 1.2 copy-start.7
  101.4 1.2 copy-start.8
  102.7 1.2 copy-start.9
  117.8 1.0 copy-start
  118.8 22.2 %all-to-all-start = ((bf16[16,264,128]{2,1,0:T(8,128)(2,1)}), bf16[16,264,128]{2,1,0:T(8,128)(2,1)S(1)}, u32[]{:S(2)}, u32[]{:S(2)}) async-start(bf16[16,264,128]{2,1,0:T(8,128)(2,1)} %copy-done), calls=%async_computation | async-start | bytes 2162688 | tf_op jit(solution)/shard_map/all_to_all | solution.py:492
  144.0 1.7 copy-start.3
  145.7 3.5 %copy-start.2 = (s32[384,2]{0,1:T(2,128)S(1)}, s32[384,2]{0,1:T(2,128)}, u32[]{:S(2)}) copy-start(s32[384,2]{0,1:T(2,128)} %param.29) | copy-start | bytes 9220
  145.7 3.7 %copy-start.20 = (f32[384,2]{0,1:T(2,128)S(1)}, f32[384,2]{0,1:T(2,128)}, u32[]{:S(2)}) copy-start(f32[384,2]{0,1:T(2,128)} %param.30) | copy-start | bytes 9220
  149.2 7.2 %collective-permute-start.2 = (bf16[4,128,256]{2,1,0:T(8,128)(2,1)}, bf16[4,128,256]{2,1,0:T(8,128)(2,1)S(1)}, u32[]{:S(2)}, u32[]{:S(2)}) collective-permute-start(bf16[4,128,256]{2,1,0:T(8,128)(2,1)} %get-tuple-element.24), channel_id=1, source_target_pairs={{0,1},{1,0},{2,3},{3,2},{4,5},{5,4},{6,7},{7,6},{8,9},{9,8},{10,11... | collective-permute-start | bytes 786440 | tf_op jit(solution)/shard_map/ppermute | solution.py:512
  149.5 47.0 %all-to-all-start.2 = ((bf16[64,72,256]{2,1,0:T(8,128)(2,1)}), bf16[64,72,256]{2,1,0:T(8,128)(2,1)S(1)}, u32[]{:S(2)}, u32[]{:S(2)}) async-start(bf16[64,72,256]{2,1,0:T(8,128)(2,1)} %bitcast.26.refs_9_), calls=%async_computation.2 | async-start | bytes 4718592 | tf_op jit(solution)/shard_map/all_to_all | solution.py:507
  156.5 0.7 copy-start.18
  158.3 32.8 %collective-permute-start.5 = (bf16[2,128,256]{2,1,0:T(8,128)(2,1)S(1)}, bf16[2,128,256]{2,1,0:T(8,128)(2,1)S(1)}, u32[]{:S(2)}, u32[]{:S(2)}) collective-permute-start(bf16[2,128,256]{2,1,0:T(8,128)(2,1)S(1)} %pad_maximum_fusion.9), channel_id=1, source_target_pairs={{0,6},{2,0},{4,2},{6,4},{1,7},{3,1},{5,3},{7,5},{8,14},{10,8},{12,... | collective-permute-start | bytes 393224 | tf_op jit(solution)/shard_map/ppermute | solution.py:516
  161.3 29.7 %collective-permute-start.4 = (bf16[2,128,256]{2,1,0:T(8,128)(2,1)S(1)}, bf16[2,128,256]{2,1,0:T(8,128)(2,1)S(1)}, u32[]{:S(2)}, u32[]{:S(2)}) collective-permute-start(bf16[2,128,256]{2,1,0:T(8,128)(2,1)S(1)} %pad_maximum_fusion.8), channel_id=1, source_target_pairs={{0,4},{2,6},{4,0},{6,2},{1,5},{3,7},{5,1},{7,3},{8,12},{10,14},{12... | collective-permute-start | bytes 393224 | tf_op jit(solution)/shard_map/ppermute | solution.py:516
  162.1 28.9 %collective-permute-start.3 = (bf16[2,128,256]{2,1,0:T(8,128)(2,1)S(1)}, bf16[2,128,256]{2,1,0:T(8,128)(2,1)S(1)}, u32[]{:S(2)}, u32[]{:S(2)}) collective-permute-start(bf16[2,128,256]{2,1,0:T(8,128)(2,1)S(1)} %pad_maximum_fusion.7), channel_id=1, source_target_pairs={{0,2},{2,4},{4,6},{6,0},{1,3},{3,5},{5,7},{7,1},{8,10},{10,12},{12... | collective-permute-start | bytes 393224 | tf_op jit(solution)/shard_map/ppermute | solution.py:516

commit v3 on v2

--- a/solution.py
+++ b/solution.py
@@ -17,7 +17,7 @@
 EPSILON = 1e-06
 BF = jnp.bfloat16
 F32 = jnp.float32
-CHUNKS = ((0, 72),)
+CHUNKS = ((0, 40), (40, 32))
 COST_UNIT = 250e6
 
 
@@ -103,7 +103,7 @@
             pl.BlockSpec(memory_space=pltpu.VMEM),
         ],
         out_specs=tuple(pl.BlockSpec(memory_space=pltpu.VMEM) for _ in CHUNKS),
-        compiler_params=params(16),
+        compiler_params=params(56),
         cost_estimate=cost(5),
         name="dispatch",
     )(idx, tokens, gain, routes_t)
@@ -125,10 +125,19 @@
     wv_ref,
     floor_ref,
     shift_ref,
+    wg_ref,
+    wu_ref,
+    wd_ref,
+    wo_ref,
     o_ref,
     qf_ref,
     qb_ref,
     msg_ref,
+    wg_out,
+    wu_out,
+    theirs_out,
+    mine_out,
+    wo_out,
     q_s,
     v_s,
     kb_s,
@@ -136,13 +145,67 @@
     st_s,
     off_s,
     kept_s,
+    wg_s,
+    wu_s,
+    theirs_s,
+    mine_s,
+    wo_s,
+    sems,
     *,
     steps,
     rows,
     heads,
+    groups,
 ):
     step = pl.program_id(0)
     width = heads * DK
+    core, chip = idx_ref[0], idx_ref[1]
+    loads = []
+
+    def load(source, target):
+        loads.append(pltpu.make_async_copy(source, target, sems.at[len(loads)]))
+
+    half = wg_ref.shape[0] // 2
+    for i in range(2):
+        taken = pl.ds(pl.multiple_of(lax.rem(core + i, 2) * half, half), half)
+        put = slice(i * half, (i + 1) * half)
+        load(wg_ref.at[taken, :], wg_s.at[put, :])
+        load(wu_ref.at[taken, :], wu_s.at[put, :])
+    cols = wd_ref.shape[1] // (2 * groups)
+    share = wo_ref.shape[0] // groups
+    for d in range(groups):
+        put = slice(d * cols, (d + 1) * cols)
+        block = 2 * lax.rem(chip + d, groups)
+        for target, which in ((theirs_s, 1 - core), (mine_s, core)):
+            taken = pl.ds(pl.multiple_of((block + which) * cols, cols), cols)
+            load(wd_ref.at[:, taken], target.at[:, put])
+        source = lax.rem(chip + groups - d, groups)
+        taken = pl.ds(pl.multiple_of(source * share, share), share)
+        load(wo_ref.at[taken, :], wo_s.at[d * share : (d + 1) * share, :])
+    stores = [
+        pltpu.make_async_copy(source, target, sems.at[len(loads) + i])
+        for i, (source, target) in enumerate(
+            (
+                (wg_s, wg_out),
+                (wu_s, wu_out),
+                (theirs_s, theirs_out),
+                (mine_s, mine_out),
+                (wo_s, wo_out),
+            )
+        )
+    ]
+
+    @pl.when(step == 0)
+    def _():
+        for copy in loads:
+            copy.start()
+
+    @pl.when(step == steps // 2)
+    def _():
+        for copy in loads:
+            copy.wait()
+        for copy in stores:
+            copy.start()
 
     @pl.when(step == 0)
     def _():
@@ -251,9 +314,13 @@
             o_ref[rs, :] = o_ref[rs, :] + result
             qb_ref[rs, :] = carried
         write_message(1, back, total)
-
-
-def local_sweeps(idx, tokens, gain, wq, wf, wb, wv, floor, shift, segments, deps=()):
+        for copy in stores:
+            copy.wait()
+
+
+def local_sweeps(
+    idx, tokens, gain, wq, wf, wb, wv, floor, shift, wg, wu, wd, wo, segments, groups, deps=()
+):
     seg, model = tokens.shape
     width = wq.shape[1]
     heads = width // DK
@@ -261,13 +328,22 @@
     steps = seg // rows
     whole = lambda shape: pl.BlockSpec(shape, lambda i: tuple(0 for _ in shape))
     return pl.pallas_call(
-        after(functools.partial(local_kernel, steps=steps, rows=rows, heads=heads), 9, deps),
+        after(
+            functools.partial(local_kernel, steps=steps, rows=rows, heads=heads, groups=groups),
+            13,
+            deps,
+        ),
         grid=(steps,),
         out_shape=(
             jax.ShapeDtypeStruct((seg, width), F32),
             jax.ShapeDtypeStruct((seg, width), BF),
             jax.ShapeDtypeStruct((seg, width), BF),
             jax.ShapeDtypeStruct((segments, heads * DV + 8, DK), BF),
+            jax.ShapeDtypeStruct(wg.shape, BF),
+            jax.ShapeDtypeStruct(wu.shape, BF),
+            jax.ShapeDtypeStruct((wd.shape[0], wd.shape[1] // 2), BF),
+            jax.ShapeDtypeStruct((wd.shape[0], wd.shape[1] // 2), BF),
+            jax.ShapeDtypeStruct(wo.shape, BF),
         ),
         in_specs=[
             pl.BlockSpec(memory_space=pltpu.SMEM),
@@ -279,6 +355,7 @@
             whole((model, width)),
             whole((1, width)),
             pl.BlockSpec((rows, heads), lambda i: (i, 0)),
+            *any_specs((wg, wu, wd, wo)),
             *any_specs(deps),
         ],
         out_specs=(
@@ -286,6 +363,7 @@
             whole((seg, width)),
             whole((seg, width)),
             whole((segments, heads * DV + 8, DK)),
+            *any_specs(range(5)),
         ),
         scratch_shapes=[
             pltpu.VMEM((seg, width), F32),
@@ -295,11 +373,17 @@
             pltpu.VMEM((heads, DV, DK), F32),
             pltpu.VMEM((1, width), F32),
             pltpu.VMEM((8, DK), F32),
+            pltpu.VMEM(wg.shape, BF),
+            pltpu.VMEM(wu.shape, BF),
+            pltpu.VMEM((wd.shape[0], wd.shape[1] // 2), BF),
+            pltpu.VMEM((wd.shape[0], wd.shape[1] // 2), BF),
+            pltpu.VMEM(wo.shape, BF),
+            pltpu.SemaphoreType.DMA((9 + 3 * groups,)),
         ],
-        compiler_params=params(28, "arbitrary"),
+        compiler_params=params(48, "arbitrary"),
         cost_estimate=cost(17),
         name="local_sweeps",
-    )(idx, tokens, gain, wq, wf, wb, wv, floor, shift, *deps)
+    )(idx, tokens, gain, wq, wf, wb, wv, floor, shift, wg, wu, wd, wo, *deps)
 
 
 def finish_kernel(idx_ref, *refs, heads):
@@ -408,7 +492,7 @@
     rows = routes.shape[0]
     cols = returned[0].shape[1]
     return pl.pallas_call(
-        functools.partial(combine_kernel, chunks=CHUNKS, experts=experts),
+        functools.partial(combine_kernel, chunks=((0, sum(n for _, n in CHUNKS)),), experts=experts),
         out_shape=jax.ShapeDtypeStruct((rows, cols), BF),
         in_specs=[pl.BlockSpec(memory_space=pltpu.VMEM) for _ in range(2 + len(returned))],
         out_specs=pl.BlockSpec(memory_space=pltpu.VMEM),
@@ -449,7 +533,7 @@
     wg, wu, wd = w_expert_gate[0], w_expert_up[0], w_expert_down[0]
 
     outgoing = dispatch(idx, moe_tokens, moe_gain[None], routes.T, experts)
-    o, qf, qb, message = local_sweeps(
+    o, qf, qb, message, wg, wu, wd_theirs, wd_mine, w_out_rolled = local_sweeps(
         idx,
         mix_tokens,
         mix_gain[None],
@@ -459,64 +543,55 @@
         w_value,
         decay_floor[None],
         decay_shift,
+        wg,
+        wu,
+        wd,
+        w_out,
         experts,
+        groups,
         deps=outgoing,
     )
-    part = wd.shape[1] // (2 * groups)
-
-    def by_core(which):
-        return jnp.concatenate(
-            [
-                lax.dynamic_slice_in_dim(wd, (2 * g + which) * part, part, axis=1)
-                for g in range(groups)
-            ],
-            axis=1,
-        )
-
-    def rolled(weight, shares, order):
-        rows = weight.shape[0] // shares
-        return jnp.concatenate(
-            [lax.dynamic_slice_in_dim(weight, at * rows, rows) for at in order], axis=0
-        )
-
-    wg, wu = (rolled(w, 2, (core, 1 - core)) for w in (wg, wu))
-    w_out_rolled = rolled(w_out, groups, [(chip + groups - d) % groups for d in range(groups)])
-    wd_theirs, wd_mine, wg, wu, w_out_rolled = lax.optimization_barrier(
-        (by_core(1 - core), by_core(core), wg, wu, w_out_rolled)
-    )
-    (rows,), ((_, count),) = outgoing, CHUNKS
-    shaped = rows.reshape(experts, count, rows.shape[1])
-    got = lax.all_to_all(shaped, EP, split_axis=0, concat_axis=0, tiled=True)
-    own = got.reshape(rows.shape)
-    other = lax.ppermute(own, "c", swap)
+    landed = []
+    arrived = []
+    for rows, (_, count) in zip(outgoing, CHUNKS):
+        shaped = rows.reshape(experts, count, rows.shape[1])
+        got = lax.all_to_all(shaped, EP, split_axis=0, concat_axis=0, tiled=True)
+        arrived.append(got.reshape(rows.shape))
+    arrived[-1], message = lax.optimization_barrier((arrived[-1], message))
     line = lax.all_to_all(message, EP, split_axis=0, concat_axis=0, tiled=True)
-    x = lax.optimization_barrier(jnp.concatenate([own, other], axis=1))
-    hidden = (jax.nn.silu(dot(x, wg)) * dot(x, wu)).astype(BF)
-    for_partner = dot(hidden, wd_theirs).astype(BF)
-    received = lax.ppermute(for_partner, "c", swap)
-    mine = lax.optimization_barrier(dot(hidden, wd_mine).astype(BF))
-    received, _ = lax.optimization_barrier((received, line))
-    cols = received.shape[1] // groups
-    pair = jnp.stack(
-        [
-            (mine[:, at : at + cols].astype(F32) + received[:, at : at + cols].astype(F32)).astype(BF)
+    for own in arrived:
+        other = lax.ppermute(own, "c", swap)
+        x = lax.optimization_barrier(jnp.concatenate([own, other], axis=1))
+        hidden = (jax.nn.silu(dot(x, wg)) * dot(x, wu)).astype(BF)
+        for_partner = dot(hidden, wd_theirs).astype(BF)
+        received = lax.ppermute(for_partner, "c", swap)
+        mine = lax.optimization_barrier(dot(hidden, wd_mine).astype(BF))
+        cols = received.shape[1] // groups
+        pair = [
+            (
+                mine[:, at : at + cols].astype(F32) + received[:, at : at + cols].astype(F32)
+            ).astype(BF)
             for at in range(0, received.shape[1], cols)
         ]
-    )
-    shaped = pair.reshape((groups * experts, count, cols))
-    back = lax.all_to_all(shaped, ("y", "z", "x"), split_axis=0, concat_axis=0, tiled=True)
-    back = back.reshape(pair.shape)
-    summed = sum(back[g].astype(F32) for g in range(groups)).astype(BF)
-    returned = [summed]
-    keep, give = finish(idx, o, qf, qb, line, head_gain[None], groups, deps=(shaped,))
+        landed.append([pair[0]] + [lax.ppermute(pair[d], "y", ring(groups, d)) for d in (2, 1, 3)])
+    keep, give = finish(idx, o, qf, qb, line, head_gain[None], groups, deps=tuple(pair[1:]))
     given = lax.ppermute(give, "c", swap)
     lower = jnp.where(core == 0, keep, given)
     upper = jnp.where(core == 0, given, keep)
     parts = [jnp.stack([lower[d], upper[d]]) for d in range(groups)]
     moved = [parts[0]] + [lax.ppermute(parts[d], "y", ring(groups, d)) for d in range(1, groups)]
-    moe_out = combine(routes, route_logits, returned, experts)
+    shaped = jnp.concatenate(
+        [
+            sum(part.astype(F32) for part in chunk).astype(BF).reshape(experts, -1, cols)
+            for chunk in landed
+        ],
+        axis=1,
+    )
+    back = lax.all_to_all(shaped, EP, split_axis=0, concat_axis=0, tiled=True)
+    returned = [back.reshape(-1, cols)]
     features = jnp.concatenate([part[i] for part in moved for i in range(2)], axis=1)
     mixed_out = dot(features, w_out_rolled).astype(BF)
+    moe_out = combine(routes, route_logits, returned, experts)
     return (mixed_out, moe_out)
 
 

time: 200 us -> 157 us (0.79)
  waiting for transfers between devices: 76.9 us -> 50.9 us
  other arithmetic: 30.9 us -> 10.3 us
  starting transfers between devices: 23.9 us -> 39.8 us
  local copies, waits for them, and re-layouts: 20.6 us -> 8.78 us
  matrix products: 22.1 us -> 19 us
  Pallas kernels: 23.2 us -> 26.2 us
    ppermute x0 -> x6, waiting for transfers between devices: none -> 24.9 us  [body(): lax.ppermute(pair[d], 'y', ring(groups, d))]
    ppermute x3, waiting for transfers between devices: 27.9 us -> 3.5 us  [body(): lax.ppermute(parts[d], 'y', ring(groups, d))]
    concatenate x4 -> x1, other arithmetic: 22.5 us -> 0.87 us  [body(): jnp.concatenate([sum((part.astype(F32) for part in chunk)).astype(BF).res...]
    all_to_all x1 -> x2, waiting for transfers between devices: 35.7 us -> 17.5 us  [body(): got = lax.all_to_all(shaped, EP, split_axis=0, concat_axis=0, tiled=True)]
    all_to_all x1, waiting for transfers between devices: 13.3 us -> 0.01 us  [body(): line = lax.all_to_all(message, EP, split_axis=0, concat_axis=0, tiled=True)]
    ppermute x0 -> x6, starting transfers between devices: none -> 9.38 us  [body(): lax.ppermute(pair[d], 'y', ring(groups, d))]
    unnamed x58 -> x60, local copies, waits for them, and re-layouts: 15.5 us -> 8.75 us
    dynamic_slice x3 -> x0, local copies, waits for them, and re-layouts: 5.1 us -> none  [the longest x2 3.22 us: rolled(): lax.dynamic_slice_in_dim(weight, at * rows, rows)]
  transfers between devices with their start and end apart: 9 -> 18, of which waited for: 3 -> 7; matrix products, arithmetic and copies ran while one was open for 20% -> 18% of each run, Pallas kernels for 7% -> 13%
where the time goes in v3:
time: 157 us; the launch traced here: 156 us
  waiting for transfers between devices  50.9 us (32%)
  starting transfers between devices  39.8 us (25%)
  Pallas kernels  26.2 us (17%)
  matrix products  19 us (12%)
  other arithmetic  10.3 us (7%)
  local copies, waits for them, and re-layouts  8.78 us (6%)
    ppermute x6, waiting for transfers between devices, body(): lax.ppermute(pair[d], 'y', ring(groups, d))  24.9 us
    dot_general x9, matrix products, dot(): return jnp.dot(a, b, preferred_element_type=F32)  19 us
    all_to_all x2, waiting for transfers between devices, body(): got = lax.all_to_all(shaped, EP, split_axis=0, concat_axis=0, tiled=True)  17.5 us
    pallas_call x1, Pallas kernels, local_sweeps(): pl.pallas_call(after(functools.partial(local_kernel, steps=steps, rows=ro...  17.3 us
    all_to_all x2, starting transfers between devices, body(): got = lax.all_to_all(shaped, EP, split_axis=0, concat_axis=0, tiled=True)  12.6 us
    ppermute x6, starting transfers between devices, body(): lax.ppermute(pair[d], 'y', ring(groups, d))  9.38 us
    unnamed x60, local copies, waits for them, and re-layouts  8.75 us
    all_to_all x1, starting transfers between devices, body(): back = lax.all_to_all(shaped, EP, split_axis=0, concat_axis=0, tiled=True)  7.41 us
  transfers between devices with their start and end apart: 18, of which 7 were waited for; matrix products, arithmetic and copies ran while one was open for 18% of the time, Pallas kernels for 13%

profile of v3, /device:TPU:0, one launch (start us, length us, event | category | flops | bytes accessed | tf_op | source)
XLA Modules:
  0.0 156.0 jit_solution(1856796914387246733)
XLA Ops:
  0.6 0.7 pad_add_fusion.idx_ref.refs_0_
  1.3 4.2 %dispatch.1 = (bf16[640,1024]{1,0:T(8,128)(2,1)}, bf16[512,1024]{1,0:T(8,128)(2,1)}) custom-call(s32[3]{0:T(128)} %pad_add_fusion.idx_ref.refs_0_, bf16[384,2048]{1,0:T(8,128)(2,1)} %tok_ref.1, f32[1,2048]{1,0:T(1,128)} %bitcast.79, s32[2,384]{1,0:T(2,128)} %bitcast.78), custom_call_target="tpu_custom_call" | custom-call | flops 1250000000 | tf_op jit(solution)/shard_map/dispatch/pallas_call | solution.py:96
  5.5 8.2 %all-to-all-start = ((bf16[16,32,1024]{2,1,0:T(8,128)(2,1)}), bf16[16,32,1024]{2,1,0:T(8,128)(2,1)}, u32[]{:S(2)}, u32[]{:S(2)}) async-start(bf16[16,32,1024]{2,1,0:T(8,128)(2,1)} %bitcast.72), calls=%async_computation | async-start | bytes 2097152 | tf_op jit(solution)/shard_map/all_to_all | solution.py:558
  14.0 17.5 %all-to-all-done = bf16[16,32,1024]{2,1,0:T(8,128)(2,1)} async-done(((bf16[16,32,1024]{2,1,0:T(8,128)(2,1)}), bf16[16,32,1024]{2,1,0:T(8,128)(2,1)}, u32[]{:S(2)}, u32[]{:S(2)}) %all-to-all-start) | async-done | bytes 1048608 | tf_op jit(solution)/shard_map/all_to_all | solution.py:558
  31.4 4.4 %all-to-all-start.2 = ((bf16[16,40,1024]{2,1,0:T(8,128)(2,1)}), bf16[16,40,1024]{2,1,0:T(8,128)(2,1)}, u32[]{:S(2)}, u32[]{:S(2)}) async-start(bf16[16,40,1024]{2,1,0:T(8,128)(2,1)} %bitcast.21), calls=%async_computation.2 | async-start | bytes 2621440 | tf_op jit(solution)/shard_map/all_to_all | solution.py:558
  35.9 1.2 copy-done
  37.1 1.2 copy-done.1
  38.3 1.2 copy-done.2
  39.5 17.3 %local_sweeps.1 = (f32[1024,256]{1,0:T(8,128)S(1)}, bf16[1024,256]{1,0:T(8,128)(2,1)S(1)}, bf16[1024,256]{1,0:T(8,128)(2,1)S(1)}, bf16[16,264,128]{2,1,0:T(8,128...) custom-call(s32[3]{0:T(128)S(1)} %copy-done.10, ...), custom_call_target="tpu_custom_call" | custom-call | flops 4249999872 | tf_op jit(solution)/shard_map/local_sweeps/pallas_call | solution.py:330
  57.0 0.8 copy.20.routes_ref
  57.8 0.8 copy.21.logits_ref
  58.6 7.1 %all-to-all-start.1 = ((bf16[16,264,128]{2,1,0:T(8,128)(2,1)}), bf16[16,264,128]{2,1,0:T(8,128)(2,1)S(1)}, u32[]{:S(2)}, u32[]{:S(2)}) async-start(bf16[16,264,128]{2,1,0:T(8,128)(2,1)} %get-tuple-element.23), calls=%async_computation.1 | async-start | bytes 2162688 | tf_op jit(solution)/shard_map/all_to_all | solution.py:561
  65.7 0.3 collective-permute-start.6
  66.0 1.9 %pad_maximum_fusion.1 = bf16[512,2048]{1,0:T(8,128)(2,1)S(1)} fusion(bf16[512,1024]{1,0:T(8,128)(2,1)} %collective-permute-done, bf16[512,1024]{1,0:T(8,128)(2,1)} %bitcast.11), kind=kLoop, calls=%fused_computation.2 | loop fusion | flops 4194304 | bytes 4194304 | tf_op jit(solution)/shard_map/concatenate | solution.py:564
  68.1 1.8 %fusion.10 = f32[512,640]{1,0:T(8,128)S(1)} fusion(bf16[512,2048]{1,0:T(8,128)(2,1)S(1)} %pad_maximum_fusion.1, bf16[2048,640]{1,0:T(8,128)(2,1)S(1)} %copy-done.19), kind=kOutput, calls=%fused_computation.44 | convolution fusion | flops 1342177280 | bytes 6029312 | tf_op jit(solution)/shard_map/dot_general | solution.py:46
  69.9 1.8 %multiply_convert_fusion.1 = bf16[512,640]{1,0:T(8,128)(2,1)S(1)} fusion(f32[512,640]{1,0:T(8,128)S(1)} %fusion.10, bf16[512,2048]{1,0:T(8,128)(2,1)S(1)} %pad_maximum_fusion.1, bf16[2048,640]{1,0:T(8,128)(2,1)S(1)} %copy-done.18), kind=kOutput, calls=%fused_computation.8 | convolution fusion | flops 1344143360 | bytes 6684672 | tf_op jit(solution)/shard_map/dot_general | solution.py:46
  71.8 1.0 convolution_convert_fusion.3
  72.8 0.5 collective-permute-start.1
  73.3 1.0 convolution_convert_fusion.4
  74.3 1.9 %pad_maximum_fusion = bf16[640,2048]{1,0:T(8,128)(2,1)S(1)} fusion(bf16[640,1024]{1,0:T(8,128)(2,1)S(1)} %collective-permute-done.6, bf16[640,1024]{1,0:T(8,128)(2,1)} %bitcast.22), kind=kLoop, calls=%fused_computation | loop fusion | flops 5242880 | bytes 5242880 | tf_op jit(solution)/shard_map/concatenate | solution.py:564
  76.3 2.2 %fusion.11 = f32[640,640]{1,0:T(8,128)S(1)} fusion(bf16[640,2048]{1,0:T(8,128)(2,1)S(1)} %pad_maximum_fusion, bf16[2048,640]{1,0:T(8,128)(2,1)S(1)} %copy-done.19), kind=kOutput, calls=%fused_computation.45 | convolution fusion | flops 1677721600 | bytes 6881280 | tf_op jit(solution)/shard_map/dot_general | solution.py:46
  78.5 2.3 %multiply_convert_fusion = bf16[640,640]{1,0:T(8,128)(2,1)S(1)} fusion(f32[640,640]{1,0:T(8,128)S(1)} %fusion.11, bf16[640,2048]{1,0:T(8,128)(2,1)S(1)} %pad_maximum_fusion, bf16[2048,640]{1,0:T(8,128)(2,1)S(1)} %copy-done.18), kind=kOutput, calls=%fused_computation.3 | convolution fusion | flops 1680179200 | bytes 7700480 | tf_op jit(solution)/shard_map/dot_general | solution.py:46
  80.7 2.2 %convolution_convert_fusion.1 = bf16[640,1024]{1,0:T(8,128)(2,1)} fusion(bf16[640,640]{1,0:T(8,128)(2,1)S(1)} %multiply_convert_fusion, bf16[640,1024]{1,0:T(8,128)(2,1)S(1)} %copy-done.22), kind=kOutput, calls=%fused_computation.4 | convolution fusion | flops 839516160 | bytes 3440640 | tf_op jit(solution)/shard_map/dot_general | solution.py:46
  83.0 0.3 collective-permute-start.7
  83.3 1.0 copy-done.13
  84.3 1.0 add_convert_fusion.7
  85.4 0.9 copy-done.3
  86.3 0.9 copy-done.5
  87.3 2.7 %finish.1 = (bf16[4,128,256]{2,1,0:T(8,128)(2,1)S(1)}, bf16[4,128,256]{2,1,0:T(8,128)(2,1)S(1)}) custom-call(s32[3]{0:T(128)S(1)} %copy-done.10, f32[1024,256]{1,0:T(8,128)S(1)} %get-tuple-element.19.refs_1_.refs_4_, bf16[1024,256]{1,0:T(8,128)(2,1)S(1)} %get-tuple-element.20.refs_2_.refs_5_, bf16[1024,256]{1,0:T(8,128)(2,1)S(1)} %get-tuple-element.21.refs_3_.refs_6_, ...), custom_call_target="tpu_custom_call" | custom-call | flops 1000000000 | tf_op jit(solution)/shard_map/finish/pallas_call | solution.py:437
  90.2 1.2 convolution_convert_fusion.2
  91.4 3.1 %collective-permute-start.13 = (bf16[512,256]{1,0:T(8,128)(2,1)S(1)}, bf16[512,256]{1,0:T(8,128)(2,1)S(1)}, u32[]{:S(2)}, u32[]{:S(2)}) collective-permute-start(bf16[512,256]{1,0:T(8,128)(2,1)S(1)} %copy-done.6), channel_id=1, source_target_pairs={{0,6},{2,0},{4,2},{6,4},{1,7},{3,1},{5,3},{7,5},{8,14},{10,8},{12,... | collective-permute-start | bytes 786440 | tf_op jit(solution)/shard_map/ppermute | solution.py:576
  94.5 2.2 %collective-permute-start.11 = (bf16[512,256]{1,0:T(8,128)(2,1)S(1)}, bf16[512,256]{1,0:T(8,128)(2,1)S(1)}, u32[]{:S(2)}, u32[]{:S(2)}) collective-permute-start(bf16[512,256]{1,0:T(8,128)(2,1)S(1)} %get-tuple-element.36.refs_10_), channel_id=1, source_target_pairs={{0,4},{2,6},{4,0},{6,2},{1,5},{3,7},{5,1},{7,3},{8,12},{10,14},{12... | collective-permute-start | bytes 786440 | tf_op jit(solution)/shard_map/ppermute | solution.py:576
  96.8 2.0 %collective-permute-start.3 = (bf16[2,128,256]{2,1,0:T(8,128)(2,1)S(1)}, bf16[2,128,256]{2,1,0:T(8,128)(2,1)S(1)}, u32[]{:S(2)}, u32[]{:S(2)}) collective-permute-start(bf16[2,128,256]{2,1,0:T(8,128)(2,1)S(1)} %pad_maximum_fusion.3), channel_id=1, source_target_pairs={{0,2},{2,4},{4,6},{6,0},{1,3},{3,5},{5,7},{7,1},{8,10},{10,12},{12... | collective-permute-start | bytes 393224 | tf_op jit(solution)/shard_map/ppermute | solution.py:582
  98.8 7.4 %collective-permute-done.13 = bf16[512,256]{1,0:T(8,128)(2,1)S(1)} collective-permute-done((bf16[512,256]{1,0:T(8,128)(2,1)S(1)}, bf16[512,256]{1,0:T(8,128)(2,1)S(1)}, u32[]{:S(2)}, u32[]{:S(2)}) %collective-permute-start.13) | collective-permute-done | bytes 262176 | tf_op jit(solution)/shard_map/ppermute | solution.py:576
  106.2 4.3 %collective-permute-done.12 = bf16[512,256]{1,0:T(8,128)(2,1)S(1)} collective-permute-done((bf16[512,256]{1,0:T(8,128)(2,1)S(1)}, bf16[512,256]{1,0:T(8,128)(2,1)S(1)}, u32[]{:S(2)}, u32[]{:S(2)}) %collective-permute-start.12) | collective-permute-done | bytes 262176 | tf_op jit(solution)/shard_map/ppermute | solution.py:576
  110.5 1.2 add_convert_fusion.5
  111.8 3.5 %collective-permute-done.3 = bf16[2,128,256]{2,1,0:T(8,128)(2,1)S(1)} collective-permute-done((bf16[2,128,256]{2,1,0:T(8,128)(2,1)S(1)}, bf16[2,128,256]{2,1,0:T(8,128)(2,1)S(1)}, u32[]{:S(2)}, u32[]{:S(2)}) %collective-permute-start.3) | collective-permute-done | bytes 131104 | tf_op jit(solution)/shard_map/ppermute | solution.py:582
  115.3 1.4 add_convert_fusion.3
  116.7 2.5 %collective-permute-start.10 = (bf16[640,256]{1,0:T(8,128)(2,1)S(1)}, bf16[640,256]{1,0:T(8,128)(2,1)S(1)}, u32[]{:S(2)}, u32[]{:S(2)}) collective-permute-start(bf16[640,256]{1,0:T(8,128)(2,1)S(1)} %get-tuple-element.33), channel_id=1, source_target_pairs={{0,6},{2,0},{4,2},{6,4},{1,7},{3,1},{5,3},{7,5},{8,14},{10,8},{12,... | collective-permute-start | bytes 983048 | tf_op jit(solution)/shard_map/ppermute | solution.py:576
  119.3 1.5 collective-permute-start.8
  120.8 6.5 %collective-permute-done.10 = bf16[640,256]{1,0:T(8,128)(2,1)S(1)} collective-permute-done((bf16[640,256]{1,0:T(8,128)(2,1)S(1)}, bf16[640,256]{1,0:T(8,128)(2,1)S(1)}, u32[]{:S(2)}, u32[]{:S(2)}) %collective-permute-start.10) | collective-permute-done | bytes 327712 | tf_op jit(solution)/shard_map/ppermute | solution.py:576
  127.4 6.7 %collective-permute-done.9 = bf16[640,256]{1,0:T(8,128)(2,1)S(1)} collective-permute-done((bf16[640,256]{1,0:T(8,128)(2,1)S(1)}, bf16[640,256]{1,0:T(8,128)(2,1)S(1)}, u32[]{:S(2)}, u32[]{:S(2)}) %collective-permute-start.9) | collective-permute-done | bytes 327712 | tf_op jit(solution)/shard_map/ppermute | solution.py:576
  134.1 1.2 add_convert_fusion
  135.3 0.9 pad_maximum_fusion.2
  136.2 7.4 %all-to-all-start.3 = ((bf16[16,72,256]{2,1,0:T(8,128)(2,1)}), bf16[16,72,256]{2,1,0:T(8,128)(2,1)S(1)}, u32[]{:S(2)}, u32[]{:S(2)}) async-start(bf16[16,72,256]{2,1,0:T(8,128)(2,1)} %pad_maximum_fusion.2), calls=%async_computation.3 | async-start | bytes 1179648 | tf_op jit(solution)/shard_map/all_to_all | solution.py:590
  143.6 5.5 %convolution_convert_fusion = bf16[128,2048]{1,0:T(8,128)(2,1)} fusion(bf16[128,2048]{1,0:T(8,128)(2,1)S(1)} %fusion, bf16[2048,2048]{1,0:T(8,128)(2,1)} %get-tuple-element.31), kind=kOutput, calls=%fused_computation.1 | convolution fusion | flops 1074003968 | bytes 9437184 | tf_op jit(solution)/shard_map/dot_general | solution.py:46
  149.1 5.0 %all-to-all-done.3 = bf16[16,72,256]{2,1,0:T(8,128)(2,1)S(1)} async-done(((bf16[16,72,256]{2,1,0:T(8,128)(2,1)}), bf16[16,72,256]{2,1,0:T(8,128)(2,1)S(1)}, u32[]{:S(2)}, u32[]{:S(2)}) %all-to-all-start.3) | async-done | bytes 589856 | tf_op jit(solution)/shard_map/all_to_all | solution.py:590
  154.1 2.0 %combine.1 = bf16[384,256]{1,0:T(8,128)(2,1)} custom-call(s32[384,2]{1,0:T(8,128)S(1)} %copy-done.7, f32[384,2]{1,0:T(8,128)S(1)} %copy-done.8, bf16[1152,256]{1,0:T(8,128)(2,1)S(1)} %bitcast.68), custom_call_target="tpu_custom_call" | custom-call | flops 1000000000 | tf_op jit(solution)/shard_map/combine/pallas_call | solution.py:494
  (75 shorter events, 1.0 us)
Async XLA Ops:
  5.5 8.2 %copy-start.15 = (f32[1024,2]{0,1:T(2,128)S(1)}, f32[1024,2]{0,1:T(2,128)}, u32[]{:S(2)}) copy-start(f32[1024,2]{0,1:T(2,128)} %param.24) | copy-start | bytes 24580
  5.5 25.9 %all-to-all-start = ((bf16[16,32,1024]{2,1,0:T(8,128)(2,1)}), bf16[16,32,1024]{2,1,0:T(8,128)(2,1)}, u32[]{:S(2)}, u32[]{:S(2)}) async-start(bf16[16,32,1024]{2,1,0:T(8,128)(2,1)} %bitcast.72), calls=%async_computation | async-start | bytes 2097152 | tf_op jit(solution)/shard_map/all_to_all | solution.py:558
  13.7 22.1 %copy-start.9 = (f32[2048]{0:T(1024)S(1)}, f32[2048]{0:T(1024)}, u32[]{:S(2)}) copy-start(f32[2048]{0:T(1024)} %param.18) | copy-start | bytes 24580
  13.7 22.1 %copy-start.10 = (s32[3]{0:T(128)S(1)}, s32[3]{0:T(128)}, u32[]{:S(2)}) copy-start(s32[3]{0:T(128)} %pad_add_fusion.idx_ref.refs_0_) | copy-start | bytes 40
  13.7 22.1 %copy-start.11 = (f32[256]{0:T(256)S(1)}, f32[256]{0:T(256)}, u32[]{:S(2)}) copy-start(f32[256]{0:T(256)} %param.23) | copy-start | bytes 3076
  31.4 27.2 %all-to-all-start.2 = ((bf16[16,40,1024]{2,1,0:T(8,128)(2,1)}), bf16[16,40,1024]{2,1,0:T(8,128)(2,1)}, u32[]{:S(2)}, u32[]{:S(2)}) async-start(bf16[16,40,1024]{2,1,0:T(8,128)(2,1)} %bitcast.21), calls=%async_computation.2 | async-start | bytes 2621440 | tf_op jit(solution)/shard_map/all_to_all | solution.py:558
  35.9 1.2 copy-start
  37.1 1.2 copy-start.1
  38.3 1.2 copy-start.2
  39.5 17.4 %copy-start.16 = (s32[384,2]{0,1:T(2,128)S(1)}, s32[384,2]{0,1:T(2,128)}, u32[]{:S(2)}) copy-start(s32[384,2]{0,1:T(2,128)} %param.29) | copy-start | bytes 9220
  39.5 18.2 %copy-start.17 = (f32[384,2]{0,1:T(2,128)S(1)}, f32[384,2]{0,1:T(2,128)}, u32[]{:S(2)}) copy-start(f32[384,2]{0,1:T(2,128)} %param.30) | copy-start | bytes 9220
  56.9 9.2 %collective-permute-start = (bf16[512,1024]{1,0:T(8,128)(2,1)}, bf16[512,1024]{1,0:T(8,128)(2,1)}, u32[]{:S(2)}, u32[]{:S(2)}) collective-permute-start(bf16[512,1024]{1,0:T(8,128)(2,1)} %bitcast.11), channel_id=1, source_target_pairs={{0,1},{1,0},{2,3},{3,2},{4,5},{5,4},{6,7},{7,6},{8,9},{9,8},{10,11... | collective-permute-start | bytes 3145736 | tf_op jit(solution)/shard_map/ppermute | solution.py:563
  58.6 26.7 %all-to-all-start.1 = ((bf16[16,264,128]{2,1,0:T(8,128)(2,1)}), bf16[16,264,128]{2,1,0:T(8,128)(2,1)S(1)}, u32[]{:S(2)}, u32[]{:S(2)}) async-start(bf16[16,264,128]{2,1,0:T(8,128)(2,1)} %get-tuple-element.23), calls=%async_computation.1 | async-start | bytes 2162688 | tf_op jit(solution)/shard_map/all_to_all | solution.py:561
  65.7 2.4 %copy-start.19 = (bf16[2048,640]{1,0:T(8,128)(2,1)S(1)}, bf16[2048,640]{1,0:T(8,128)(2,1)}, u32[]{:S(2)}) copy-start(bf16[2048,640]{1,0:T(8,128)(2,1)} %get-tuple-element.25) | copy-start | bytes 7864324
  65.7 8.6 %collective-permute-start.6 = (bf16[640,1024]{1,0:T(8,128)(2,1)}, bf16[640,1024]{1,0:T(8,128)(2,1)S(1)}, u32[]{:S(2)}, u32[]{:S(2)}) collective-permute-start(bf16[640,1024]{1,0:T(8,128)(2,1)} %bitcast.22), channel_id=1, source_target_pairs={{0,1},{1,0},{2,3},{3,2},{4,5},{5,4},{6,7},{7,6},{8,9},{9,8},{10,11... | collective-permute-start | bytes 3932168 | tf_op jit(solution)/shard_map/ppermute | solution.py:563
  68.1 1.8 %copy-start.18 = (bf16[2048,640]{1,0:T(8,128)(2,1)S(1)}, bf16[2048,640]{1,0:T(8,128)(2,1)}, u32[]{:S(2)}) copy-start(bf16[2048,640]{1,0:T(8,128)(2,1)} %get-tuple-element.26) | copy-start | bytes 7864324
  69.9 1.9 %copy-start.22 = (bf16[640,1024]{1,0:T(8,128)(2,1)S(1)}, bf16[640,1024]{1,0:T(8,128)(2,1)}, u32[]{:S(2)}) copy-start(bf16[640,1024]{1,0:T(8,128)(2,1)} %get-tuple-element.28) | copy-start | bytes 3932164
  71.8 1.5 copy-start.20
  72.8 10.5 %collective-permute-start.1 = (bf16[512,1024]{1,0:T(8,128)(2,1)S(1)}, bf16[512,1024]{1,0:T(8,128)(2,1)S(1)}, u32[]{:S(2)}, u32[]{:S(2)}) collective-permute-start(bf16[512,1024]{1,0:T(8,128)(2,1)S(1)} %convolution_convert_fusion.3), channel_id=1, source_target_pairs={{0,1},{1,0},{2,3},{3,2},{4,5},{5,4},{6,7},{7,6},{8,9},{9,8},{10,11... | collective-permute-start | bytes 3145736 | tf_op jit(solution)/shard_map/ppermute | solution.py:567
  74.3 9.0 %copy-start.14 = (bf16[512,1024]{1,0:T(8,128)(2,1)}, bf16[512,1024]{1,0:T(8,128)(2,1)S(1)}, u32[]{:S(2)}) copy-start(bf16[512,1024]{1,0:T(8,128)(2,1)S(1)} %convolution_convert_fusion.4) | copy-start | bytes 3145732
  80.7 2.2 %copy-start.23 = (bf16[640,640]{1,0:T(8,128)(2,1)}, bf16[640,640]{1,0:T(8,128)(2,1)S(1)}, u32[]{:S(2)}) copy-start(bf16[640,640]{1,0:T(8,128)(2,1)S(1)} %multiply_convert_fusion) | copy-start | bytes 2457604
  83.0 2.4 %copy-start.12 = (f32[128]{0:T(128)S(1)}, f32[128]{0:T(128)}, u32[]{:S(2)}) copy-start(f32[128]{0:T(128)} %param.25) | copy-start | bytes 1540
  83.0 32.3 %collective-permute-start.7 = (bf16[640,1024]{1,0:T(8,128)(2,1)}, bf16[640,1024]{1,0:T(8,128)(2,1)}, u32[]{:S(2)}, u32[]{:S(2)}) collective-permute-start(bf16[640,1024]{1,0:T(8,128)(2,1)} %convolution_convert_fusion.1), channel_id=1, source_target_pairs={{0,1},{1,0},{2,3},{3,2},{4,5},{5,4},{6,7},{7,6},{8,9},{9,8},{10,11... | collective-permute-start | bytes 3932168 | tf_op jit(solution)/shard_map/ppermute | solution.py:567
  83.3 1.0 copy-start.13
  85.4 1.0 copy-start.3
  86.3 0.9 copy-start.5
  87.3 3.0 %copy-start.21 = (bf16[640,1024]{1,0:T(8,128)(2,1)S(1)}, bf16[640,1024]{1,0:T(8,128)(2,1)}, u32[]{:S(2)}) copy-start(bf16[640,1024]{1,0:T(8,128)(2,1)} %get-tuple-element.27) | copy-start | bytes 3932164
  87.3 3.0 %copy-start.24 = (bf16[640,640]{1,0:T(8,128)(2,1)S(1)}, bf16[640,640]{1,0:T(8,128)(2,1)}, u32[]{:S(2)}) copy-start(bf16[640,640]{1,0:T(8,128)(2,1)} %copy-done.23) | copy-start | bytes 2457604
  90.0 1.5 copy-start.6
  90.0 4.5 %copy-start.4 = (bf16[512,256]{1,0:T(8,128)(2,1)S(1)}, bf16[512,256]{1,0:T(8,128)(2,1)}, u32[]{:S(2)}) copy-start(bf16[512,256]{1,0:T(8,128)(2,1)} %get-tuple-element.37.refs_9_) | copy-start | bytes 786436
  90.0 6.7 %collective-permute-start.2 = (bf16[4,128,256]{2,1,0:T(8,128)(2,1)S(1)}, bf16[4,128,256]{2,1,0:T(8,128)(2,1)S(1)}, u32[]{:S(2)}, u32[]{:S(2)}) collective-permute-start(bf16[4,128,256]{2,1,0:T(8,128)(2,1)S(1)} %get-tuple-element.30), channel_id=1, source_target_pairs={{0,1},{1,0},{2,3},{3,2},{4,5},{5,4},{6,7},{7,6},{8,9},{9,8},{10,11... | collective-permute-start | bytes 786440 | tf_op jit(solution)/shard_map/ppermute | solution.py:578
  91.4 14.8 %collective-permute-start.13 = (bf16[512,256]{1,0:T(8,128)(2,1)S(1)}, bf16[512,256]{1,0:T(8,128)(2,1)S(1)}, u32[]{:S(2)}, u32[]{:S(2)}) collective-permute-start(bf16[512,256]{1,0:T(8,128)(2,1)S(1)} %copy-done.6), channel_id=1, source_target_pairs={{0,6},{2,0},{4,2},{6,4},{1,7},{3,1},{5,3},{7,5},{8,14},{10,8},{12,... | collective-permute-start | bytes 786440 | tf_op jit(solution)/shard_map/ppermute | solution.py:576
  94.5 16.0 %collective-permute-start.12 = (bf16[512,256]{1,0:T(8,128)(2,1)S(1)}, bf16[512,256]{1,0:T(8,128)(2,1)S(1)}, u32[]{:S(2)}, u32[]{:S(2)}) collective-permute-start(bf16[512,256]{1,0:T(8,128)(2,1)S(1)} %copy-done.4), channel_id=1, source_target_pairs={{0,2},{2,4},{4,6},{6,0},{1,3},{3,5},{5,7},{7,1},{8,10},{10,12},{12... | collective-permute-start | bytes 786440 | tf_op jit(solution)/shard_map/ppermute | solution.py:576
  94.5 16.0 %collective-permute-start.11 = (bf16[512,256]{1,0:T(8,128)(2,1)S(1)}, bf16[512,256]{1,0:T(8,128)(2,1)S(1)}, u32[]{:S(2)}, u32[]{:S(2)}) collective-permute-start(bf16[512,256]{1,0:T(8,128)(2,1)S(1)} %get-tuple-element.36.refs_10_), channel_id=1, source_target_pairs={{0,4},{2,6},{4,0},{6,2},{1,5},{3,7},{5,1},{7,3},{8,12},{10,14},{12... | collective-permute-start | bytes 786440 | tf_op jit(solution)/shard_map/ppermute | solution.py:576
  96.8 18.4 %collective-permute-start.3 = (bf16[2,128,256]{2,1,0:T(8,128)(2,1)S(1)}, bf16[2,128,256]{2,1,0:T(8,128)(2,1)S(1)}, u32[]{:S(2)}, u32[]{:S(2)}) collective-permute-start(bf16[2,128,256]{2,1,0:T(8,128)(2,1)S(1)} %pad_maximum_fusion.3), channel_id=1, source_target_pairs={{0,2},{2,4},{4,6},{6,0},{1,3},{3,5},{5,7},{7,1},{8,10},{10,12},{12... | collective-permute-start | bytes 393224 | tf_op jit(solution)/shard_map/ppermute | solution.py:582
  106.2 9.0 %collective-permute-start.4 = (bf16[2,128,256]{2,1,0:T(8,128)(2,1)S(1)}, bf16[2,128,256]{2,1,0:T(8,128)(2,1)S(1)}, u32[]{:S(2)}, u32[]{:S(2)}) collective-permute-start(bf16[2,128,256]{2,1,0:T(8,128)(2,1)S(1)} %pad_maximum_fusion.4), channel_id=1, source_target_pairs={{0,4},{2,6},{4,0},{6,2},{1,5},{3,7},{5,1},{7,3},{8,12},{10,14},{12... | collective-permute-start | bytes 393224 | tf_op jit(solution)/shard_map/ppermute | solution.py:582
  110.5 10.3 %collective-permute-start.5 = (bf16[2,128,256]{2,1,0:T(8,128)(2,1)S(1)}, bf16[2,128,256]{2,1,0:T(8,128)(2,1)S(1)}, u32[]{:S(2)}, u32[]{:S(2)}) collective-permute-start(bf16[2,128,256]{2,1,0:T(8,128)(2,1)S(1)} %pad_maximum_fusion.5), channel_id=1, source_target_pairs={{0,6},{2,0},{4,2},{6,4},{1,7},{3,1},{5,3},{7,5},{8,14},{10,8},{12,... | collective-permute-start | bytes 393224 | tf_op jit(solution)/shard_map/ppermute | solution.py:582
  116.7 10.7 %collective-permute-start.10 = (bf16[640,256]{1,0:T(8,128)(2,1)S(1)}, bf16[640,256]{1,0:T(8,128)(2,1)S(1)}, u32[]{:S(2)}, u32[]{:S(2)}) collective-permute-start(bf16[640,256]{1,0:T(8,128)(2,1)S(1)} %get-tuple-element.33), channel_id=1, source_target_pairs={{0,6},{2,0},{4,2},{6,4},{1,7},{3,1},{5,3},{7,5},{8,14},{10,8},{12,... | collective-permute-start | bytes 983048 | tf_op jit(solution)/shard_map/ppermute | solution.py:576
  119.3 14.8 %collective-permute-start.9 = (bf16[640,256]{1,0:T(8,128)(2,1)S(1)}, bf16[640,256]{1,0:T(8,128)(2,1)S(1)}, u32[]{:S(2)}, u32[]{:S(2)}) collective-permute-start(bf16[640,256]{1,0:T(8,128)(2,1)S(1)} %get-tuple-element.34), channel_id=1, source_target_pairs={{0,2},{2,4},{4,6},{6,0},{1,3},{3,5},{5,7},{7,1},{8,10},{10,12},{12... | collective-permute-start | bytes 983048 | tf_op jit(solution)/shard_map/ppermute | solution.py:576
  119.3 14.8 %collective-permute-start.8 = (bf16[640,256]{1,0:T(8,128)(2,1)S(1)}, bf16[640,256]{1,0:T(8,128)(2,1)S(1)}, u32[]{:S(2)}, u32[]{:S(2)}) collective-permute-start(bf16[640,256]{1,0:T(8,128)(2,1)S(1)} %get-tuple-element.32), channel_id=1, source_target_pairs={{0,4},{2,6},{4,0},{6,2},{1,5},{3,7},{5,1},{7,3},{8,12},{10,14},{12... | collective-permute-start | bytes 983048 | tf_op jit(solution)/shard_map/ppermute | solution.py:576
  136.2 17.9 %all-to-all-start.3 = ((bf16[16,72,256]{2,1,0:T(8,128)(2,1)}), bf16[16,72,256]{2,1,0:T(8,128)(2,1)S(1)}, u32[]{:S(2)}, u32[]{:S(2)}) async-start(bf16[16,72,256]{2,1,0:T(8,128)(2,1)} %pad_maximum_fusion.2), calls=%async_computation.3 | async-start | bytes 1179648 | tf_op jit(solution)/shard_map/all_to_all | solution.py:590
  143.6 10.5 %copy-start.7 = (s32[384,2]{1,0:T(8,128)S(1)}, s32[384,2]{1,0:T(8,128)}, u32[]{:S(2)}) copy-start(s32[384,2]{1,0:T(8,128)} %copy.20.routes_ref) | copy-start | bytes 9220
  143.6 10.5 %copy-start.8 = (f32[384,2]{1,0:T(8,128)S(1)}, f32[384,2]{1,0:T(8,128)}, u32[]{:S(2)}) copy-start(f32[384,2]{1,0:T(8,128)} %copy.21.logits_ref) | copy-start | bytes 9220

commit v4 on v3

--- a/solution.py
+++ b/solution.py
@@ -128,7 +128,6 @@
     wg_ref,
     wu_ref,
     wd_ref,
-    wo_ref,
     o_ref,
     qf_ref,
     qb_ref,
@@ -137,7 +136,6 @@
     wu_out,
     theirs_out,
     mine_out,
-    wo_out,
     q_s,
     v_s,
     kb_s,
@@ -149,7 +147,6 @@
     wu_s,
     theirs_s,
     mine_s,
-    wo_s,
     sems,
     *,
     steps,
@@ -172,16 +169,12 @@
         load(wg_ref.at[taken, :], wg_s.at[put, :])
         load(wu_ref.at[taken, :], wu_s.at[put, :])
     cols = wd_ref.shape[1] // (2 * groups)
-    share = wo_ref.shape[0] // groups
     for d in range(groups):
         put = slice(d * cols, (d + 1) * cols)
         block = 2 * lax.rem(chip + d, groups)
         for target, which in ((theirs_s, 1 - core), (mine_s, core)):
             taken = pl.ds(pl.multiple_of((block + which) * cols, cols), cols)
             load(wd_ref.at[:, taken], target.at[:, put])
-        source = lax.rem(chip + groups - d, groups)
-        taken = pl.ds(pl.multiple_of(source * share, share), share)
-        load(wo_ref.at[taken, :], wo_s.at[d * share : (d + 1) * share, :])
     stores = [
         pltpu.make_async_copy(source, target, sems.at[len(loads) + i])
         for i, (source, target) in enumerate(
@@ -190,7 +183,6 @@
                 (wu_s, wu_out),
                 (theirs_s, theirs_out),
                 (mine_s, mine_out),
-                (wo_s, wo_out),
             )
         )
     ]
@@ -319,7 +311,7 @@
 
 
 def local_sweeps(
-    idx, tokens, gain, wq, wf, wb, wv, floor, shift, wg, wu, wd, wo, segments, groups, deps=()
+    idx, tokens, gain, wq, wf, wb, wv, floor, shift, wg, wu, wd, segments, groups, deps=()
 ):
     seg, model = tokens.shape
     width = wq.shape[1]
@@ -330,7 +322,7 @@
     return pl.pallas_call(
         after(
             functools.partial(local_kernel, steps=steps, rows=rows, heads=heads, groups=groups),
-            13,
+            12,
             deps,
         ),
         grid=(steps,),
@@ -343,7 +335,6 @@
             jax.ShapeDtypeStruct(wu.shape, BF),
             jax.ShapeDtypeStruct((wd.shape[0], wd.shape[1] // 2), BF),
             jax.ShapeDtypeStruct((wd.shape[0], wd.shape[1] // 2), BF),
-            jax.ShapeDtypeStruct(wo.shape, BF),
         ),
         in_specs=[
             pl.BlockSpec(memory_space=pltpu.SMEM),
@@ -355,7 +346,7 @@
             whole((model, width)),
             whole((1, width)),
             pl.BlockSpec((rows, heads), lambda i: (i, 0)),
-            *any_specs((wg, wu, wd, wo)),
+            *any_specs((wg, wu, wd)),
             *any_specs(deps),
         ],
         out_specs=(
@@ -363,7 +354,7 @@
             whole((seg, width)),
             whole((seg, width)),
             whole((segments, heads * DV + 8, DK)),
-            *any_specs(range(5)),
+            *any_specs(range(4)),
         ),
         scratch_shapes=[
             pltpu.VMEM((seg, width), F32),
@@ -377,13 +368,12 @@
             pltpu.VMEM(wu.shape, BF),
             pltpu.VMEM((wd.shape[0], wd.shape[1] // 2), BF),
             pltpu.VMEM((wd.shape[0], wd.shape[1] // 2), BF),
-            pltpu.VMEM(wo.shape, BF),
-            pltpu.SemaphoreType.DMA((9 + 3 * groups,)),
+            pltpu.SemaphoreType.DMA((8 + 2 * groups,)),
         ],
         compiler_params=params(48, "arbitrary"),
         cost_estimate=cost(17),
         name="local_sweeps",
-    )(idx, tokens, gain, wq, wf, wb, wv, floor, shift, wg, wu, wd, wo, *deps)
+    )(idx, tokens, gain, wq, wf, wb, wv, floor, shift, wg, wu, wd, *deps)
 
 
 def finish_kernel(idx_ref, *refs, heads):
@@ -533,7 +523,7 @@
     wg, wu, wd = w_expert_gate[0], w_expert_up[0], w_expert_down[0]
 
     outgoing = dispatch(idx, moe_tokens, moe_gain[None], routes.T, experts)
-    o, qf, qb, message, wg, wu, wd_theirs, wd_mine, w_out_rolled = local_sweeps(
+    o, qf, qb, message, wg, wu, wd_theirs, wd_mine = local_sweeps(
         idx,
         mix_tokens,
         mix_gain[None],
@@ -546,11 +536,12 @@
         wg,
         wu,
         wd,
-        w_out,
         experts,
         groups,
         deps=outgoing,
     )
+    late_idx, qf = lax.optimization_barrier((idx, qf))
+    late_idx = jnp.maximum(late_idx, 0)
     landed = []
     arrived = []
     for rows, (_, count) in zip(outgoing, CHUNKS):
@@ -574,7 +565,7 @@
             for at in range(0, received.shape[1], cols)
         ]
         landed.append([pair[0]] + [lax.ppermute(pair[d], "y", ring(groups, d)) for d in (2, 1, 3)])
-    keep, give = finish(idx, o, qf, qb, line, head_gain[None], groups, deps=tuple(pair[1:]))
+    keep, give = finish(late_idx, o, qf, qb, line, head_gain[None], groups, deps=tuple(pair[1:]))
     given = lax.ppermute(give, "c", swap)
     lower = jnp.where(core == 0, keep, given)
     upper = jnp.where(core == 0, given, keep)
@@ -589,8 +580,13 @@
     )
     back = lax.all_to_all(shaped, EP, split_axis=0, concat_axis=0, tiled=True)
     returned = [back.reshape(-1, cols)]
-    features = jnp.concatenate([part[i] for part in moved for i in range(2)], axis=1)
-    mixed_out = dot(features, w_out_rolled).astype(BF)
+    turned = [moved[0]] + moved[:0:-1]
+    features = jnp.concatenate([part[i] for part in turned for i in range(2)], axis=1)
+    start = lax.rem(groups - chip, groups) * (features.shape[1] // groups)
+    features = lax.dynamic_slice_in_dim(
+        jnp.concatenate([features, features], axis=1), start, features.shape[1], axis=1
+    )
+    mixed_out = dot(features, w_out).astype(BF)
     moe_out = combine(routes, route_logits, returned, experts)
     return (mixed_out, moe_out)
 

time: 157 us -> 157 us (level)
  waiting for transfers between devices: 50.9 us -> 53.2 us
    ppermute x6, starting transfers between devices: 9.38 us -> 7.38 us  [body(): lax.ppermute(pair[d], 'y', ring(groups, d))]
    unnamed x60 -> x68, local copies, waits for them, and re-layouts: 8.75 us -> 8.75 us
  transfers between devices with their start and end apart: 18 -> 18, of which waited for: 7 -> 8; matrix products, arithmetic and copies ran while one was open for 18% -> 17% of each run, Pallas kernels for 13% -> 12%
where the time goes in v4:
time: 157 us; the launch traced here: 156 us
  waiting for transfers between devices  53.2 us (34%)
  starting transfers between devices  38.5 us (25%)
  Pallas kernels  25.1 us (16%)
  matrix products  19 us (12%)
  other arithmetic  10.2 us (6%)
  local copies, waits for them, and re-layouts  8.79 us (6%)
    ppermute x6, waiting for transfers between devices, body(): lax.ppermute(pair[d], 'y', ring(groups, d))  26 us
    dot_general x9, matrix products, dot(): return jnp.dot(a, b, preferred_element_type=F32)  19 us
    all_to_all x2, waiting for transfers between devices, body(): got = lax.all_to_all(shaped, EP, split_axis=0, concat_axis=0, tiled=True)  17.5 us
    pallas_call x1, Pallas kernels, local_sweeps(): pl.pallas_call(after(functools.partial(local_kernel, steps=steps, rows=ro...  16.2 us
    all_to_all x2, starting transfers between devices, body(): got = lax.all_to_all(shaped, EP, split_axis=0, concat_axis=0, tiled=True)  12.6 us
    unnamed x68, local copies, waits for them, and re-layouts  8.75 us
    all_to_all x1, starting transfers between devices, body(): back = lax.all_to_all(shaped, EP, split_axis=0, concat_axis=0, tiled=True)  8.71 us
    ppermute x6, starting transfers between devices, body(): lax.ppermute(pair[d], 'y', ring(groups, d))  7.38 us
  transfers between devices with their start and end apart: 18, of which 8 were waited for; matrix products, arithmetic and copies ran while one was open for 17% of the time, Pallas kernels for 12%

profile of v4, /device:TPU:0, one launch (start us, length us, event | category | flops | bytes accessed | tf_op | source)
XLA Modules:
  0.0 155.9 jit_solution(16988521812709757126)
XLA Ops:
  0.6 0.6 pad_add_fusion.idx_ref.refs_0_
  1.2 4.2 %dispatch.1 = (bf16[640,1024]{1,0:T(8,128)(2,1)}, bf16[512,1024]{1,0:T(8,128)(2,1)}) custom-call(s32[3]{0:T(128)} %pad_add_fusion.idx_ref.refs_0_, bf16[384,2048]{1,0:T(8,128)(2,1)} %tok_ref.1, f32[1,2048]{1,0:T(1,128)} %bitcast.94, s32[2,384]{1,0:T(2,128)} %bitcast.93), custom_call_target="tpu_custom_call" | custom-call | flops 1250000000 | tf_op jit(solution)/shard_map/dispatch/pallas_call | solution.py:96
  5.5 8.2 %all-to-all-start = ((bf16[16,32,1024]{2,1,0:T(8,128)(2,1)}), bf16[16,32,1024]{2,1,0:T(8,128)(2,1)}, u32[]{:S(2)}, u32[]{:S(2)}) async-start(bf16[16,32,1024]{2,1,0:T(8,128)(2,1)} %bitcast.87), calls=%async_computation | async-start | bytes 2097152 | tf_op jit(solution)/shard_map/all_to_all | solution.py:549
  13.9 17.5 %all-to-all-done = bf16[16,32,1024]{2,1,0:T(8,128)(2,1)} async-done(((bf16[16,32,1024]{2,1,0:T(8,128)(2,1)}), bf16[16,32,1024]{2,1,0:T(8,128)(2,1)}, u32[]{:S(2)}, u32[]{:S(2)}) %all-to-all-start) | async-done | bytes 1048608 | tf_op jit(solution)/shard_map/all_to_all | solution.py:549
  31.4 4.4 %all-to-all-start.2 = ((bf16[16,40,1024]{2,1,0:T(8,128)(2,1)}), bf16[16,40,1024]{2,1,0:T(8,128)(2,1)}, u32[]{:S(2)}, u32[]{:S(2)}) async-start(bf16[16,40,1024]{2,1,0:T(8,128)(2,1)} %bitcast.21), calls=%async_computation.2 | async-start | bytes 2621440 | tf_op jit(solution)/shard_map/all_to_all | solution.py:549
  35.8 1.2 copy-done.4
  37.0 1.2 copy-done.5
  38.2 1.2 copy-done.6
  39.5 16.2 %local_sweeps.1 = (f32[1024,256]{1,0:T(8,128)S(1)}, bf16[1024,256]{1,0:T(8,128)(2,1)S(1)}, bf16[1024,256]{1,0:T(8,128)(2,1)S(1)}, bf16[16,264,128]{2,1,0:T(8,128...) custom-call(s32[3]{0:T(128)S(1)} %copy-done.10, ...), custom_call_target="tpu_custom_call" | custom-call | flops 4249999872 | tf_op jit(solution)/shard_map/local_sweeps/pallas_call | solution.py:322
  55.8 0.8 copy.20.routes_ref
  56.6 0.8 copy.21.logits_ref
  57.4 7.1 %all-to-all-start.1 = ((bf16[16,264,128]{2,1,0:T(8,128)(2,1)}), bf16[16,264,128]{2,1,0:T(8,128)(2,1)S(1)}, u32[]{:S(2)}, u32[]{:S(2)}) async-start(bf16[16,264,128]{2,1,0:T(8,128)(2,1)} %get-tuple-element.26), calls=%async_computation.1 | async-start | bytes 2162688 | tf_op jit(solution)/shard_map/all_to_all | solution.py:552
  64.5 0.3 collective-permute-start.6
  64.8 1.9 %pad_maximum_fusion.1 = bf16[512,2048]{1,0:T(8,128)(2,1)S(1)} fusion(bf16[512,1024]{1,0:T(8,128)(2,1)} %collective-permute-done, bf16[512,1024]{1,0:T(8,128)(2,1)} %bitcast.11), kind=kLoop, calls=%fused_computation.2 | loop fusion | flops 4194304 | bytes 4194304 | tf_op jit(solution)/shard_map/concatenate | solution.py:555
  66.9 1.8 %fusion.20 = f32[512,640]{1,0:T(8,128)S(1)} fusion(bf16[512,2048]{1,0:T(8,128)(2,1)S(1)} %pad_maximum_fusion.1, bf16[2048,640]{1,0:T(8,128)(2,1)S(1)} %copy-done.19), kind=kOutput, calls=%fused_computation.55 | convolution fusion | flops 1342177280 | bytes 6029312 | tf_op jit(solution)/shard_map/dot_general | solution.py:46
  68.7 1.8 %multiply_convert_fusion.1 = bf16[512,640]{1,0:T(8,128)(2,1)S(1)} fusion(f32[512,640]{1,0:T(8,128)S(1)} %fusion.20, bf16[512,2048]{1,0:T(8,128)(2,1)S(1)} %pad_maximum_fusion.1, bf16[2048,640]{1,0:T(8,128)(2,1)S(1)} %copy-done.18), kind=kOutput, calls=%fused_computation.8 | convolution fusion | flops 1344143360 | bytes 6684672 | tf_op jit(solution)/shard_map/dot_general | solution.py:46
  70.6 1.0 convolution_convert_fusion.3
  71.6 0.5 collective-permute-start.1
  72.1 1.0 convolution_convert_fusion.4
  73.1 1.9 %pad_maximum_fusion = bf16[640,2048]{1,0:T(8,128)(2,1)S(1)} fusion(bf16[640,1024]{1,0:T(8,128)(2,1)S(1)} %collective-permute-done.6, bf16[640,1024]{1,0:T(8,128)(2,1)} %bitcast.22), kind=kLoop, calls=%fused_computation | loop fusion | flops 5242880 | bytes 5242880 | tf_op jit(solution)/shard_map/concatenate | solution.py:555
  75.0 2.2 %fusion.21 = f32[640,640]{1,0:T(8,128)S(1)} fusion(bf16[640,2048]{1,0:T(8,128)(2,1)S(1)} %pad_maximum_fusion, bf16[2048,640]{1,0:T(8,128)(2,1)S(1)} %copy-done.19), kind=kOutput, calls=%fused_computation.56 | convolution fusion | flops 1677721600 | bytes 6881280 | tf_op jit(solution)/shard_map/dot_general | solution.py:46
  77.2 2.2 %multiply_convert_fusion = bf16[640,640]{1,0:T(8,128)(2,1)S(1)} fusion(f32[640,640]{1,0:T(8,128)S(1)} %fusion.21, bf16[640,2048]{1,0:T(8,128)(2,1)S(1)} %pad_maximum_fusion, bf16[2048,640]{1,0:T(8,128)(2,1)S(1)} %copy-done.18), kind=kOutput, calls=%fused_computation.3 | convolution fusion | flops 1680179200 | bytes 7700480 | tf_op jit(solution)/shard_map/dot_general | solution.py:46
  79.5 2.3 %convolution_convert_fusion.1 = bf16[640,1024]{1,0:T(8,128)(2,1)} fusion(bf16[640,640]{1,0:T(8,128)(2,1)S(1)} %multiply_convert_fusion, bf16[640,1024]{1,0:T(8,128)(2,1)S(1)} %copy-done.22), kind=kOutput, calls=%fused_computation.4 | convolution fusion | flops 839516160 | bytes 3440640 | tf_op jit(solution)/shard_map/dot_general | solution.py:46
  81.8 0.3 collective-permute-start.7
  82.1 1.0 copy-done.13
  83.1 1.0 add_convert_fusion.7
  84.1 0.9 copy-done
  85.0 0.9 copy-done.2
  86.0 2.7 %finish.1 = (bf16[4,128,256]{2,1,0:T(8,128)(2,1)S(1)}, bf16[4,128,256]{2,1,0:T(8,128)(2,1)S(1)}) custom-call(s32[3]{0:T(128)S(1)} %broadcast_maximum_fusion.refs_0_, f32[1024,256]{1,0:T(8,128)S(1)} %get-tuple-element.22.refs_1_.refs_4_, bf16[1024,256]{1,0:T(8,128)(2,1)S(1)} %get-tuple-element.23.refs_2_.refs_5_, ...), custom_call_target="tpu_custom_call" | custom-call | flops 1000000000 | tf_op jit(solution)/shard_map/finish/pallas_call | solution.py:427
  89.0 1.2 convolution_convert_fusion.2
  90.2 3.1 %collective-permute-start.13 = (bf16[512,256]{1,0:T(8,128)(2,1)S(1)}, bf16[512,256]{1,0:T(8,128)(2,1)S(1)}, u32[]{:S(2)}, u32[]{:S(2)}) collective-permute-start(bf16[512,256]{1,0:T(8,128)(2,1)S(1)} %copy-done.3), channel_id=1, source_target_pairs={{0,6},{2,0},{4,2},{6,4},{1,7},{3,1},{5,3},{7,5},{8,14},{10,8},{12,... | collective-permute-start | bytes 786440 | tf_op jit(solution)/shard_map/ppermute | solution.py:567
  93.3 2.2 %collective-permute-start.11 = (bf16[512,256]{1,0:T(8,128)(2,1)S(1)}, bf16[512,256]{1,0:T(8,128)(2,1)S(1)}, u32[]{:S(2)}, u32[]{:S(2)}) collective-permute-start(bf16[512,256]{1,0:T(8,128)(2,1)S(1)} %get-tuple-element.38.refs_10_), channel_id=1, source_target_pairs={{0,4},{2,6},{4,0},{6,2},{1,5},{3,7},{5,1},{7,3},{8,12},{10,14},{12... | collective-permute-start | bytes 786440 | tf_op jit(solution)/shard_map/ppermute | solution.py:567
  95.6 1.1 collective-permute-start.3
  96.7 8.8 %collective-permute-done.13 = bf16[512,256]{1,0:T(8,128)(2,1)S(1)} collective-permute-done((bf16[512,256]{1,0:T(8,128)(2,1)S(1)}, bf16[512,256]{1,0:T(8,128)(2,1)S(1)}, u32[]{:S(2)}, u32[]{:S(2)}) %collective-permute-start.13) | collective-permute-done | bytes 262176 | tf_op jit(solution)/shard_map/ppermute | solution.py:567
  105.6 4.3 %collective-permute-done.12 = bf16[512,256]{1,0:T(8,128)(2,1)S(1)} collective-permute-done((bf16[512,256]{1,0:T(8,128)(2,1)S(1)}, bf16[512,256]{1,0:T(8,128)(2,1)S(1)}, u32[]{:S(2)}, u32[]{:S(2)}) %collective-permute-start.12) | collective-permute-done | bytes 262176 | tf_op jit(solution)/shard_map/ppermute | solution.py:567
  110.1 1.2 add_convert_fusion.5
  111.4 1.5 collective-permute-done.4
  112.9 3.1 %collective-permute-done.5 = bf16[2,128,256]{2,1,0:T(8,128)(2,1)S(1)} collective-permute-done((bf16[2,128,256]{2,1,0:T(8,128)(2,1)S(1)}, bf16[2,128,256]{2,1,0:T(8,128)(2,1)S(1)}, u32[]{:S(2)}, u32[]{:S(2)}) %collective-permute-start.5) | collective-permute-done | bytes 131104 | tf_op jit(solution)/shard_map/ppermute | solution.py:573
  116.2 1.4 add_convert_fusion.3
  117.7 2.0 %collective-permute-start.9 = (bf16[640,256]{1,0:T(8,128)(2,1)S(1)}, bf16[640,256]{1,0:T(8,128)(2,1)S(1)}, u32[]{:S(2)}, u32[]{:S(2)}) collective-permute-start(bf16[640,256]{1,0:T(8,128)(2,1)S(1)} %get-tuple-element.36), channel_id=1, source_target_pairs={{0,2},{2,4},{4,6},{6,0},{1,3},{3,5},{5,7},{7,1},{8,10},{10,12},{12... | collective-permute-start | bytes 983048 | tf_op jit(solution)/shard_map/ppermute | solution.py:567
  119.7 6.8 %collective-permute-done.10 = bf16[640,256]{1,0:T(8,128)(2,1)S(1)} collective-permute-done((bf16[640,256]{1,0:T(8,128)(2,1)S(1)}, bf16[640,256]{1,0:T(8,128)(2,1)S(1)}, u32[]{:S(2)}, u32[]{:S(2)}) %collective-permute-start.10) | collective-permute-done | bytes 327712 | tf_op jit(solution)/shard_map/ppermute | solution.py:567
  126.5 6.1 %collective-permute-done.9 = bf16[640,256]{1,0:T(8,128)(2,1)S(1)} collective-permute-done((bf16[640,256]{1,0:T(8,128)(2,1)S(1)}, bf16[640,256]{1,0:T(8,128)(2,1)S(1)}, u32[]{:S(2)}, u32[]{:S(2)}) %collective-permute-start.9) | collective-permute-done | bytes 327712 | tf_op jit(solution)/shard_map/ppermute | solution.py:567
  132.6 1.2 add_convert_fusion
  133.8 0.9 pad_maximum_fusion.2
  134.6 8.7 %all-to-all-start.3 = ((bf16[16,72,256]{2,1,0:T(8,128)(2,1)}), bf16[16,72,256]{2,1,0:T(8,128)(2,1)S(1)}, u32[]{:S(2)}, u32[]{:S(2)}) async-start(bf16[16,72,256]{2,1,0:T(8,128)(2,1)} %pad_maximum_fusion.2), calls=%async_computation.3 | async-start | bytes 1179648 | tf_op jit(solution)/shard_map/all_to_all | solution.py:581
  143.4 5.5 %convolution_convert_fusion = bf16[128,2048]{1,0:T(8,128)(2,1)} fusion(bf16[2048,2048]{1,0:T(8,128)(2,1)} %param.26, bf16[128,4096]{1,0:T(8,128)(2,1)S(1)} %fusion.16, s32[]{:T(128)S(6)} %select_n.18), kind=kOutput, calls=%fused_computation.1 | convolution fusion | flops 1074003968 | bytes 9437188 | tf_op jit(solution)/shard_map/dot_general | solution.py:46
  148.9 5.0 %all-to-all-done.3 = bf16[16,72,256]{2,1,0:T(8,128)(2,1)S(1)} async-done(((bf16[16,72,256]{2,1,0:T(8,128)(2,1)}), bf16[16,72,256]{2,1,0:T(8,128)(2,1)S(1)}, u32[]{:S(2)}, u32[]{:S(2)}) %all-to-all-start.3) | async-done | bytes 589856 | tf_op jit(solution)/shard_map/all_to_all | solution.py:581
  153.9 2.0 %combine.1 = bf16[384,256]{1,0:T(8,128)(2,1)} custom-call(s32[384,2]{1,0:T(8,128)S(1)} %copy-done.7, f32[384,2]{1,0:T(8,128)S(1)} %copy-done.8, bf16[1152,256]{1,0:T(8,128)(2,1)S(1)} %bitcast.83), custom_call_target="tpu_custom_call" | custom-call | flops 1000000000 | tf_op jit(solution)/shard_map/combine/pallas_call | solution.py:484
  (84 shorter events, 1.4 us)
Async XLA Ops:
  5.5 8.2 %copy-start.15 = (f32[1024,2]{0,1:T(2,128)S(1)}, f32[1024,2]{0,1:T(2,128)}, u32[]{:S(2)}) copy-start(f32[1024,2]{0,1:T(2,128)} %param.24) | copy-start | bytes 24580
  5.5 25.9 %all-to-all-start = ((bf16[16,32,1024]{2,1,0:T(8,128)(2,1)}), bf16[16,32,1024]{2,1,0:T(8,128)(2,1)}, u32[]{:S(2)}, u32[]{:S(2)}) async-start(bf16[16,32,1024]{2,1,0:T(8,128)(2,1)} %bitcast.87), calls=%async_computation | async-start | bytes 2097152 | tf_op jit(solution)/shard_map/all_to_all | solution.py:549
  13.6 22.1 %copy-start.9 = (f32[2048]{0:T(1024)S(1)}, f32[2048]{0:T(1024)}, u32[]{:S(2)}) copy-start(f32[2048]{0:T(1024)} %param.18) | copy-start | bytes 24580
  13.7 22.1 %copy-start.10 = (s32[3]{0:T(128)S(1)}, s32[3]{0:T(128)}, u32[]{:S(2)}) copy-start(s32[3]{0:T(128)} %pad_add_fusion.idx_ref.refs_0_) | copy-start | bytes 40
  13.7 22.1 %copy-start.11 = (f32[256]{0:T(256)S(1)}, f32[256]{0:T(256)}, u32[]{:S(2)}) copy-start(f32[256]{0:T(256)} %param.23) | copy-start | bytes 3076
  31.4 26.1 %all-to-all-start.2 = ((bf16[16,40,1024]{2,1,0:T(8,128)(2,1)}), bf16[16,40,1024]{2,1,0:T(8,128)(2,1)}, u32[]{:S(2)}, u32[]{:S(2)}) async-start(bf16[16,40,1024]{2,1,0:T(8,128)(2,1)} %bitcast.21), calls=%async_computation.2 | async-start | bytes 2621440 | tf_op jit(solution)/shard_map/all_to_all | solution.py:549
  35.8 1.2 copy-start.4
  37.0 1.2 copy-start.5
  38.2 1.2 copy-start.6
  39.5 16.3 %copy-start.16 = (s32[384,2]{0,1:T(2,128)S(1)}, s32[384,2]{0,1:T(2,128)}, u32[]{:S(2)}) copy-start(s32[384,2]{0,1:T(2,128)} %param.29) | copy-start | bytes 9220
  39.5 17.1 %copy-start.17 = (f32[384,2]{0,1:T(2,128)S(1)}, f32[384,2]{0,1:T(2,128)}, u32[]{:S(2)}) copy-start(f32[384,2]{0,1:T(2,128)} %param.30) | copy-start | bytes 9220
  55.7 9.1 %collective-permute-start = (bf16[512,1024]{1,0:T(8,128)(2,1)}, bf16[512,1024]{1,0:T(8,128)(2,1)}, u32[]{:S(2)}, u32[]{:S(2)}) collective-permute-start(bf16[512,1024]{1,0:T(8,128)(2,1)} %bitcast.11), channel_id=1, source_target_pairs={{0,1},{1,0},{2,3},{3,2},{4,5},{5,4},{6,7},{7,6},{8,9},{9,8},{10,11... | collective-permute-start | bytes 3145736 | tf_op jit(solution)/shard_map/ppermute | solution.py:554
  57.4 26.6 %all-to-all-start.1 = ((bf16[16,264,128]{2,1,0:T(8,128)(2,1)}), bf16[16,264,128]{2,1,0:T(8,128)(2,1)S(1)}, u32[]{:S(2)}, u32[]{:S(2)}) async-start(bf16[16,264,128]{2,1,0:T(8,128)(2,1)} %get-tuple-element.26), calls=%async_computation.1 | async-start | bytes 2162688 | tf_op jit(solution)/shard_map/all_to_all | solution.py:552
  64.5 2.4 %copy-start.19 = (bf16[2048,640]{1,0:T(8,128)(2,1)S(1)}, bf16[2048,640]{1,0:T(8,128)(2,1)}, u32[]{:S(2)}) copy-start(bf16[2048,640]{1,0:T(8,128)(2,1)} %get-tuple-element.28) | copy-start | bytes 7864324
  64.5 8.6 %collective-permute-start.6 = (bf16[640,1024]{1,0:T(8,128)(2,1)}, bf16[640,1024]{1,0:T(8,128)(2,1)S(1)}, u32[]{:S(2)}, u32[]{:S(2)}) collective-permute-start(bf16[640,1024]{1,0:T(8,128)(2,1)} %bitcast.22), channel_id=1, source_target_pairs={{0,1},{1,0},{2,3},{3,2},{4,5},{5,4},{6,7},{7,6},{8,9},{9,8},{10,11... | collective-permute-start | bytes 3932168 | tf_op jit(solution)/shard_map/ppermute | solution.py:554
  66.9 1.8 %copy-start.18 = (bf16[2048,640]{1,0:T(8,128)(2,1)S(1)}, bf16[2048,640]{1,0:T(8,128)(2,1)}, u32[]{:S(2)}) copy-start(bf16[2048,640]{1,0:T(8,128)(2,1)} %get-tuple-element.29) | copy-start | bytes 7864324
  68.7 1.8 %copy-start.22 = (bf16[640,1024]{1,0:T(8,128)(2,1)S(1)}, bf16[640,1024]{1,0:T(8,128)(2,1)}, u32[]{:S(2)}) copy-start(bf16[640,1024]{1,0:T(8,128)(2,1)} %get-tuple-element.31) | copy-start | bytes 3932164
  70.6 1.5 copy-start.20
  71.6 10.5 %collective-permute-start.1 = (bf16[512,1024]{1,0:T(8,128)(2,1)S(1)}, bf16[512,1024]{1,0:T(8,128)(2,1)S(1)}, u32[]{:S(2)}, u32[]{:S(2)}) collective-permute-start(bf16[512,1024]{1,0:T(8,128)(2,1)S(1)} %convolution_convert_fusion.3), channel_id=1, source_target_pairs={{0,1},{1,0},{2,3},{3,2},{4,5},{5,4},{6,7},{7,6},{8,9},{9,8},{10,11... | collective-permute-start | bytes 3145736 | tf_op jit(solution)/shard_map/ppermute | solution.py:558
  73.1 9.0 %copy-start.14 = (bf16[512,1024]{1,0:T(8,128)(2,1)}, bf16[512,1024]{1,0:T(8,128)(2,1)S(1)}, u32[]{:S(2)}) copy-start(bf16[512,1024]{1,0:T(8,128)(2,1)S(1)} %convolution_convert_fusion.4) | copy-start | bytes 3145732
  79.5 2.3 %copy-start.23 = (bf16[640,640]{1,0:T(8,128)(2,1)}, bf16[640,640]{1,0:T(8,128)(2,1)S(1)}, u32[]{:S(2)}) copy-start(bf16[640,640]{1,0:T(8,128)(2,1)S(1)} %multiply_convert_fusion) | copy-start | bytes 2457604
  81.8 2.3 %copy-start.12 = (f32[128]{0:T(128)S(1)}, f32[128]{0:T(128)}, u32[]{:S(2)}) copy-start(f32[128]{0:T(128)} %param.25) | copy-start | bytes 1540
  81.8 34.4 %collective-permute-start.7 = (bf16[640,1024]{1,0:T(8,128)(2,1)}, bf16[640,1024]{1,0:T(8,128)(2,1)}, u32[]{:S(2)}, u32[]{:S(2)}) collective-permute-start(bf16[640,1024]{1,0:T(8,128)(2,1)} %convolution_convert_fusion.1), channel_id=1, source_target_pairs={{0,1},{1,0},{2,3},{3,2},{4,5},{5,4},{6,7},{7,6},{8,9},{9,8},{10,11... | collective-permute-start | bytes 3932168 | tf_op jit(solution)/shard_map/ppermute | solution.py:558
  82.1 1.0 copy-start.13
  84.1 1.0 copy-start
  85.0 0.9 copy-start.2
  86.0 3.0 %copy-start.21 = (bf16[640,1024]{1,0:T(8,128)(2,1)S(1)}, bf16[640,1024]{1,0:T(8,128)(2,1)}, u32[]{:S(2)}) copy-start(bf16[640,1024]{1,0:T(8,128)(2,1)} %get-tuple-element.30) | copy-start | bytes 3932164
  86.0 3.0 %copy-start.24 = (bf16[640,640]{1,0:T(8,128)(2,1)S(1)}, bf16[640,640]{1,0:T(8,128)(2,1)}, u32[]{:S(2)}) copy-start(bf16[640,640]{1,0:T(8,128)(2,1)} %copy-done.23) | copy-start | bytes 2457604
  88.7 1.5 copy-start.3
  88.7 4.6 %copy-start.1 = (bf16[512,256]{1,0:T(8,128)(2,1)S(1)}, bf16[512,256]{1,0:T(8,128)(2,1)}, u32[]{:S(2)}) copy-start(bf16[512,256]{1,0:T(8,128)(2,1)} %get-tuple-element.39.refs_9_) | copy-start | bytes 786436
  88.7 6.8 %collective-permute-start.2 = (bf16[4,128,256]{2,1,0:T(8,128)(2,1)S(1)}, bf16[4,128,256]{2,1,0:T(8,128)(2,1)S(1)}, u32[]{:S(2)}, u32[]{:S(2)}) collective-permute-start(bf16[4,128,256]{2,1,0:T(8,128)(2,1)S(1)} %get-tuple-element.33), channel_id=1, source_target_pairs={{0,1},{1,0},{2,3},{3,2},{4,5},{5,4},{6,7},{7,6},{8,9},{9,8},{10,11... | collective-permute-start | bytes 786440 | tf_op jit(solution)/shard_map/ppermute | solution.py:569
  90.2 15.4 %collective-permute-start.13 = (bf16[512,256]{1,0:T(8,128)(2,1)S(1)}, bf16[512,256]{1,0:T(8,128)(2,1)S(1)}, u32[]{:S(2)}, u32[]{:S(2)}) collective-permute-start(bf16[512,256]{1,0:T(8,128)(2,1)S(1)} %copy-done.3), channel_id=1, source_target_pairs={{0,6},{2,0},{4,2},{6,4},{1,7},{3,1},{5,3},{7,5},{8,14},{10,8},{12,... | collective-permute-start | bytes 786440 | tf_op jit(solution)/shard_map/ppermute | solution.py:567
  93.3 16.6 %collective-permute-start.12 = (bf16[512,256]{1,0:T(8,128)(2,1)S(1)}, bf16[512,256]{1,0:T(8,128)(2,1)S(1)}, u32[]{:S(2)}, u32[]{:S(2)}) collective-permute-start(bf16[512,256]{1,0:T(8,128)(2,1)S(1)} %copy-done.1), channel_id=1, source_target_pairs={{0,2},{2,4},{4,6},{6,0},{1,3},{3,5},{5,7},{7,1},{8,10},{10,12},{12... | collective-permute-start | bytes 786440 | tf_op jit(solution)/shard_map/ppermute | solution.py:567
  93.3 16.9 %collective-permute-start.11 = (bf16[512,256]{1,0:T(8,128)(2,1)S(1)}, bf16[512,256]{1,0:T(8,128)(2,1)S(1)}, u32[]{:S(2)}, u32[]{:S(2)}) collective-permute-start(bf16[512,256]{1,0:T(8,128)(2,1)S(1)} %get-tuple-element.38.refs_10_), channel_id=1, source_target_pairs={{0,4},{2,6},{4,0},{6,2},{1,5},{3,7},{5,1},{7,3},{8,12},{10,14},{12... | collective-permute-start | bytes 786440 | tf_op jit(solution)/shard_map/ppermute | solution.py:567
  95.6 15.8 %collective-permute-start.3 = (bf16[2,128,256]{2,1,0:T(8,128)(2,1)S(1)}, bf16[2,128,256]{2,1,0:T(8,128)(2,1)S(1)}, u32[]{:S(2)}, u32[]{:S(2)}) collective-permute-start(bf16[2,128,256]{2,1,0:T(8,128)(2,1)S(1)} %pad_maximum_fusion.3), channel_id=1, source_target_pairs={{0,6},{2,0},{4,2},{6,4},{1,7},{3,1},{5,3},{7,5},{8,14},{10,8},{12,... | collective-permute-start | bytes 393224 | tf_op jit(solution)/shard_map/ppermute | solution.py:573
  105.6 7.4 %collective-permute-start.4 = (bf16[2,128,256]{2,1,0:T(8,128)(2,1)S(1)}, bf16[2,128,256]{2,1,0:T(8,128)(2,1)S(1)}, u32[]{:S(2)}, u32[]{:S(2)}) collective-permute-start(bf16[2,128,256]{2,1,0:T(8,128)(2,1)S(1)} %pad_maximum_fusion.4), channel_id=1, source_target_pairs={{0,4},{2,6},{4,0},{6,2},{1,5},{3,7},{5,1},{7,3},{8,12},{10,14},{12... | collective-permute-start | bytes 393224 | tf_op jit(solution)/shard_map/ppermute | solution.py:573
  109.9 6.2 %collective-permute-start.5 = (bf16[2,128,256]{2,1,0:T(8,128)(2,1)S(1)}, bf16[2,128,256]{2,1,0:T(8,128)(2,1)S(1)}, u32[]{:S(2)}, u32[]{:S(2)}) collective-permute-start(bf16[2,128,256]{2,1,0:T(8,128)(2,1)S(1)} %pad_maximum_fusion.5), channel_id=1, source_target_pairs={{0,2},{2,4},{4,6},{6,0},{1,3},{3,5},{5,7},{7,1},{8,10},{10,12},{12... | collective-permute-start | bytes 393224 | tf_op jit(solution)/shard_map/ppermute | solution.py:573
  117.6 8.9 %collective-permute-start.10 = (bf16[640,256]{1,0:T(8,128)(2,1)S(1)}, bf16[640,256]{1,0:T(8,128)(2,1)S(1)}, u32[]{:S(2)}, u32[]{:S(2)}) collective-permute-start(bf16[640,256]{1,0:T(8,128)(2,1)S(1)} %get-tuple-element.35), channel_id=1, source_target_pairs={{0,6},{2,0},{4,2},{6,4},{1,7},{3,1},{5,3},{7,5},{8,14},{10,8},{12,... | collective-permute-start | bytes 983048 | tf_op jit(solution)/shard_map/ppermute | solution.py:567
  117.7 14.9 %collective-permute-start.9 = (bf16[640,256]{1,0:T(8,128)(2,1)S(1)}, bf16[640,256]{1,0:T(8,128)(2,1)S(1)}, u32[]{:S(2)}, u32[]{:S(2)}) collective-permute-start(bf16[640,256]{1,0:T(8,128)(2,1)S(1)} %get-tuple-element.36), channel_id=1, source_target_pairs={{0,2},{2,4},{4,6},{6,0},{1,3},{3,5},{5,7},{7,1},{8,10},{10,12},{12... | collective-permute-start | bytes 983048 | tf_op jit(solution)/shard_map/ppermute | solution.py:567
  119.7 12.9 %collective-permute-start.8 = (bf16[640,256]{1,0:T(8,128)(2,1)S(1)}, bf16[640,256]{1,0:T(8,128)(2,1)S(1)}, u32[]{:S(2)}, u32[]{:S(2)}) collective-permute-start(bf16[640,256]{1,0:T(8,128)(2,1)S(1)} %get-tuple-element.34), channel_id=1, source_target_pairs={{0,4},{2,6},{4,0},{6,2},{1,5},{3,7},{5,1},{7,3},{8,12},{10,14},{12... | collective-permute-start | bytes 983048 | tf_op jit(solution)/shard_map/ppermute | solution.py:567
  134.6 19.2 %all-to-all-start.3 = ((bf16[16,72,256]{2,1,0:T(8,128)(2,1)}), bf16[16,72,256]{2,1,0:T(8,128)(2,1)S(1)}, u32[]{:S(2)}, u32[]{:S(2)}) async-start(bf16[16,72,256]{2,1,0:T(8,128)(2,1)} %pad_maximum_fusion.2), calls=%async_computation.3 | async-start | bytes 1179648 | tf_op jit(solution)/shard_map/all_to_all | solution.py:581
  143.4 10.5 %copy-start.7 = (s32[384,2]{1,0:T(8,128)S(1)}, s32[384,2]{1,0:T(8,128)}, u32[]{:S(2)}) copy-start(s32[384,2]{1,0:T(8,128)} %copy.20.routes_ref) | copy-start | bytes 9220
  143.4 10.5 %copy-start.8 = (f32[384,2]{1,0:T(8,128)S(1)}, f32[384,2]{1,0:T(8,128)}, u32[]{:S(2)}) copy-start(f32[384,2]{1,0:T(8,128)} %copy.21.logits_ref) | copy-start | bytes 9220
